TPU v7x, 512 devices: a whole 4x4x16 slice. The times are simulated.
512 devices in a mesh: ep: 128 (over z, x, core), tp: 4 (over y).
Axes of the slice: x: 4, y: 4, z: 16, core: 2. Of those that a mesh axis runs over, the one named last changes fastest.
Arguments:
- hidden_in: bfloat16 [2048, 1024], P('ep'), may hold values from -6 to 6
- attn_gain: float32 [1024], replicated, may hold values from 0.1 to 1.9
- w_qdown: bfloat16 [1024, 256], replicated, may hold values from -0.1875 to 0.1875
- q_gain: float32 [256], replicated, may hold values from 0.1 to 1.9
- w_qnope: bfloat16 [256, 512], replicated, may hold values from -0.375 to 0.375
- w_qrope: bfloat16 [256, 256], replicated, may hold values from -0.375 to 0.375
- w_kvdown: bfloat16 [1024, 128], replicated, may hold values from -0.1875 to 0.1875
- kv_gain: float32 [128], replicated, may hold values from 0.1 to 1.9
- w_krope: bfloat16 [1024, 32], replicated, may hold values from -0.1875 to 0.1875
- w_ukey: bfloat16 [128, 512], replicated, may hold values from -0.75 to 0.75
- w_uvalue: bfloat16 [128, 512], replicated, may hold values from -0.5 to 0.5
- w_out: bfloat16 [512, 1024], P('tp'), may hold values from -0.25 to 0.25
- cache_latent: bfloat16 [2048, 1024, 128], P(('ep', 'tp')), may hold values from -6 to 6
- cache_rope: bfloat16 [2048, 32, 1024], P(('ep', 'tp')), may hold values from -900 to 900
- lengths: int32 [2048], P(('ep', 'tp')), may hold values from 1 to 1024, as said below
- ffn_gain: float32 [1024], replicated, may hold values from 0.1 to 1.9
- routes: int32 [2048, 2], P('ep'), may hold values from 0 to 63, all different within a row; in each aligned block of 16 rows (0 to 15, 16 to 31, ...) at most 2 rows name the same one
- route_weights: float32 [2048, 2], P('ep'), may hold values from 0.25 to 1
- w_gate: bfloat16 [128, 1024, 1792], P('ep', None, 'tp'), may hold values from -0.1875 to 0.1875
- w_up: bfloat16 [128, 1024, 1792], P('ep', None, 'tp'), may hold values from -0.1875 to 0.1875
- w_down: bfloat16 [128, 1792, 1024], P('ep', 'tp'), may hold values from -0.09375 to 0.09375
Outputs:
- next_hidden: bfloat16 [2048, 1024], P('ep', 'tp')
Inputs may be any that keep to these rules, and one draw needn't show every extreme that they name: `lengths`: each sequence has 1 to 1024 valid cached positions; in every aligned block of 16 sequences one has all 1024. `routes`: each row names two different experts. In the aligned blocks of 16 rows no expert is named by more than 2 rows, and in some block one expert is named by exactly 2.
All inputs are finite; a program needn't handle non-finite values.
Results may differ from a plain program's by a relative error of at most 0.014.
The roundings to bfloat16 on the way count: a program that leaves them out, or rounds other values in their place, can miss the bound.
Values may be sent and summed in bfloat16 or wider, within the bound.
No kernel may reach another device: no remote copies, remote signals or barrier semaphores. Data moves between devices by JAX's collectives and lax.ppermute only.
A program may use at most 64 MiB of HBM per device.

v0:
```python
import jax
import jax.numpy as jnp
from jax import lax
from jax.sharding import PartitionSpec as P

HEADS = 8
NOPE = 64
ROPE = 32
VDIM = 64
KVLORA = 128


eps = 1e-06
rope_base = 10000.0


def split_up(array, dim, count):
    shape = array.shape
    pieces = array.reshape(*shape[:dim], count, shape[dim] // count, *shape[dim + 1 :])
    return jnp.moveaxis(pieces, dim, 0)


def summed_on_arrival(array, axis, dim):
    count = lax.axis_size(axis)
    pieces = lax.all_to_all(split_up(array, dim, count), axis, 0, 0, tiled=True)
    return jnp.sum(pieces.astype(jnp.float32), axis=0)


def from_everyone(array, axis):
    copies = jnp.broadcast_to(array, (lax.axis_size(axis), *array.shape))
    return lax.all_to_all(copies, axis, split_axis=0, concat_axis=0, tiled=True)


def taken_together(array, axis):
    everything = from_everyone(array, axis)
    return jnp.sum(everything.astype(jnp.float32), axis=0)


def laid_out(pieces, dim):
    shape = list(pieces.shape[1:])
    shape[dim] *= pieces.shape[0]
    return jnp.moveaxis(pieces, 0, dim).reshape(shape)


def gather_directly(array, axis, dim):
    pieces = from_everyone(array, axis)
    return laid_out(pieces, dim)


def rms_scale(values, gain):
    return values * lax.rsqrt(jnp.mean(values * values, axis=-1, keepdims=True) + eps) * gain


def rotate(values, positions):
    width = values.shape[-1]
    middle = width // 2
    inverse = jnp.power(rope_base, -jnp.arange(0, width, 2).astype(jnp.float32) / width)
    angles = positions.astype(jnp.float32)[:, None] * inverse[None, :]
    angles = jnp.concatenate([angles, angles], axis=-1)
    target = (angles.shape[0],) + (1,) * (values.ndim - 2) + (width,)
    cosine = jnp.cos(angles).reshape(target)
    sine = jnp.sin(angles).reshape(target)
    turned = jnp.concatenate([-values[..., middle:], values[..., :middle]], axis=-1)
    return values * cosine + turned * sine


def route_slots(route_table, expert_count):
    flat_ids = route_table.reshape(-1)
    onehot = (flat_ids[:, None] == jnp.arange(expert_count, dtype=jnp.int32)[None, :]).astype(
        jnp.int32
    )
    before = jnp.cumsum(onehot, axis=0) - onehot
    return jnp.sum(before * onehot, axis=1).reshape(route_table.shape)


def unit_block(arrived, w_gate, w_up, w_down):
    gate_part = jnp.einsum("scd,df->scf", arrived, w_gate[0], preferred_element_type=jnp.float32)
    up_part = jnp.einsum("scd,df->scf", arrived, w_up[0], preferred_element_type=jnp.float32)
    inner = (jax.nn.silu(gate_part) * up_part).astype(jnp.bfloat16)
    block_term = jnp.einsum("scf,fd->scd", inner, w_down[0], preferred_element_type=jnp.float32)
    summed = summed_on_arrival(block_term.astype(jnp.bfloat16), "tp", 2).astype(jnp.bfloat16)
    return lax.all_to_all(summed, "ep", split_axis=0, concat_axis=0, tiled=True)


def per_device(
    hidden_in,
    attn_gain,
    w_qdown,
    q_gain,
    w_qnope,
    w_qrope,
    w_kvdown,
    kv_gain,
    w_krope,
    w_ukey,
    w_uvalue,
    w_out,
    cache_latent,
    cache_rope,
    lengths,
    ffn_gain,
    routes,
    route_weights,
    w_gate,
    w_up,
    w_down,
):
    group_rows, width = hidden_in.shape
    own_count = lengths.shape[0]
    tp_rank = lax.axis_index("tp")
    score_scale = (NOPE + ROPE) ** (-0.5)
    own_rows = lax.dynamic_slice_in_dim(hidden_in, tp_rank * own_count, own_count, 0).astype(
        jnp.float32
    )
    normed = rms_scale(own_rows, attn_gain).astype(jnp.bfloat16)
    q_small = rms_scale(
        jnp.dot(normed, w_qdown, preferred_element_type=jnp.float32), q_gain
    ).astype(jnp.bfloat16)
    q_plain = (
        jnp.dot(q_small, w_qnope, preferred_element_type=jnp.float32)
        .astype(jnp.bfloat16)
        .reshape(own_count, HEADS, NOPE)
    )
    q_turned = rotate(
        jnp.dot(q_small, w_qrope, preferred_element_type=jnp.float32).reshape(
            own_count, HEADS, ROPE
        ),
        lengths,
    ).astype(jnp.bfloat16)
    q_latent = jnp.einsum(
        "shn,chn->shc",
        q_plain,
        w_ukey.reshape(KVLORA, HEADS, NOPE),
        preferred_element_type=jnp.float32,
    ).astype(jnp.bfloat16)
    new_latent = rms_scale(
        jnp.dot(normed, w_kvdown, preferred_element_type=jnp.float32), kv_gain
    ).astype(jnp.bfloat16)
    new_rope = rotate(jnp.dot(normed, w_krope, preferred_element_type=jnp.float32), lengths).astype(
        jnp.bfloat16
    )
    past_scores = (
        jnp.einsum("shc,spc->shp", q_latent, cache_latent, preferred_element_type=jnp.float32)
        + jnp.einsum("shr,srp->shp", q_turned, cache_rope, preferred_element_type=jnp.float32)
    ) * score_scale
    in_range = jnp.arange(cache_latent.shape[1])[None, None, :] < lengths[:, None, None]
    past_scores = jnp.where(in_range, past_scores, -1e30)
    fresh_score = (
        jnp.einsum("shc,sc->sh", q_latent, new_latent, preferred_element_type=jnp.float32)
        + jnp.einsum("shr,sr->sh", q_turned, new_rope, preferred_element_type=jnp.float32)
    ) * score_scale
    highest = jnp.maximum(jnp.max(past_scores, axis=-1), fresh_score)
    past_exp = jnp.exp(past_scores - highest[..., None])
    fresh_exp = jnp.exp(fresh_score - highest)
    divisor = jnp.sum(past_exp, axis=-1) + fresh_exp
    past_prob = (past_exp / divisor[..., None]).astype(jnp.bfloat16)
    fresh_prob = (fresh_exp / divisor).astype(jnp.bfloat16)
    latent_mix = (
        jnp.einsum("shp,spc->shc", past_prob, cache_latent, preferred_element_type=jnp.float32)
        + fresh_prob.astype(jnp.float32)[..., None] * new_latent.astype(jnp.float32)[:, None, :]
    ).astype(jnp.bfloat16)
    head_values = (
        jnp.einsum(
            "shc,chv->shv",
            latent_mix,
            w_uvalue.reshape(KVLORA, HEADS, VDIM),
            preferred_element_type=jnp.float32,
        )
        .astype(jnp.bfloat16)
        .reshape(own_count, HEADS * VDIM)
    )
    by_heads = lax.all_to_all(head_values, "tp", split_axis=1, concat_axis=0, tiled=True)
    attended = taken_together(
        jnp.dot(by_heads, w_out, preferred_element_type=jnp.float32).astype(jnp.bfloat16), "tp"
    ).astype(jnp.float32)
    residual = hidden_in.astype(jnp.float32) + attended
    normed_two = rms_scale(residual, ffn_gain).astype(jnp.bfloat16)
    unit_count = lax.axis_size("ep")
    expert_count = unit_count // 2
    capacity = max(2, 4 * group_rows // expert_count)
    quarter = width // lax.axis_size("tp")
    slots = route_slots(routes, expert_count)
    expert_of_unit = jnp.arange(unit_count, dtype=jnp.int32) // 2
    slot_range = jnp.arange(capacity, dtype=jnp.int32)
    chosen = (routes[None, None, :, :] == expert_of_unit[:, None, None, None]) & (
        slots[None, None, :, :] == slot_range[None, :, None, None]
    )
    chooser = jnp.sum(chosen.astype(jnp.int32), axis=-1).astype(jnp.bfloat16)
    columns = lax.dynamic_slice_in_dim(normed_two, tp_rank * quarter, quarter, 1)
    outgoing = jnp.einsum(
        "ucr,rd->ucd", chooser, columns, preferred_element_type=jnp.float32
    ).astype(jnp.bfloat16)
    joined = gather_directly(
        lax.all_to_all(outgoing, "ep", split_axis=0, concat_axis=0, tiled=True), "tp", 2
    )
    returned = unit_block(joined, w_gate, w_up, w_down)
    stacked = returned.reshape(unit_count * capacity, quarter)
    first_row = routes * (2 * capacity) + slots
    first_half = stacked[first_row].astype(jnp.float32)
    second_half = stacked[first_row + capacity].astype(jnp.float32)
    blended = jnp.sum(route_weights[..., None] * (first_half + second_half), axis=1)
    own_columns = lax.dynamic_slice_in_dim(residual, tp_rank * quarter, quarter, 1)
    return (own_columns + blended).astype(jnp.bfloat16)


def solution(mesh):
    placed = (
        P("ep", None),
        P(),
        P(),
        P(),
        P(),
        P(),
        P(),
        P(),
        P(),
        P(),
        P(),
        P("tp", None),
        P(("ep", "tp"), None, None),
        P(("ep", "tp"), None, None),
        P(("ep", "tp")),
        P(),
        P("ep", None),
        P("ep", None),
        P("ep", None, "tp"),
        P("ep", None, "tp"),
        P("ep", "tp", None),
    )
    return jax.shard_map(
        per_device, mesh=mesh, in_specs=placed, out_specs=P("ep", "tp"), check_vma=False
    )
```

profile of v0, /device:TPU:1, one launch (start us, length us, event | category | flops | bytes accessed | tf_op | source)
XLA Modules:
  0.0 122.5 jit_solution(15920216882785840790)
XLA Ops:
  0.0 0.8 convert_element_type.108
  0.8 0.7 iota_compare_fusion.1
  1.5 0.8 fusion.20
  2.4 1.1 fusion.50
  3.4 1.4 %multiply_reduce_fusion.2 = (f32[4]{0:T(128)S(1)}, f32[4,256]{1,0:T(4,128)S(1)}) fusion(bf16[1024,256]{1,0:T(8,128)(2,1)} %param.23, f32[1024]{0:T(1024)S(1)} %copy-done.8, f32[4]{0:T(128)S(1)} %add_rsqrt_fusion.3, bf16[16,1024]{1,0:T(8,128)(2,1)S(1)} %copy-done.6, s32[]{:T(128)S(6)} %select_n.26), kind=kOutput, calls=%fused_computation.67 | convolution fusion | flops 2115580 | bytes 541204 | tf_op jit(solution)/shard_map/dot_general | solution.py:117
  4.9 0.7 copy-done.15
  5.5 0.2 fusion.49
  5.7 0.1 reshape.181
  5.9 0.2 convolution_convert_fusion.5
  6.1 0.1 reshape.179
  6.2 0.6 copy-done.4
  6.7 0.1 copy.98
  6.9 0.1 fusion.43
  7.0 0.1 fusion.24
  7.1 0.2 fusion.58
  7.3 0.1 fusion.38
  7.4 0.4 copy-done.13
  7.8 0.3 multiply_reduce_fusion.3
  8.1 0.2 fusion.4
  8.3 0.7 copy-done.10
  9.0 0.1 fusion.33
  9.1 0.5 fusion.57
  9.6 0.2 fusion.17
  9.8 0.7 copy-done.5
  10.5 0.1 copy.101
  10.6 0.3 fusion.3
  11.0 0.2 fusion.5
  11.1 0.1 all_to_all.29
  11.2 0.6 copy.104
  11.8 5.0 %all-to-all-start = ((bf16[4,4,128]{2,0,1:T(4,128)(2,1)}), bf16[4,4,128]{2,0,1:T(4,128)(2,1)S(1)}, u32[]{:S(2)}, u32[]{:S(2)}) async-start(bf16[4,4,128]{2,0,1:T(4,128)(2,1)} %copy.104), calls=%async_computation | async-start | bytes 8192 | tf_op jit(solution)/shard_map/all_to_all | solution.py:172
  16.9 0.1 copy.106
  16.9 0.1 eq.56
  17.2 0.2 select_reduce_fusion
  17.3 0.1 eq.60
  17.4 0.1 copy.107
  17.6 0.8 dynamic-slice
  18.4 2.6 %all-to-all-done = bf16[4,4,128]{2,0,1:T(4,128)(2,1)S(1)} async-done(((bf16[4,4,128]{2,0,1:T(4,128)(2,1)}), bf16[4,4,128]{2,0,1:T(4,128)(2,1)S(1)}, u32[]{:S(2)}, u32[]{:S(2)}) %all-to-all-start) | async-done | bytes 4128 | tf_op jit(solution)/shard_map/all_to_all | solution.py:172
  21.0 0.1 convolution_convert_fusion.2
  21.1 0.7 broadcast_in_dim.22
  21.8 3.3 %all-to-all-start.1 = ((bf16[4,16,1024]{2,1,0:T(8,128)(2,1)}), bf16[4,16,1024]{2,1,0:T(8,128)(2,1)S(1)}, u32[]{:S(2)}, u32[]{:S(2)}) async-start(bf16[4,16,1024]{2,1,0:T(8,128)(2,1)} %broadcast_in_dim.22), calls=%async_computation.1 | async-start | bytes 262144 | tf_op jit(solution)/shard_map/all_to_all | solution.py:31
  25.2 4.7 %all-to-all-done.1 = bf16[4,16,1024]{2,1,0:T(8,128)(2,1)S(1)} async-done(((bf16[4,16,1024]{2,1,0:T(8,128)(2,1)}), bf16[4,16,1024]{2,1,0:T(8,128)(2,1)S(1)}, u32[]{:S(2)}, u32[]{:S(2)}) %all-to-all-start.1) | async-done | bytes 131104 | tf_op jit(solution)/shard_map/all_to_all | solution.py:31
  29.9 0.1 multiply_reduce_fusion
  30.1 0.2 convolution_convert_fusion.1
  30.3 0.1 copy.108
  30.5 38.3 %all_to_all.44 = bf16[128,2,256]{2,1,0:T(2,128)(2,1)S(1)} all-to-all(bf16[128,2,256]{2,1,0:T(2,128)(2,1)S(1)} %copy.108), channel_id=1, replica_groups=mesh['ep'=128,'tp'=4] {'ep'}, dimensions={0} | all-to-all | bytes 262144 | tf_op jit(solution)/shard_map/all_to_all | solution.py:194
  68.8 11.7 %all_to_all.45 = bf16[4,128,2,256]{3,1,2,0:T(8,128)(2,1)S(1)} all-to-all(bf16[4,128,2,256]{3,1,2,0:T(8,128)(2,1)S(1)} %broadcast_in_dim.23), channel_id=1, replica_groups=mesh['ep'=128,'tp'=4] {'tp'}, dimensions={0} | all-to-all | bytes 1048576 | tf_op jit(solution)/shard_map/all_to_all | solution.py:31
  80.6 0.4 fusion.9
  81.1 0.7 copy-done.11
  81.8 2.5 %convolution_convert_fusion = bf16[128,2,1024]{2,0,1:T(8,128)(2,1)S(1)} fusion(bf16[128,2,1024]{2,0,1:T(8,128)(2,1)S(1)} %bitcast.61, bf16[1,448,1024]{2,1,0:T(8,128)(2,1)S(1)} %copy-done.11, bf16[1,1024,448]{1,2,0:T(8,128)(2,1)} %param.40, f32[128,2,448]{0,2,1:T(8,128)S(1)} %fusion.9), kind=kOutput, calls=%fused_computation.2 | convolution fusion | flops 470712320 | bytes 3342336 | tf_op jit(solution)/shard_map/scf,fd->scd/dot_general | solution.py:80
  84.3 10.7 %all_to_all.46 = bf16[4,128,2,256]{3,1,2,0:T(8,128)(2,1)S(1)} all-to-all(bf16[4,128,2,256]{3,1,2,0:T(8,128)(2,1)S(1)} %bitcast.59), channel_id=1, replica_groups=mesh['ep'=128,'tp'=4] {'tp'}, dimensions={0} | all-to-all | bytes 1048576 | tf_op jit(solution)/shard_map/all_to_all | solution.py:25
  95.0 0.1 reduce_sum.101
  95.1 0.8 copy.113
  95.9 8.5 %all-to-all-start.5 = ((bf16[128,2,256]{2,1,0:T(2,128)(2,1)}), bf16[128,2,256]{2,1,0:T(2,128)(2,1)S(1)}, u32[]{:S(2)}, u32[]{:S(2)}) async-start(bf16[128,2,256]{2,1,0:T(2,128)(2,1)} %copy.113), calls=%async_computation.5 | async-start | bytes 262144 | tf_op jit(solution)/shard_map/all_to_all | solution.py:82
  104.4 0.1 copy.115
  104.5 0.1 reshape.188
  104.6 0.1 copy.116
  104.7 0.1 reshape.196
  104.8 0.6 copy-done.9
  105.4 0.1 copy.105
  105.5 14.9 %all-to-all-done.5 = bf16[128,2,256]{2,1,0:T(2,128)(2,1)S(1)} async-done(((bf16[128,2,256]{2,1,0:T(2,128)(2,1)}), bf16[128,2,256]{2,1,0:T(2,128)(2,1)S(1)}, u32[]{:S(2)}, u32[]{:S(2)}) %all-to-all-start.5) | async-done | bytes 131104 | tf_op jit(solution)/shard_map/all_to_all | solution.py:82
  120.5 0.6 gather_fusion
  121.1 0.6 gather_fusion.1
  121.8 0.1 multiply_reduce_fusion.1
  121.9 0.6 add_convert_fusion
  (53 shorter events, 0.9 us)
Async XLA Ops:
  0.0 9.1 %copy-start = (bf16[4,1024,128]{2,1,0:T(8,128)(2,1)S(1)}, bf16[4,1024,128]{2,1,0:T(8,128)(2,1)}, u32[]{:S(2)}) copy-start(bf16[4,1024,128]{2,1,0:T(8,128)(2,1)} %param.33) | copy-start | bytes 3145732
  0.0 2.3 %copy-start.6 = (bf16[16,1024]{1,0:T(8,128)(2,1)S(1)}, bf16[16,1024]{1,0:T(8,128)(2,1)}, u32[]{:S(2)}) copy-start(bf16[16,1024]{1,0:T(8,128)(2,1)} %param.21) | copy-start | bytes 98308
  2.4 1.1 copy-start.8
  3.4 1.5 %copy-start.14 = (bf16[256,256]{1,0:T(8,128)(2,1)S(1)}, bf16[256,256]{1,0:T(8,128)(2,1)}, u32[]{:S(2)}) copy-start(bf16[256,256]{1,0:T(8,128)(2,1)} %param.26) | copy-start | bytes 393220
  3.4 2.5 %copy-start.12 = (bf16[256,512]{1,0:T(8,128)(2,1)S(1)}, bf16[256,512]{1,0:T(8,128)(2,1)}, u32[]{:S(2)}) copy-start(bf16[256,512]{1,0:T(8,128)(2,1)} %param.25) | copy-start | bytes 786436
  4.9 0.7 copy-start.15
  5.8 0.9 copy-start.4
  5.9 1.3 %copy-start.3 = (bf16[4,32,1024]{2,1,0:T(8,128)(2,1)S(1)}, bf16[4,32,1024]{2,1,0:T(8,128)(2,1)}, u32[]{:S(2)}) copy-start(bf16[4,32,1024]{2,1,0:T(8,128)(2,1)} %param.34) | copy-start | bytes 786436
  6.8 1.0 copy-start.13
  8.3 0.7 copy-start.10
  9.6 0.9 copy-start.5
  10.6 6.2 %copy-start.7 = (s32[16,2]{0,1:T(2,128)S(1)}, s32[16,2]{0,1:T(2,128)}, u32[]{:S(2)}) copy-start(s32[16,2]{0,1:T(2,128)} %param.37) | copy-start | bytes 388
  11.0 10.0 %copy-start.2 = (bf16[128,1024]{1,0:T(8,128)(2,1)S(1)}, bf16[128,1024]{1,0:T(8,128)(2,1)}, u32[]{:S(2)}) copy-start(bf16[128,1024]{1,0:T(8,128)(2,1)} %param.32) | copy-start | bytes 786436
  11.8 9.1 %all-to-all-start = ((bf16[4,4,128]{2,0,1:T(4,128)(2,1)}), bf16[4,4,128]{2,0,1:T(4,128)(2,1)S(1)}, u32[]{:S(2)}, u32[]{:S(2)}) async-start(bf16[4,4,128]{2,0,1:T(4,128)(2,1)} %copy.104), calls=%async_computation | async-start | bytes 8192 | tf_op jit(solution)/shard_map/all_to_all | solution.py:172
  21.8 8.1 %all-to-all-start.1 = ((bf16[4,16,1024]{2,1,0:T(8,128)(2,1)}), bf16[4,16,1024]{2,1,0:T(8,128)(2,1)S(1)}, u32[]{:S(2)}, u32[]{:S(2)}) async-start(bf16[4,16,1024]{2,1,0:T(8,128)(2,1)} %broadcast_in_dim.22), calls=%async_computation.1 | async-start | bytes 262144 | tf_op jit(solution)/shard_map/all_to_all | solution.py:31
  68.8 11.8 %copy-start.1 = (bf16[1,1024,448]{1,2,0:T(8,128)(2,1)S(1)}, bf16[1,1024,448]{1,2,0:T(8,128)(2,1)}, u32[]{:S(2)}) copy-start(bf16[1,1024,448]{1,2,0:T(8,128)(2,1)} %param.39) | copy-start | bytes 2752516
  80.6 1.2 copy-start.11
  95.9 24.5 %all-to-all-start.5 = ((bf16[128,2,256]{2,1,0:T(2,128)(2,1)}), bf16[128,2,256]{2,1,0:T(2,128)(2,1)S(1)}, u32[]{:S(2)}, u32[]{:S(2)}) async-start(bf16[128,2,256]{2,1,0:T(2,128)(2,1)} %copy.113), calls=%async_computation.5 | async-start | bytes 262144 | tf_op jit(solution)/shard_map/all_to_all | solution.py:82
  104.7 0.7 copy-start.9
where the time goes:
time: 123 us
  blocking collectives  60.7 us (49%)
  waiting for transfers between devices  22.3 us (18%)
  starting transfers between devices  16.8 us (14%)
  local copies, waits for them, and re-layouts  10 us (8%)
  matrix products  7.94 us (6%)
  other arithmetic  4.43 us (4%)
    all_to_all x1, blocking collectives, per_device(): lax.all_to_all(outgoing, 'ep', split_axis=0, concat_axis=0, tiled=True)  38.3 us
    all_to_all x1, waiting for transfers between devices, unit_block(): return lax.all_to_all(summed, 'ep', split_axis=0, concat_axis=0, tiled=True)  14.9 us
    all_to_all x1, blocking collectives, from_everyone(): return lax.all_to_all(copies, axis, split_axis=0, concat_axis=0, tiled=True)  11.7 us
    all_to_all x1, blocking collectives, summed_on_arrival(): pieces = lax.all_to_all(split_up(array, dim, count), axis, 0, 0, tiled=True)  10.7 us
    all_to_all x1, starting transfers between devices, unit_block(): return lax.all_to_all(summed, 'ep', split_axis=0, concat_axis=0, tiled=True)  8.52 us
    all_to_all x1, starting transfers between devices, per_device(): lax.all_to_all(head_values, 'tp', split_axis=1, concat_axis=0, tiled=True)  5 us
    unnamed x36, local copies, waits for them, and re-layouts  4.74 us
    all_to_all x1, waiting for transfers between devices, from_everyone(): return lax.all_to_all(copies, axis, split_axis=0, concat_axis=0, tiled=True)  4.71 us
  transfers between devices with their start and end apart: 3, of which 3 were waited for; matrix products, arithmetic and copies ran while one was open for 2% of the time, Pallas kernels for 0%

commit v1 on v0

v1 whole, which is shorter than its diff:
```python
import jax
import jax.numpy as jnp
from jax import lax
from jax.sharding import PartitionSpec as P

HEADS = 8
NOPE = 64
ROPE = 32
VDIM = 64
KVLORA = 128

eps = 1e-06
rope_base = 10000.0


def rms_scale(values, gain):
    return values * lax.rsqrt(jnp.mean(values * values, axis=-1, keepdims=True) + eps) * gain


def rotate(values, positions):
    width = values.shape[-1]
    middle = width // 2
    inverse = jnp.power(rope_base, -jnp.arange(0, width, 2).astype(jnp.float32) / width)
    angles = positions.astype(jnp.float32)[:, None] * inverse[None, :]
    angles = jnp.concatenate([angles, angles], axis=-1)
    target = (angles.shape[0],) + (1,) * (values.ndim - 2) + (width,)
    cosine = jnp.cos(angles).reshape(target)
    sine = jnp.sin(angles).reshape(target)
    turned = jnp.concatenate([-values[..., middle:], values[..., :middle]], axis=-1)
    return values * cosine + turned * sine


def route_slots(route_table, expert_count):
    flat_ids = route_table.reshape(-1)
    order = jnp.arange(flat_ids.shape[0])
    same = (flat_ids[:, None] == flat_ids[None, :]) & (order[None, :] < order[:, None])
    return jnp.sum(same.astype(jnp.int32), axis=1).reshape(route_table.shape)


def from_everyone(array, axis):
    copies = jnp.broadcast_to(array, (lax.axis_size(axis), *array.shape))
    return lax.all_to_all(copies, axis, split_axis=0, concat_axis=0, tiled=True)


def attention(own_rows, attn_gain, w_qdown, q_gain, w_qnope, w_qrope, w_kvdown, kv_gain, w_krope,
              w_ukey, w_uvalue, cache_latent, cache_rope, lengths):
    own_count = lengths.shape[0]
    score_scale = (NOPE + ROPE) ** (-0.5)
    normed = rms_scale(own_rows, attn_gain).astype(jnp.bfloat16)
    q_small = rms_scale(
        jnp.dot(normed, w_qdown, preferred_element_type=jnp.float32), q_gain
    ).astype(jnp.bfloat16)
    q_plain = (
        jnp.dot(q_small, w_qnope, preferred_element_type=jnp.float32)
        .astype(jnp.bfloat16)
        .reshape(own_count, HEADS, NOPE)
    )
    q_turned = rotate(
        jnp.dot(q_small, w_qrope, preferred_element_type=jnp.float32).reshape(
            own_count, HEADS, ROPE
        ),
        lengths,
    ).astype(jnp.bfloat16)
    q_latent = jnp.einsum(
        "shn,chn->shc",
        q_plain,
        w_ukey.reshape(KVLORA, HEADS, NOPE),
        preferred_element_type=jnp.float32,
    ).astype(jnp.bfloat16)
    new_latent = rms_scale(
        jnp.dot(normed, w_kvdown, preferred_element_type=jnp.float32), kv_gain
    ).astype(jnp.bfloat16)
    new_rope = rotate(jnp.dot(normed, w_krope, preferred_element_type=jnp.float32), lengths).astype(
        jnp.bfloat16
    )
    past_scores = (
        jnp.einsum("shc,spc->shp", q_latent, cache_latent, preferred_element_type=jnp.float32)
        + jnp.einsum("shr,srp->shp", q_turned, cache_rope, preferred_element_type=jnp.float32)
    ) * score_scale
    in_range = jnp.arange(cache_latent.shape[1])[None, None, :] < lengths[:, None, None]
    past_scores = jnp.where(in_range, past_scores, -1e30)
    fresh_score = (
        jnp.einsum("shc,sc->sh", q_latent, new_latent, preferred_element_type=jnp.float32)
        + jnp.einsum("shr,sr->sh", q_turned, new_rope, preferred_element_type=jnp.float32)
    ) * score_scale
    highest = jnp.maximum(jnp.max(past_scores, axis=-1), fresh_score)
    past_exp = jnp.exp(past_scores - highest[..., None])
    fresh_exp = jnp.exp(fresh_score - highest)
    divisor = jnp.sum(past_exp, axis=-1) + fresh_exp
    past_prob = (past_exp / divisor[..., None]).astype(jnp.bfloat16)
    fresh_prob = (fresh_exp / divisor).astype(jnp.bfloat16)
    latent_mix = (
        jnp.einsum("shp,spc->shc", past_prob, cache_latent, preferred_element_type=jnp.float32)
        + fresh_prob.astype(jnp.float32)[..., None] * new_latent.astype(jnp.float32)[:, None, :]
    ).astype(jnp.bfloat16)
    return (
        jnp.einsum(
            "shc,chv->shv",
            latent_mix,
            w_uvalue.reshape(KVLORA, HEADS, VDIM),
            preferred_element_type=jnp.float32,
        )
        .astype(jnp.bfloat16)
        .reshape(own_count, HEADS * VDIM)
    )


def per_device(
    hidden_in, attn_gain, w_qdown, q_gain, w_qnope, w_qrope, w_kvdown, kv_gain, w_krope, w_ukey,
    w_uvalue, w_out, cache_latent, cache_rope, lengths, ffn_gain, routes, route_weights, w_gate,
    w_up, w_down,
):
    group_rows, width = hidden_in.shape
    own_count = lengths.shape[0]
    tp = lax.axis_size("tp")
    ep = lax.axis_size("ep")
    experts = ep // 2
    capacity = 2
    quarter = width // tp
    block = quarter // 2
    tp_rank = lax.axis_index("tp")
    core = lax.axis_index("ep") % 2
    columns = [[(2 * k + c) * tp + t for c in range(2) for t in range(tp)] for k in range(experts)]
    same_core = [[2 * k + c for k in range(experts)] for c in range(2)]
    pairs = [[2 * k, 2 * k + 1] for k in range(experts)]

    w_all = from_everyone(w_out, "tp")
    own_rows = lax.dynamic_slice_in_dim(hidden_in, tp_rank * own_count, own_count, 0).astype(
        jnp.float32
    )
    head_values = attention(
        own_rows, attn_gain, w_qdown, q_gain, w_qnope, w_qrope, w_kvdown, kv_gain, w_krope,
        w_ukey, w_uvalue, cache_latent, cache_rope, lengths,
    )
    terms = jnp.einsum(
        "sbf,bfd->bsd",
        head_values.reshape(own_count, tp, -1),
        w_all,
        preferred_element_type=jnp.float32,
    ).astype(jnp.bfloat16)
    attended = jnp.sum(terms.astype(jnp.float32), axis=0)
    residual = own_rows + attended
    normed_two = rms_scale(residual, ffn_gain).astype(jnp.bfloat16)

    slots = route_slots(routes, experts)
    targets = routes * (2 * capacity) + core * capacity + slots
    meta = jnp.concatenate([targets.astype(jnp.float32), route_weights], axis=1)
    meta = lax.dynamic_slice_in_dim(meta, tp_rank * own_count, own_count, 0)
    meta = jnp.pad(meta, ((0, 0), (0, 124)))
    normed_blocks = normed_two.astype(jnp.float32).reshape(own_count, tp, 2, block)
    outgoing = jnp.concatenate(
        [
            jnp.broadcast_to(
                residual.reshape(own_count, tp, quarter).transpose(1, 0, 2)[None],
                (2, tp, own_count, quarter),
            ),
            normed_blocks.transpose(2, 1, 0, 3),
            jnp.broadcast_to(meta[None, None], (2, tp, own_count, 128)),
        ],
        axis=-1,
    ).reshape(2 * tp, own_count, quarter + block + 128)
    inbox = lax.all_to_all(
        outgoing, ("ep", "tp"), 0, 0, axis_index_groups=columns, tiled=True
    ).reshape(2 * group_rows, quarter + block + 128)
    own_columns = lax.dynamic_slice_in_dim(inbox, core * group_rows, group_rows, 0)[:, :quarter]
    chip_rows = inbox[:, quarter : quarter + block].astype(jnp.bfloat16)
    chip_targets = inbox[:, quarter + block : quarter + block + 2].astype(jnp.int32)
    chip_weights = inbox[:, quarter + block + 2 : quarter + block + 4]

    rows = experts * 2 * capacity
    picks = chip_targets[:, :, None] == jnp.arange(rows)[None, None, :]
    chooser = jnp.sum(picks.astype(jnp.float32), axis=1).astype(jnp.bfloat16)
    sent = jnp.einsum("ru,rd->ud", chooser, chip_rows, preferred_element_type=jnp.float32).astype(
        jnp.bfloat16
    )
    arrived = lax.all_to_all(
        sent.reshape(experts, 2 * capacity, block), "ep", 0, 0, axis_index_groups=same_core,
        tiled=True,
    ).reshape(rows, block)
    over_tp = from_everyone(arrived, "tp")
    both = lax.all_gather(over_tp, "ep", axis_index_groups=pairs)
    joined = both.transpose(2, 1, 0, 3).reshape(rows, width)
    gate_part = jnp.dot(joined, w_gate[0], preferred_element_type=jnp.float32)
    up_part = jnp.dot(joined, w_up[0], preferred_element_type=jnp.float32)
    inner = (jax.nn.silu(gate_part) * up_part).astype(jnp.bfloat16)
    block_term = jnp.dot(inner, w_down[0], preferred_element_type=jnp.float32).astype(jnp.bfloat16)
    pieces = lax.all_to_all(
        block_term.reshape(rows, tp, quarter).transpose(1, 0, 2), "tp", 0, 0, tiled=True
    )
    half_out = jnp.sum(pieces.astype(jnp.float32), axis=0).astype(jnp.bfloat16)
    returned = lax.all_to_all(
        half_out.reshape(experts, 2 * capacity, quarter), "ep", 0, 0, axis_index_groups=same_core,
        tiled=True,
    ).reshape(rows, quarter)
    chosen = jnp.einsum(
        "rku,ud->rkd", picks.astype(jnp.bfloat16), returned, preferred_element_type=jnp.float32
    )
    blended = jnp.sum(chip_weights[:, :, None] * chosen, axis=1)
    others = lax.dynamic_slice_in_dim(blended, (1 - core) * group_rows, group_rows, 0)
    mine = lax.dynamic_slice_in_dim(blended, core * group_rows, group_rows, 0)
    swapped = lax.all_gather(others, "ep", axis_index_groups=pairs)
    partner = lax.dynamic_index_in_dim(swapped, 1 - core, 0, keepdims=False)
    return (own_columns + (mine + partner)).astype(jnp.bfloat16)


def solution(mesh):
    placed = (
        P("ep", None),
        P(),
        P(),
        P(),
        P(),
        P(),
        P(),
        P(),
        P(),
        P(),
        P(),
        P("tp", None),
        P(("ep", "tp"), None, None),
        P(("ep", "tp"), None, None),
        P(("ep", "tp")),
        P(),
        P("ep", None),
        P("ep", None),
        P("ep", None, "tp"),
        P("ep", None, "tp"),
        P("ep", "tp", None),
    )
    return jax.shard_map(
        per_device, mesh=mesh, in_specs=placed, out_specs=P("ep", "tp"), check_vma=False
    )
```

time: 123 us -> 120 us (0.976)
  blocking collectives: 60.7 us -> 74.2 us
  starting transfers between devices: 16.8 us -> 9.72 us
  waiting for transfers between devices: 22.3 us -> 15.5 us
  other arithmetic: 4.43 us -> 2.05 us
  matrix products: 7.94 us -> 6.42 us
    all_gather x0 -> x2, blocking collectives: none -> 9.66 us  [the longest x1 5.06 us: per_device(): both = lax.all_gather(over_tp, 'ep', axis_index_groups=pairs)]
    all_to_all x2 -> x1, starting transfers between devices: 13.5 us -> 4.59 us  [per_device(): lax.all_to_all(half_out.reshape(experts, 2 * capacity, quarter), 'ep', 0,...]
    all_to_all x2 -> x3, blocking collectives: 49 us -> 56.6 us  [the longest x1 30.1 us: per_device(): lax.all_to_all(sent.reshape(experts, 2 * capacity, block), 'ep', 0, 0, ax...]
    all_to_all x1, waiting for transfers between devices: 4.71 us -> 0.01 us  [from_everyone(): return lax.all_to_all(copies, axis, split_axis=0, concat_axis=0, tiled=True)]
    all_to_all x1, blocking collectives: 11.7 us -> 7.92 us  [from_everyone(): return lax.all_to_all(copies, axis, split_axis=0, concat_axis=0, tiled=True)]
    unnamed x36 -> x45, local copies, waits for them, and re-layouts: 4.74 us -> 7.25 us
    all_to_all x2 -> x1, waiting for transfers between devices: 17.6 us -> 15.5 us  [per_device(): lax.all_to_all(half_out.reshape(experts, 2 * capacity, quarter), 'ep', 0,...]
    all_to_all x1, starting transfers between devices: 3.32 us -> 5.13 us  [from_everyone(): return lax.all_to_all(copies, axis, split_axis=0, concat_axis=0, tiled=True)]
  transfers between devices with their start and end apart: 3 -> 2, of which waited for: 3 -> 1; matrix products, arithmetic and copies ran while one was open for 2% -> 4% of each run, Pallas kernels for 0% -> 0%
where the time goes in v1:
time: 120 us; the launch traced here: 119 us
  blocking collectives  74.2 us (62%)
  waiting for transfers between devices  15.5 us (13%)
  local copies, waits for them, and re-layouts  11.2 us (9%)
  starting transfers between devices  9.72 us (8%)
  matrix products  6.42 us (5%)
  other arithmetic  2.05 us (2%)
    all_to_all x1, blocking collectives, per_device(): lax.all_to_all(sent.reshape(experts, 2 * capacity, block), 'ep', 0, 0, ax...  30.1 us
    all_to_all x1, waiting for transfers between devices, per_device(): lax.all_to_all(half_out.reshape(experts, 2 * capacity, quarter), 'ep', 0,...  15.5 us
    all_to_all x1, blocking collectives, per_device(): lax.all_to_all(outgoing, ('ep', 'tp'), 0, 0, axis_index_groups=columns, t...  14.9 us
    all_to_all x1, blocking collectives, per_device(): lax.all_to_all(block_term.reshape(rows, tp, quarter).transpose(1, 0, 2),...  11.6 us
    all_to_all x1, blocking collectives, from_everyone(): return lax.all_to_all(copies, axis, split_axis=0, concat_axis=0, tiled=True)  7.92 us
    unnamed x45, local copies, waits for them, and re-layouts  7.25 us
    all_to_all x1, starting transfers between devices, from_everyone(): return lax.all_to_all(copies, axis, split_axis=0, concat_axis=0, tiled=True)  5.13 us
    all_gather x1, blocking collectives, per_device(): both = lax.all_gather(over_tp, 'ep', axis_index_groups=pairs)  5.06 us
  transfers between devices with their start and end apart: 2, of which 1 were waited for; matrix products, arithmetic and copies ran while one was open for 4% of the time, Pallas kernels for 0%

profile of v1, /device:TPU:1, one launch (start us, length us, event | category | flops | bytes accessed | tf_op | source)
XLA Modules:
  0.0 119.4 jit_solution(14610091435894286966)
XLA Ops:
  0.0 2.1 %broadcast_in_dim.22 = bf16[4,128,1024]{2,1,0:T(8,128)(2,1)} broadcast(bf16[128,1024]{1,0:T(8,128)(2,1)} %param.32), dimensions={1,2} | broadcast | bytes 1310720 | tf_op jit(solution)/shard_map/broadcast_in_dim | solution.py:41
  2.2 5.1 %all-to-all-start = ((bf16[4,128,1024]{2,1,0:T(8,128)(2,1)}), bf16[4,128,1024]{2,1,0:T(8,128)(2,1)S(1)}, u32[]{:S(2)}, u32[]{:S(2)}) async-start(bf16[4,128,1024]{2,1,0:T(8,128)(2,1)} %broadcast_in_dim.22), calls=%async_computation | async-start | bytes 2097152 | tf_op jit(solution)/shard_map/all_to_all | solution.py:42
  7.3 0.1 iota_compare_fusion.3
  7.4 0.7 copy-done.6
  8.0 0.1 fusion.24
  8.2 0.5 copy-done.7
  8.7 0.2 fusion.52
  8.9 0.3 multiply_reduce_fusion.1
  9.3 0.6 copy-done.17
  9.8 0.1 copy-done.19
  10.0 0.2 fusion.51
  10.1 0.1 reshape.176
  10.3 0.2 convolution_convert_fusion.5
  10.5 0.1 reshape.174
  10.6 0.6 copy-done.4
  11.1 0.1 copy.122
  11.3 0.1 slice_negate_fusion.1
  11.3 0.1 fusion.46
  11.5 0.1 fusion.29
  11.6 0.2 fusion.61
  11.7 0.1 fusion.41
  11.8 0.4 copy-done.16
  12.2 0.3 multiply_reduce_fusion.2
  12.5 0.2 fusion.7
  12.7 0.7 copy-done.14
  13.4 0.1 fusion.35
  13.6 0.5 fusion.60
  14.0 0.2 fusion.20
  14.2 0.7 copy-done.5
  14.9 0.1 copy.125
  15.1 0.3 fusion.6
  15.4 0.2 fusion.8
  15.6 0.1 reshape_reshape.3
  15.7 0.7 copy-done.9
  16.3 0.1 copy.130
  16.4 0.1 eq.30
  16.5 0.2 convert_reduce_fusion.1
  16.7 0.1 reshape.180
  16.8 0.1 copy.131
  16.9 0.7 copy-done.12
  17.7 0.1 copy.143
  17.8 0.3 fusion.5
  18.0 0.1 multiply_reduce_fusion
  18.2 0.7 copy-done.8
  19.0 14.9 %all_to_all.30 = f32[8,4,512]{2,1,0:T(4,128)S(1)} all-to-all(f32[8,4,512]{2,1,0:T(4,128)S(1)} %bitcast.69), channel_id=1, replica_groups={{0,1,2,3,4,5,6,7},{8,9,10,11,12,13,14,15},{16,17,18,19,20,21,22,23},{24..., dimensions={0} | all-to-all | bytes 131072 | tf_op jit(solution)/shard_map/all_to_all | solution.py:162
  34.0 0.1 copy.142
  34.1 0.1 convert_reduce_fusion
  34.2 0.5 copy-done.10
  34.7 0.2 convolution_convert_fusion.1
  34.9 30.1 %all_to_all.31 = bf16[64,4,128]{2,1,0:T(4,128)(2,1)S(1)} all-to-all(bf16[64,4,128]{2,1,0:T(4,128)(2,1)S(1)} %bitcast.70), channel_id=1, replica_groups={{0,8,16,24,32,40,48,56,64,72,80,88,96,104,112,120,128,136,144,152,160,1..., dimensions={0} | all-to-all | bytes 131072 | tf_op jit(solution)/shard_map/all_to_all | solution.py:176
  65.0 7.9 %all_to_all.32 = bf16[4,256,128]{2,1,0:T(8,128)(2,1)S(1)} all-to-all(bf16[4,256,128]{2,1,0:T(8,128)(2,1)S(1)} %broadcast_in_dim.25), channel_id=1, replica_groups=mesh['ep'=128,'tp'=4] {'tp'}, dimensions={0} | all-to-all | bytes 524288 | tf_op jit(solution)/shard_map/all_to_all | solution.py:42
  72.9 5.1 %all-gather = bf16[8,256,128]{2,1,0:T(8,128)(2,1)S(1)} all-gather(bf16[4,256,128]{2,1,0:T(8,128)(2,1)S(1)} %all_to_all.32), channel_id=2, replica_groups={{0,4},{8,12},{16,20},{24,28},{32,36},{40,44},{48,52},{56,60},{64,68},{7..., dimensions={0}, use_global_device_ids=true | all-gather | bytes 786432 | tf_op jit(solution)/shard_map/all_gather | solution.py:181
  78.0 0.2 copy.136
  78.2 0.4 fusion.12
  78.6 2.7 %convolution_convert_fusion = bf16[256,1024]{1,0:T(8,128)(2,1)S(1)} fusion(bf16[256,1024]{0,1:T(8,128)(2,1)S(1)} %bitcast.64, bf16[1,448,1024]{2,1,0:T(8,128)(2,1)} %param.41, bf16[1,1024,448]{1,2,0:T(8,128)(2,1)} %param.40, f32[256,448]{0,1:T(8,128)S(1)} %fusion.12), kind=kOutput, calls=%fused_computation | convolution fusion | flops 470712320 | bytes 3342336 | tf_op jit(solution)/shard_map/dot_general | solution.py:186
  81.4 11.6 %all_to_all.33 = bf16[4,256,256]{2,1,0:T(8,128)(2,1)S(1)} all-to-all(bf16[4,256,256]{2,1,0:T(8,128)(2,1)S(1)} %bitcast.62), channel_id=1, replica_groups=mesh['ep'=128,'tp'=4] {'tp'}, dimensions={0} | all-to-all | bytes 1048576 | tf_op jit(solution)/shard_map/all_to_all | solution.py:187
  93.0 0.1 reduce_sum.101
  93.1 0.7 reshape.187
  93.7 4.6 %all-to-all-start.5 = ((bf16[64,4,256]{2,1,0:T(4,128)(2,1)}), bf16[64,4,256]{2,1,0:T(4,128)(2,1)S(1)}, u32[]{:S(2)}, u32[]{:S(2)}) async-start(bf16[64,4,256]{2,1,0:T(4,128)(2,1)} %reshape.187), calls=%async_computation.5 | async-start | bytes 262144 | tf_op jit(solution)/shard_map/all_to_all | solution.py:191
  98.3 0.1 copy.134
  98.4 15.5 %all-to-all-done.5 = bf16[64,4,256]{2,1,0:T(4,128)(2,1)S(1)} async-done(((bf16[64,4,256]{2,1,0:T(4,128)(2,1)}), bf16[64,4,256]{2,1,0:T(4,128)(2,1)S(1)}, u32[]{:S(2)}, u32[]{:S(2)}) %all-to-all-start.5) | async-done | bytes 131104 | tf_op jit(solution)/shard_map/all_to_all | solution.py:191
  114.0 0.2 fusion.3
  114.2 4.6 %all-gather.1 = f32[32,256]{1,0:T(8,128)S(1)} all-gather(f32[16,256]{1,0:T(8,128)S(1)} %constant_dynamic-slice_fusion), channel_id=3, replica_groups={{0,4},{8,12},{16,20},{24,28},{32,36},{40,44},{48,52},{56,60},{64,68},{7..., dimensions={0}, use_global_device_ids=true | all-gather | bytes 49152 | tf_op jit(solution)/shard_map/all_gather | solution.py:201
  118.8 0.6 fusion.27
  (59 shorter events, 0.8 us)
Async XLA Ops:
  0.0 13.6 %copy-start = (bf16[4,1024,128]{2,1,0:T(8,128)(2,1)S(1)}, bf16[4,1024,128]{2,1,0:T(8,128)(2,1)}, u32[]{:S(2)}) copy-start(bf16[4,1024,128]{2,1,0:T(8,128)(2,1)} %param.33) | copy-start | bytes 3145732
  2.1 5.2 %copy-start.13 = (s32[4]{0:T(128)S(1)}, s32[4]{0:T(128)}, u32[]{:S(2)}) copy-start(s32[4]{0:T(128)} %param.35) | copy-start | bytes 52
  2.1 6.0 %copy-start.18 = (bf16[1024,32]{0,1:T(8,128)(2,1)S(1)}, bf16[1024,32]{0,1:T(8,128)(2,1)}, u32[]{:S(2)}) copy-start(bf16[1024,32]{0,1:T(8,128)(2,1)} %param.29) | copy-start | bytes 196612
  2.2 6.8 %copy-start.2 = (bf16[1024,256]{1,0:T(8,128)(2,1)S(1)}, bf16[1024,256]{1,0:T(8,128)(2,1)}, u32[]{:S(2)}) copy-start(bf16[1024,256]{1,0:T(8,128)(2,1)} %param.23) | copy-start | bytes 1572868
  2.2 15.6 %all-to-all-start = ((bf16[4,128,1024]{2,1,0:T(8,128)(2,1)}), bf16[4,128,1024]{2,1,0:T(8,128)(2,1)S(1)}, u32[]{:S(2)}, u32[]{:S(2)}) async-start(bf16[4,128,1024]{2,1,0:T(8,128)(2,1)} %broadcast_in_dim.22), calls=%async_computation | async-start | bytes 2097152 | tf_op jit(solution)/shard_map/all_to_all | solution.py:42
  7.3 0.8 copy-start.6
  8.0 0.7 copy-start.7
  8.9 0.9 copy-start.17
  8.9 1.4 %copy-start.15 = (bf16[256,512]{1,0:T(8,128)(2,1)S(1)}, bf16[256,512]{1,0:T(8,128)(2,1)}, u32[]{:S(2)}) copy-start(bf16[256,512]{1,0:T(8,128)(2,1)} %param.25) | copy-start | bytes 786436
  9.3 0.7 copy-start.19
  10.2 0.9 copy-start.4
  10.3 1.3 %copy-start.3 = (bf16[4,32,1024]{2,1,0:T(8,128)(2,1)S(1)}, bf16[4,32,1024]{2,1,0:T(8,128)(2,1)}, u32[]{:S(2)}) copy-start(bf16[4,32,1024]{2,1,0:T(8,128)(2,1)} %param.34) | copy-start | bytes 786436
  11.3 1.0 copy-start.16
  12.7 0.7 copy-start.14
  14.0 0.9 copy-start.5
  15.6 0.7 copy-start.9
  16.9 0.7 copy-start.12
  18.2 0.7 copy-start.8
  34.1 0.6 copy-start.10
  72.9 5.3 %copy-start.1 = (bf16[1,1024,448]{1,2,0:T(8,128)(2,1)S(1)}, bf16[1,1024,448]{1,2,0:T(8,128)(2,1)}, u32[]{:S(2)}) copy-start(bf16[1,1024,448]{1,2,0:T(8,128)(2,1)} %param.39) | copy-start | bytes 2752516
  93.7 20.2 %all-to-all-start.5 = ((bf16[64,4,256]{2,1,0:T(4,128)(2,1)}), bf16[64,4,256]{2,1,0:T(4,128)(2,1)S(1)}, u32[]{:S(2)}, u32[]{:S(2)}) async-start(bf16[64,4,256]{2,1,0:T(4,128)(2,1)} %reshape.187), calls=%async_computation.5 | async-start | bytes 262144 | tf_op jit(solution)/shard_map/all_to_all | solution.py:191
  98.4 15.6 %copy-start.11 = (s32[32,2]{0,1:T(2,128)S(1)}, s32[32,2]{0,1:T(2,128)}, u32[]{:S(2)}) copy-start(s32[32,2]{0,1:T(2,128)} %copy-done.10) | copy-start | bytes 772

commit v2 on v1

v2 whole, which is shorter than its diff:
```python
import jax
import jax.numpy as jnp
from jax import lax
from jax.experimental import pallas as pl
from jax.experimental.pallas import tpu as pltpu
from jax.sharding import PartitionSpec as P

HEADS = 8
NOPE = 64
ROPE = 32
VDIM = 64
KVLORA = 128

eps = 1e-06
rope_base = 10000.0
VMEM = pl.BlockSpec(memory_space=pltpu.VMEM)
SMEM = pl.BlockSpec(memory_space=pltpu.SMEM)
NT = (((1,), (1,)), ((), ()))
TN = (((0,), (0,)), ((), ()))
f32 = jnp.float32
bf16 = jnp.bfloat16


def dot(a, b, dims=(((1,), (0,)), ((), ()))):
    return lax.dot_general(a, b, dims, preferred_element_type=f32)


def iota(shape, dim):
    return lax.broadcasted_iota(jnp.int32, shape, dim)


def rms(values, gain):
    return values * lax.rsqrt(jnp.mean(values * values, axis=-1, keepdims=True) + eps) * gain


def turn(values, cosine, sine):
    width = values.shape[-1]
    lanes = iota(values.shape, 1) % ROPE
    ahead = pltpu.roll(values, width - ROPE // 2, 1)
    behind = pltpu.roll(values, ROPE // 2, 1)
    turned = jnp.where(lanes < ROPE // 2, -ahead, behind)
    return values * cosine + turned * sine


def attend_kernel(
    lengths, hidden, attn_gain, q_gain, kv_gain, table, routes, wqd, wqn, wqr, wkv, wkr, wuk, wuv,
    latent, rope, payload, mixed,
):
    own = latent.shape[0]
    rows = hidden.shape[0]
    tp = rows // own
    quarter = hidden.shape[1] // tp
    t = lax.axis_index("tp")
    c = lax.axis_index("ep") % 2
    r0, r1 = routes[0:1, :], routes[1:2, :]
    row, col = iota((rows, rows), 0), iota((rows, rows), 1)
    earlier = col < row
    ids = []
    for line in (r0, r1):
        mine = jnp.sum(jnp.where(row == col, line, 0), axis=1, keepdims=True)
        hits = (jnp.where(r0 == mine, 1, 0) + jnp.where(r1 == mine, 1, 0)) * jnp.where(
            earlier, 1, 0
        )
        slot = jnp.sum(hits, axis=1, keepdims=True)
        ids.append(mine * 4 + c * 2 + slot)
    lane = iota((rows, 128), 1)
    meta = jnp.where(lane == 0, ids[0], jnp.where(lane == 1, ids[1], 0)).astype(f32).astype(bf16)
    pick = jnp.where(
        (iota((8, rows), 1) == t * own + iota((8, rows), 0)) & (iota((8, rows), 0) < own), 1.0, 0.0
    ).astype(bf16)
    own_hidden = dot(pick, hidden[...])
    own_meta = dot(pick, meta)
    normed = rms(own_hidden, attn_gain[...]).astype(bf16)
    q_small = rms(dot(normed, wqd[...]), q_gain[...]).astype(bf16)
    q_plain = dot(q_small, wqn[...])
    cosine, sine = table[0], table[1]
    q_turned = turn(dot(q_small, wqr[...]), cosine, sine)
    new_latent = rms(dot(normed, wkv[...]), kv_gain[...]).astype(bf16).astype(f32)
    plain_key = dot(normed, wkr[...], NT)
    swap = jnp.concatenate([-plain_key[:, ROPE // 2 :], plain_key[:, : ROPE // 2]], axis=1)
    new_rope = (
        (plain_key * cosine[:, :ROPE] + swap * sine[:, :ROPE]).astype(bf16).astype(f32)
    )

    def spread(values, size):
        width = values.shape[1]
        head = iota((HEADS, width), 1) // size
        mask = head == iota((HEADS, width), 0)
        return jnp.concatenate(
            [jnp.where(mask, values[s : s + 1, :], 0.0) for s in range(own)], axis=0
        ).astype(bf16)

    q_latent = dot(spread(q_plain, NOPE), wuk[...], NT).astype(bf16)
    fold = jnp.where(
        iota((HEADS * ROPE, ROPE), 0) % ROPE == iota((HEADS * ROPE, ROPE), 1), 1.0, 0.0
    ).astype(bf16)
    q_rope = dot(spread(q_turned, ROPE), fold).astype(bf16)
    scale = (NOPE + ROPE) ** (-0.5)
    for s in range(own):
        mine = slice(s * HEADS, (s + 1) * HEADS)
        scores = (
            dot(q_latent[mine], latent[s], NT) + dot(q_rope[mine], rope[s])
        ) * scale
        scores = jnp.where(iota(scores.shape, 1) < lengths[s], scores, -1e30)
        fresh = (
            jnp.sum(q_latent[mine].astype(f32) * new_latent[s : s + 1, :], axis=1, keepdims=True)
            + jnp.sum(q_rope[mine].astype(f32) * new_rope[s : s + 1, :], axis=1, keepdims=True)
        ) * scale
        highest = jnp.maximum(jnp.max(scores, axis=1, keepdims=True), fresh)
        past = jnp.exp(scores - highest)
        now = jnp.exp(fresh - highest)
        divisor = jnp.sum(past, axis=1, keepdims=True) + now
        mix = dot((past / divisor).astype(bf16), latent[s])
        mix = mix + (now / divisor).astype(bf16).astype(f32) * new_latent[s : s + 1, :]
        mixed[mine, :] = mix.astype(bf16).astype(f32)
    values = dot(mixed[...].astype(bf16), wuv[...])
    head = iota((HEADS, HEADS * VDIM), 1) // VDIM == iota((HEADS, HEADS * VDIM), 0)
    head_values = jnp.concatenate(
        [
            jnp.sum(
                jnp.where(head, values[s * HEADS : (s + 1) * HEADS], 0.0), axis=0, keepdims=True
            )
            for s in range(own)
        ],
        axis=0,
    ).astype(bf16)
    width = HEADS * VDIM
    own_hidden = own_hidden[:own].astype(bf16)
    own_meta = own_meta[:own].astype(bf16)
    for j in range(2 * tp):
        payload[j, :, :width] = head_values
        payload[j, :, width : width + quarter] = own_hidden[
            :, (j % tp) * quarter : (j % tp + 1) * quarter
        ]
        payload[j, :, width + quarter :] = own_meta


def project_kernel(inbox, w, sent, residual_out, ids_out):
    c = lax.axis_index("ep") % 2
    rows = inbox.shape[0]
    tp, depth, quarter = w.shape
    width = tp * depth
    total = jnp.zeros((rows, quarter), f32)
    for b in range(tp):
        total = total + dot(inbox[:, b * depth : (b + 1) * depth], w[b]).astype(bf16).astype(f32)
    residual = inbox[:, width : width + quarter].astype(f32) + total
    half = quarter // 2
    block = jnp.where(c == 0, residual[:, :half], residual[:, half:]).astype(bf16)
    meta = inbox[:, width + quarter :].astype(f32).astype(jnp.int32)
    lanes = iota((rows, sent.shape[0]), 1)
    chooser = jnp.where((meta[:, 0:1] == lanes) | (meta[:, 1:2] == lanes), 1.0, 0.0).astype(bf16)
    sent[...] = dot(chooser, block, TN).astype(bf16)
    group = rows // 2
    residual_out[...] = jnp.where(c == 0, residual[:group], residual[group:])
    ids_out[...] = meta


def expert_kernel(both, gain, wg, wu, wd, out, x):
    cores, tp, rows, block = both.shape
    quarter = cores * block
    for part in range(2):
        size = rows // 2
        here = slice(part * size, (part + 1) * size)
        values = jnp.concatenate(
            [both[n, t, here, :] for t in range(tp) for n in range(cores)], axis=1
        ).astype(f32)
        x[here, :] = rms(values, gain[...]).astype(bf16)
    gate = dot(x[...], wg[...], NT)
    up = dot(x[...], wu[...], NT)
    inner = (gate / (1.0 + jnp.exp(-gate)) * up).astype(bf16)
    for t in range(tp):
        out[t] = dot(inner, wd[:, t * quarter : (t + 1) * quarter]).astype(bf16)


def combine_kernel(returned, ids, send, keep):
    c = lax.axis_index("ep") % 2
    rows = ids.shape[0]
    group = rows // 2
    lanes = iota((rows, returned.shape[0]), 1)
    for k in range(2):
        chooser = jnp.where(ids[:, k : k + 1] == lanes, 1.0, 0.0).astype(bf16)
        chosen = dot(chooser, returned[...])
        first, second = chosen[:group], chosen[group:]
        send[k] = jnp.where(c == 0, second, first).astype(bf16)
        keep[k] = jnp.where(c == 0, first, second)


def finish_kernel(swapped, keep, residual, weights, out):
    c = lax.axis_index("ep") % 2
    rows = residual.shape[0]
    same = iota((rows, rows), 0) == iota((rows, rows), 1)
    blended = jnp.zeros(residual.shape, f32)
    for k in range(2):
        partner = jnp.where(c == 0, swapped[1, k].astype(f32), swapped[0, k].astype(f32))
        weight = jnp.sum(jnp.where(same, weights[k : k + 1, :], 0.0), axis=1, keepdims=True)
        blended = blended + weight * (keep[k] + partner)
    out[...] = (residual[...] + blended).astype(bf16)


def per_device(
    hidden_in, attn_gain, w_qdown, q_gain, w_qnope, w_qrope, w_kvdown, kv_gain, w_krope, w_ukey,
    w_uvalue, w_out, cache_latent, cache_rope, lengths, ffn_gain, routes, route_weights, w_gate,
    w_up, w_down,
):
    group_rows, width = hidden_in.shape
    own = lengths.shape[0]
    tp = lax.axis_size("tp")
    experts = lax.axis_size("ep") // 2
    quarter = width // tp
    block = quarter // 2
    columns = [[(2 * k + c) * tp + t for c in range(2) for t in range(tp)] for k in range(experts)]
    same_core = [[2 * k + c for k in range(experts)] for c in range(2)]
    pairs = [[2 * k, 2 * k + 1] for k in range(experts)]

    w_mine = lax.all_to_all(
        jnp.stack([w_out[:, n * quarter : (n + 1) * quarter] for n in range(tp)]),
        "tp", 0, 0, tiled=True,
    )
    inverse = jnp.power(rope_base, -jnp.arange(0, ROPE, 2).astype(f32) / ROPE)
    positions = jnp.pad(lengths, (0, 8 - own)).astype(f32)
    angles = positions[:, None] * jnp.tile(inverse, 2 * HEADS)[None, :]
    table = jnp.stack([jnp.cos(angles), jnp.sin(angles)])
    wide = HEADS * VDIM + quarter + 128
    big = [hidden_in, w_qdown, w_qnope, w_qrope, w_kvdown, w_krope.T, w_ukey, w_uvalue,
           cache_latent, cache_rope]
    attend = pl.pallas_call(
        attend_kernel,
        out_shape=jax.ShapeDtypeStruct((2 * tp, own, wide), bf16),
        in_specs=[SMEM] + [VMEM] * 15,
        out_specs=VMEM,
        scratch_shapes=[pltpu.VMEM((own * HEADS, KVLORA), f32)],
        cost_estimate=pl.CostEstimate(
            flops=20_000_000_000, bytes_accessed=3_000_000, transcendentals=40_000
        ),
        compiler_params=pltpu.CompilerParams(vmem_limit_bytes=12 << 20),
        name="attend",
    )
    payload = attend(
        lengths, hidden_in, attn_gain[None], q_gain[None], kv_gain[None], table, routes.T,
        *big[1:],
    )
    payload, w_mine = lax.optimization_barrier((payload, w_mine))
    inbox = lax.all_to_all(
        payload, ("ep", "tp"), 0, 0, axis_index_groups=columns, tiled=True
    ).reshape(2 * group_rows, wide)
    rows = experts * 4
    sent, residual, ids = pl.pallas_call(
        project_kernel,
        out_shape=[
            jax.ShapeDtypeStruct((rows, block), bf16),
            jax.ShapeDtypeStruct((group_rows, quarter), f32),
            jax.ShapeDtypeStruct((2 * group_rows, 128), jnp.int32),
        ],
        in_specs=[VMEM] * 2,
        out_specs=[VMEM] * 3,
        compiler_params=pltpu.CompilerParams(vmem_limit_bytes=8 << 20),
        name="project",
    )(inbox, w_mine)
    arrived = lax.all_to_all(
        sent.reshape(experts, 4, block), "ep", 0, 0, axis_index_groups=same_core, tiled=True
    ).reshape(rows, block)
    over_tp = lax.all_to_all(
        jnp.broadcast_to(arrived, (tp, rows, block)), "tp", 0, 0, tiled=True
    )
    both = lax.all_gather(over_tp, "ep", axis_index_groups=pairs)
    partial = pl.pallas_call(
        expert_kernel,
        out_shape=jax.ShapeDtypeStruct((tp, rows, quarter), bf16),
        in_specs=[VMEM] * 5,
        out_specs=VMEM,
        scratch_shapes=[pltpu.VMEM((rows, width), bf16)],
        compiler_params=pltpu.CompilerParams(vmem_limit_bytes=20 << 20),
        name="expert",
    )(both, ffn_gain[None], jnp.swapaxes(w_gate[0], 0, 1), jnp.swapaxes(w_up[0], 0, 1), w_down[0])
    pieces = lax.all_to_all(partial, "tp", 0, 0, tiled=True)
    half_out = jnp.sum(pieces.astype(f32), axis=0).astype(bf16)
    returned = lax.all_to_all(
        half_out.reshape(experts, 4, quarter), "ep", 0, 0, axis_index_groups=same_core, tiled=True
    ).reshape(rows, quarter)
    send, keep = pl.pallas_call(
        combine_kernel,
        out_shape=[
            jax.ShapeDtypeStruct((2, group_rows, quarter), bf16),
            jax.ShapeDtypeStruct((2, group_rows, quarter), f32),
        ],
        in_specs=[VMEM] * 2,
        out_specs=[VMEM] * 2,
        compiler_params=pltpu.CompilerParams(vmem_limit_bytes=8 << 20),
        name="combine",
    )(returned, ids)
    swapped = lax.all_gather(send, "ep", axis_index_groups=pairs)
    return pl.pallas_call(
        finish_kernel,
        out_shape=jax.ShapeDtypeStruct((group_rows, quarter), bf16),
        in_specs=[VMEM] * 4,
        out_specs=VMEM,
        compiler_params=pltpu.CompilerParams(vmem_limit_bytes=8 << 20),
        name="finish",
    )(swapped, keep, residual, route_weights.T)


def solution(mesh):
    placed = (
        P("ep", None),
        P(),
        P(),
        P(),
        P(),
        P(),
        P(),
        P(),
        P(),
        P(),
        P(),
        P("tp", None),
        P(("ep", "tp"), None, None),
        P(("ep", "tp"), None, None),
        P(("ep", "tp")),
        P(),
        P("ep", None),
        P("ep", None),
        P("ep", None, "tp"),
        P("ep", None, "tp"),
        P("ep", "tp", None),
    )
    return jax.shard_map(
        per_device, mesh=mesh, in_specs=placed, out_specs=P("ep", "tp"), check_vma=False
    )
```

time: 120 us -> 114 us (0.950)
  blocking collectives: 74.2 us -> 91.2 us
  waiting for transfers between devices: 15.5 us -> 0.01 us
  matrix products: 6.42 us -> 0 us
  Pallas kernels: 0 us -> 6.06 us
  starting transfers between devices: 9.72 us -> 5.13 us
  local copies, waits for them, and re-layouts: 11.2 us -> 9.62 us
    all_to_all x4 -> x5, blocking collectives: 64.5 us -> 81.7 us  [the longest x1 28 us: per_device(): lax.all_to_all(sent.reshape(experts, 4, block), 'ep', 0, 0, axis_index_gr...]
    all_to_all x2 -> x1, waiting for transfers between devices: 15.5 us -> 0.01 us  [per_device(): lax.all_to_all(jnp.stack([w_out[:, n * quarter:(n + 1) * quarter] for n i...]
    dot_general x17 -> x0, matrix products: 6.42 us -> none  [the longest x1 2.7 us: per_device(): jnp.dot(inner, w_down[0], preferred_element_type=jnp.float32)]
    pallas_call x0 -> x5, Pallas kernels: none -> 6.06 us  [the longest x1 3.68 us: per_device(): attend(lengths, hidden_in, attn_gain[None], q_gain[None], kv_gain[None],...]
    all_to_all x2 -> x1, starting transfers between devices: 9.72 us -> 5.13 us  [per_device(): lax.all_to_all(jnp.stack([w_out[:, n * quarter:(n + 1) * quarter] for n i...]
    broadcast_in_dim x4 -> x1, local copies, waits for them, and re-layouts: 2.19 us -> 0.03 us  [per_device(): jnp.broadcast_to(arrived, (tp, rows, block))]
    unnamed x45 -> x40, local copies, waits for them, and re-layouts: 7.25 us -> 8.37 us
  transfers between devices with their start and end apart: 2 -> 1, of which waited for: 1 -> 0; matrix products, arithmetic and copies ran while one was open for 4% -> 0% of each run, Pallas kernels for 0% -> 3%
where the time goes in v2:
time: 114 us; the launch traced here: 113 us
  blocking collectives  91.2 us (80%)
  local copies, waits for them, and re-layouts  9.62 us (8%)
  Pallas kernels  6.06 us (5%)
  starting transfers between devices  5.13 us (4%)
    all_to_all x1, blocking collectives, per_device(): lax.all_to_all(sent.reshape(experts, 4, block), 'ep', 0, 0, axis_index_gr...  28 us
    all_to_all x1, blocking collectives, per_device(): lax.all_to_all(half_out.reshape(experts, 4, quarter), 'ep', 0, 0, axis_in...  19.5 us
    all_to_all x1, blocking collectives, per_device(): lax.all_to_all(payload, ('ep', 'tp'), 0, 0, axis_index_groups=columns, ti...  14.8 us
    all_to_all x1, blocking collectives, per_device(): pieces = lax.all_to_all(partial, 'tp', 0, 0, tiled=True)  11.6 us
    unnamed x40, local copies, waits for them, and re-layouts  8.37 us
    all_to_all x1, blocking collectives, per_device(): lax.all_to_all(jnp.broadcast_to(arrived, (tp, rows, block)), 'tp', 0, 0,...  7.92 us
    all_to_all x1, starting transfers between devices, per_device(): lax.all_to_all(jnp.stack([w_out[:, n * quarter:(n + 1) * quarter] for n i...  5.13 us
    all_gather x1, blocking collectives, per_device(): both = lax.all_gather(over_tp, 'ep', axis_index_groups=pairs)  4.93 us
  transfers between devices with their start and end apart: 1, of which 0 were waited for; matrix products, arithmetic and copies ran while one was open for 0% of the time, Pallas kernels for 3%

profile of v2, /device:TPU:1, one launch (start us, length us, event | category | flops | bytes accessed | tf_op | source)
XLA Modules:
  0.0 113.1 jit_solution(14048875040394175650)
XLA Ops:
  0.0 0.0 copy-start.5
  0.0 1.0 slice_bitcast_fusion.3
  1.0 0.0 copy-start.6
  1.1 0.7 pad_maximum_fusion
  1.8 0.0 copy-start.18
  1.8 5.1 %all-to-all-start = ((bf16[4,128,256]{2,1,0:T(8,128)(2,1)}), bf16[4,128,256]{2,1,0:T(8,128)(2,1)S(1)}, u32[]{:S(2)}, u32[]{:S(2)}) async-start(bf16[4,128,256]{2,1,0:T(8,128)(2,1)} %pad_maximum_fusion), calls=%async_computation | async-start | bytes 524288 | tf_op jit(solution)/shard_map/all_to_all | solution.py:215
  6.9 0.0 copy-start.13
  6.9 0.0 copy-done.18
  7.0 0.1 mul.35
  7.1 0.1 multiply_cosine_fusion
  7.2 0.0 copy-start.17
  7.2 0.0 copy-start.15
  7.2 0.0 copy-start.16
  7.2 0.0 copy-start.19
  7.2 0.0 copy-done.5
  7.3 0.0 copy-done.6
  7.3 0.5 copy-done.13
  7.8 0.1 copy-done.17
  7.9 0.0 copy-done.15
  7.9 0.0 copy-done.16
  7.9 0.0 copy-done.19
  7.9 0.0 copy-start.7
  7.9 0.9 copy-done.7
  8.9 0.0 copy-start.8
  8.9 0.9 copy-done.8
  9.8 0.0 copy-start.9
  9.8 0.9 copy-done.9
  10.8 0.0 copy-start.10
  10.8 0.9 copy-done.10
  11.7 0.0 copy-start.11
  11.7 0.9 copy-done.11
  12.6 0.0 copy-start.12
  12.6 0.9 copy-done.12
  13.5 0.0 copy-start.14
  13.5 0.8 copy-done.14
  14.2 0.0 copy-start.2
  14.2 3.7 %attend.1 = bf16[8,4,896]{2,1,0:T(4,128)(2,1)S(1)} custom-call(s32[4]{0:T(128)S(1)} %copy-done.18, bf16[16,1024]{1,0:T(8,128)(2,1)S(1)} %copy-done.14, f32[1,1024]{1,0:T(1,128)S(1)} %bitcast.35, f32[1,256]{1,0:T(1,128)S(1)} %bitcast.36, f32[1,128]{1,0:T(1,128)S(1)} %bitcast.38, f32[2,8,256]{2,1,0:T(8,128)S(1)} %pad_maximum_fusion.1.table, ...), custom_call_target="tpu_custom_call" | custom-call | flops 20000000000 | bytes 3000000 | tf_op jit(solution)/shard_map/attend/pallas_call | solution.py:238
  17.9 0.0 all-to-all-done.w
  17.9 14.8 %all_to_all.30 = bf16[8,4,896]{2,1,0:T(4,128)(2,1)S(1)} all-to-all(bf16[8,4,896]{2,1,0:T(4,128)(2,1)S(1)} %attend.1), channel_id=1, replica_groups={{0,1,2,3,4,5,6,7},{8,9,10,11,12,13,14,15},{16,17,18,19,20,21,22,23},{24..., dimensions={0} | all-to-all | bytes 114688 | tf_op jit(solution)/shard_map/all_to_all | solution.py:243
  32.7 0.0 copy-start.1
  32.7 0.3 project.1
  33.1 0.0 copy-start
  33.1 28.0 %all_to_all.31 = bf16[64,4,128]{2,1,0:T(4,128)(2,1)S(1)} all-to-all(bf16[64,4,128]{2,1,0:T(4,128)(2,1)S(1)} %bitcast.31), channel_id=1, replica_groups={{0,8,16,24,32,40,48,56,64,72,80,88,96,104,112,120,128,136,144,152,160,1..., dimensions={0} | all-to-all | bytes 131072 | tf_op jit(solution)/shard_map/all_to_all | solution.py:259
  61.1 7.9 %all_to_all.32 = bf16[4,256,128]{2,1,0:T(8,128)(2,1)S(1)} all-to-all(bf16[4,256,128]{2,1,0:T(8,128)(2,1)S(1)} %broadcast_in_dim.19), channel_id=1, replica_groups=mesh['ep'=128,'tp'=4] {'tp'}, dimensions={0} | all-to-all | bytes 524288 | tf_op jit(solution)/shard_map/all_to_all | solution.py:262
  69.0 4.9 %all-gather = bf16[8,256,128]{2,1,0:T(8,128)(2,1)S(1)} all-gather(bf16[4,256,128]{2,1,0:T(8,128)(2,1)S(1)} %all_to_all.32), channel_id=2, replica_groups={{0,4},{8,12},{16,20},{24,28},{32,36},{40,44},{48,52},{56,60},{64,68},{7..., dimensions={0}, use_global_device_ids=true | all-gather | bytes 786432 | tf_op jit(solution)/shard_map/all_gather | solution.py:265
  73.9 0.0 copy-start.3
  73.9 0.0 copy-done.2
  74.0 0.0 copy-done.1
  74.0 0.0 copy-done
  74.0 0.7 copy-done.3
  74.6 1.2 %expert.1 = bf16[4,256,256]{2,1,0:T(8,128)(2,1)S(1)} custom-call(bf16[2,4,256,128]{3,2,1,0:T(8,128)(2,1)S(1)} %bitcast.26, f32[1,1024]{1,0:T(1,128)S(1)} %bitcast.32, bf16[448,1024]{1,0:T(8,128)(2,1)S(1)} %bitcast.27, bf16[448,1024]{1,0:T(8,128)(2,1)S(1)} %bitcast.28, bf16[448,1024]{1,0:T(8,128)(2,1)S(1)} %bitcast.29), custom_call_target="tpu_custom_call" | custom-call | tf_op jit(solution)/shard_map/expert/pallas_call | solution.py:266
  75.8 11.6 %all_to_all.33 = bf16[4,256,256]{2,1,0:T(8,128)(2,1)S(1)} all-to-all(bf16[4,256,256]{2,1,0:T(8,128)(2,1)S(1)} %expert.1), channel_id=1, replica_groups=mesh['ep'=128,'tp'=4] {'tp'}, dimensions={0} | all-to-all | bytes 1048576 | tf_op jit(solution)/shard_map/all_to_all | solution.py:275
  87.4 0.1 reduce_sum.12
  87.5 19.5 %all_to_all.34 = bf16[64,4,256]{2,1,0:T(4,128)(2,1)S(1)} all-to-all(bf16[64,4,256]{2,1,0:T(4,128)(2,1)S(1)} %reshape.118), channel_id=1, replica_groups={{0,8,16,24,32,40,48,56,64,72,80,88,96,104,112,120,128,136,144,152,160,1..., dimensions={0} | all-to-all | bytes 262144 | tf_op jit(solution)/shard_map/all_to_all | solution.py:277
  107.0 0.2 combine.1
  107.2 4.6 %all-gather.1 = bf16[4,16,256]{2,1,0:T(8,128)(2,1)S(1)} all-gather(bf16[2,16,256]{2,1,0:T(8,128)(2,1)S(1)} %get-tuple-element.16), channel_id=3, replica_groups={{0,4},{8,12},{16,20},{24,28},{32,36},{40,44},{48,52},{56,60},{64,68},{7..., dimensions={0}, use_global_device_ids=true | all-gather | bytes 49152 | tf_op jit(solution)/shard_map/all_gather | solution.py:291
  111.8 0.0 copy-start.4
  111.8 0.7 copy-done.4
  112.5 0.7 finish.1
  (8 shorter events, 0.1 us)
Async XLA Ops:
  0.0 7.2 %copy-start.5 = (bf16[4,1024,128]{2,1,0:T(8,128)(2,1)S(1)}, bf16[4,1024,128]{2,1,0:T(8,128)(2,1)}, u32[]{:S(2)}) copy-start(bf16[4,1024,128]{2,1,0:T(8,128)(2,1)} %latent.1) | copy-start | bytes 3145732
  1.0 6.2 %copy-start.6 = (bf16[1024,256]{1,0:T(8,128)(2,1)S(1)}, bf16[1024,256]{1,0:T(8,128)(2,1)}, u32[]{:S(2)}) copy-start(bf16[1024,256]{1,0:T(8,128)(2,1)} %wqd.1) | copy-start | bytes 1572868
  1.8 5.1 %copy-start.18 = (s32[4]{0:T(128)S(1)}, s32[4]{0:T(128)}, u32[]{:S(2)}) copy-start(s32[4]{0:T(128)} %lengths.1) | copy-start | bytes 52
  1.8 16.1 %all-to-all-start = ((bf16[4,128,256]{2,1,0:T(8,128)(2,1)}), bf16[4,128,256]{2,1,0:T(8,128)(2,1)S(1)}, u32[]{:S(2)}, u32[]{:S(2)}) async-start(bf16[4,128,256]{2,1,0:T(8,128)(2,1)} %pad_maximum_fusion), calls=%async_computation | async-start | bytes 524288 | tf_op jit(solution)/shard_map/all_to_all | solution.py:215
  6.9 0.8 copy-start.13
  7.2 0.7 copy-start.17
  7.2 0.7 copy-start.15
  7.2 0.7 copy-start.16
  7.2 0.7 copy-start.19
  7.9 1.0 copy-start.7
  8.9 0.9 copy-start.8
  9.8 0.9 copy-start.9
  10.8 0.9 copy-start.10
  11.7 0.9 copy-start.11
  12.6 0.9 copy-start.12
  13.5 0.8 copy-start.14
  14.2 59.7 %copy-start.2 = (bf16[1,448,1024]{2,1,0:T(8,128)(2,1)S(1)}, bf16[1,448,1024]{2,1,0:T(8,128)(2,1)}, u32[]{:S(2)}) copy-start(bf16[1,448,1024]{2,1,0:T(8,128)(2,1)} %param.41) | copy-start | bytes 2752516
  32.7 41.2 %copy-start.1 = (bf16[1,1024,448]{1,2,0:T(8,128)(2,1)S(1)}, bf16[1,1024,448]{1,2,0:T(8,128)(2,1)}, u32[]{:S(2)}) copy-start(bf16[1,1024,448]{1,2,0:T(8,128)(2,1)} %param.40) | copy-start | bytes 2752516
  33.1 40.9 %copy-start = (bf16[1,1024,448]{1,2,0:T(8,128)(2,1)S(1)}, bf16[1,1024,448]{1,2,0:T(8,128)(2,1)}, u32[]{:S(2)}) copy-start(bf16[1,1024,448]{1,2,0:T(8,128)(2,1)} %param.39) | copy-start | bytes 2752516
  73.9 0.7 copy-start.3
  111.8 0.7 copy-start.4

commit v3 on v2

v3 whole, which is shorter than its diff:
```python
import jax
import jax.numpy as jnp
from jax import lax
from jax.experimental import pallas as pl
from jax.experimental.pallas import tpu as pltpu
from jax.sharding import PartitionSpec as P

HEADS = 8
NOPE = 64
ROPE = 32
VDIM = 64
KVLORA = 128

eps = 1e-06
rope_base = 10000.0
VMEM = pl.BlockSpec(memory_space=pltpu.VMEM)
HBM = pl.BlockSpec(memory_space=pltpu.HBM)
SMEM = pl.BlockSpec(memory_space=pltpu.SMEM)
NT = (((1,), (1,)), ((), ()))
TN = (((0,), (0,)), ((), ()))
f32 = jnp.float32
bf16 = jnp.bfloat16


def dot(a, b, dims=(((1,), (0,)), ((), ()))):
    return lax.dot_general(a, b, dims, preferred_element_type=f32)


def iota(shape, dim):
    return lax.broadcasted_iota(jnp.int32, shape, dim)


def rms(values, gain):
    return values * lax.rsqrt(jnp.mean(values * values, axis=-1, keepdims=True) + eps) * gain


def turn(values, cosine, sine):
    width = values.shape[-1]
    lanes = iota(values.shape, 1) % ROPE
    ahead = pltpu.roll(values, width - ROPE // 2, 1)
    behind = pltpu.roll(values, ROPE // 2, 1)
    turned = jnp.where(lanes < ROPE // 2, -ahead, behind)
    return values * cosine + turned * sine


def attend_kernel(
    lengths, attn_gain, q_gain, kv_gain, ffn_gain, table, routes, weights, h_hidden, h_wqd, h_wqn,
    h_wqr, h_wkv, h_wkr, h_wuk, h_rope, h_latent, h_wuv, h_wout, payload, gain_out, hidden, wqd,
    wqn, wqr, wkv, wkr, wuk, rope, latent, wuv, mixed, sems,
):
    own = latent.shape[0]
    rows, width = hidden.shape
    tp = rows // own
    block = width // (2 * tp)
    part = h_wout.shape[0] // 2
    t = lax.axis_index("tp")
    c = lax.axis_index("ep") % 2
    pairs = [
        (h_hidden, hidden), (h_wqd, wqd), (h_wqn, wqn), (h_wqr, wqr), (h_wkv, wkv), (h_wkr, wkr),
        (h_wuk, wuk), (h_rope, rope), (h_latent, latent), (h_wuv, wuv),
    ]
    copies = [pltpu.make_async_copy(src, dst, sems.at[n]) for n, (src, dst) in enumerate(pairs)]
    for j in range(2 * tp):
        column = (2 * (j % tp) + j // tp) * block
        copies.append(
            pltpu.make_async_copy(
                h_wout.at[pl.ds(pl.multiple_of(c * part, part), part), column : column + block],
                payload.at[j, 0:part, :],
                sems.at[len(copies)],
            )
        )
    for copy in copies:
        copy.start()
    gain_out[...] = ffn_gain[...]
    r0, r1 = routes[0:1, :], routes[1:2, :]
    row, col = iota((rows, rows), 0), iota((rows, rows), 1)
    earlier = col < row
    ids = []
    for line in (r0, r1):
        mine = jnp.sum(jnp.where(row == col, line, 0), axis=1, keepdims=True)
        hits = (jnp.where(r0 == mine, 1, 0) + jnp.where(r1 == mine, 1, 0)) * jnp.where(
            earlier, 1, 0
        )
        slot = jnp.sum(hits, axis=1, keepdims=True)
        ids.append(mine * 4 + c * 2 + slot)
    lane = iota((rows, 128), 1)
    meta = jnp.where(lane == 0, ids[0], jnp.where(lane == 1, ids[1], 0)).astype(f32)
    for k in range(2):
        rest = jnp.sum(jnp.where(row == col, weights[k : k + 1, :], 0.0), axis=1, keepdims=True)
        for n in range(3):
            piece = rest.astype(bf16).astype(f32)
            meta = jnp.where(lane == 2 + 3 * k + n, piece, meta)
            rest = rest - piece
    meta = meta.astype(bf16)
    pick = jnp.where(
        (iota((8, rows), 1) == t * own + iota((8, rows), 0)) & (iota((8, rows), 0) < own), 1.0, 0.0
    ).astype(bf16)
    copies[0].wait()
    own_hidden = dot(pick, hidden[...])
    own_meta = dot(pick, meta)
    normed = rms(own_hidden, attn_gain[...]).astype(bf16)
    copies[1].wait()
    q_small = rms(dot(normed, wqd[...]), q_gain[...]).astype(bf16)
    copies[2].wait()
    q_plain = dot(q_small, wqn[...])
    cosine, sine = table[0], table[1]
    copies[3].wait()
    q_turned = turn(dot(q_small, wqr[...]), cosine, sine)
    copies[4].wait()
    new_latent = rms(dot(normed, wkv[...]), kv_gain[...]).astype(bf16).astype(f32)
    copies[5].wait()
    plain_key = dot(normed, wkr[...], NT)
    swap = jnp.concatenate([-plain_key[:, ROPE // 2 :], plain_key[:, : ROPE // 2]], axis=1)
    new_rope = (
        (plain_key * cosine[:, :ROPE] + swap * sine[:, :ROPE]).astype(bf16).astype(f32)
    )

    def spread(values, size):
        width = values.shape[1]
        head = iota((HEADS, width), 1) // size
        mask = head == iota((HEADS, width), 0)
        return jnp.concatenate(
            [jnp.where(mask, values[s : s + 1, :], 0.0) for s in range(own)], axis=0
        ).astype(bf16)

    copies[6].wait()
    q_latent = dot(spread(q_plain, NOPE), wuk[...], NT).astype(bf16)
    fold = jnp.where(
        iota((HEADS * ROPE, ROPE), 0) % ROPE == iota((HEADS * ROPE, ROPE), 1), 1.0, 0.0
    ).astype(bf16)
    q_rope = dot(spread(q_turned, ROPE), fold).astype(bf16)
    scale = (NOPE + ROPE) ** (-0.5)
    copies[7].wait()
    copies[8].wait()
    for s in range(own):
        mine = slice(s * HEADS, (s + 1) * HEADS)
        scores = (
            dot(q_latent[mine], latent[s], NT) + dot(q_rope[mine], rope[s])
        ) * scale
        scores = jnp.where(iota(scores.shape, 1) < lengths[s], scores, -1e30)
        fresh = (
            jnp.sum(q_latent[mine].astype(f32) * new_latent[s : s + 1, :], axis=1, keepdims=True)
            + jnp.sum(q_rope[mine].astype(f32) * new_rope[s : s + 1, :], axis=1, keepdims=True)
        ) * scale
        highest = jnp.maximum(jnp.max(scores, axis=1, keepdims=True), fresh)
        past = jnp.exp(scores - highest)
        now = jnp.exp(fresh - highest)
        divisor = jnp.sum(past, axis=1, keepdims=True) + now
        mix = dot((past / divisor).astype(bf16), latent[s])
        mix = mix + (now / divisor).astype(bf16).astype(f32) * new_latent[s : s + 1, :]
        mixed[mine, :] = mix.astype(bf16).astype(f32)
    copies[9].wait()
    values = dot(mixed[...].astype(bf16), wuv[...])
    head = iota((HEADS, HEADS * VDIM), 1) // VDIM == iota((HEADS, HEADS * VDIM), 0)
    head_values = jnp.concatenate(
        [
            jnp.sum(
                jnp.where(head, values[s * HEADS : (s + 1) * HEADS], 0.0), axis=0, keepdims=True
            )
            for s in range(own)
        ],
        axis=0,
    )
    parts = [
        head_values[:, b * (HEADS * VDIM // tp) : (b + 1) * (HEADS * VDIM // tp)]
        for b in range(tp)
    ]
    for j in range(2 * tp):
        column = (2 * (j % tp) + j // tp) * block
        payload[j, part:, :] = jnp.concatenate(
            [*parts, own_hidden[:own, column : column + block], own_meta[:own]], axis=0
        ).astype(bf16)
    for copy in copies[len(pairs) :]:
        copy.wait()


def project_kernel(inbox, sent, residual_out, meta_out):
    devices, lines, block = inbox.shape
    tp = devices // 2
    own = 4
    part = lines - own * (tp + 2)
    tails = [inbox[j, part:, :].astype(f32) for j in range(devices)]

    def section(n):
        return jnp.concatenate([tail[n * own : (n + 1) * own] for tail in tails], axis=0)

    total = jnp.zeros((devices * own, block), f32)
    for b in range(tp):
        w = jnp.concatenate([inbox[b, :part, :], inbox[tp + b, :part, :]], axis=0)
        total = total + dot(section(b).astype(bf16), w).astype(bf16).astype(f32)
    residual = section(tp) + total
    meta = section(tp + 1)
    targets = meta.astype(jnp.int32)
    lanes = iota((devices * own, sent.shape[0]), 1)
    chooser = jnp.where(
        (targets[:, 0:1] == lanes) | (targets[:, 1:2] == lanes), 1.0, 0.0
    ).astype(bf16)
    sent[...] = dot(chooser, residual.astype(bf16), TN).astype(bf16)
    residual_out[...] = residual
    meta_out[...] = meta


def expert_kernel(both, gain, wg, wu, wd, stay, away, x):
    c = lax.axis_index("ep") % 2
    cores, tp, rows, block = both.shape
    quarter = cores * block
    for part in range(2):
        size = rows // 2
        here = slice(part * size, (part + 1) * size)
        values = jnp.concatenate(
            [both[n, t, here, :] for t in range(tp) for n in range(cores)], axis=1
        ).astype(f32)
        x[here, :] = rms(values, gain[...]).astype(bf16)
    gate = dot(x[...], wg[...], NT)
    up = dot(x[...], wu[...], NT)
    inner = (gate / (1.0 + jnp.exp(-gate)) * up).astype(bf16)
    for t in range(tp):
        term = dot(inner, wd[:, t * quarter : (t + 1) * quarter])
        first, second = term[:, :block], term[:, block:]
        stay[t] = jnp.where(c == 0, first, second).astype(bf16)
        away[t] = jnp.where(c == 0, second, first).astype(bf16)


def pair_kernel(stay, swapped, out):
    partner = 1 - lax.axis_index("ep") % 2
    for t in range(stay.shape[0]):
        out[t] = (stay[t].astype(f32) + swapped[partner, t].astype(f32)).astype(bf16)


def combine_kernel(returned, meta, residual, send, keep):
    c = lax.axis_index("ep") % 2
    rows = meta.shape[0]
    group = rows // 2
    targets = meta[...].astype(jnp.int32)
    lanes = iota((rows, returned.shape[0]), 1)
    blended = jnp.zeros(residual.shape, f32)
    for k in range(2):
        chooser = jnp.where(targets[:, k : k + 1] == lanes, 1.0, 0.0).astype(bf16)
        first = 2 + 3 * k
        weight = (meta[:, first : first + 1] + meta[:, first + 1 : first + 2]) + meta[
            :, first + 2 : first + 3
        ]
        blended = blended + weight * dot(chooser, returned[...])
    total = residual[...] + blended
    send[...] = jnp.where(c == 0, total[group:], total[:group]).astype(bf16)
    keep[...] = jnp.where(c == 0, total[:group], total[group:])


def finish_kernel(swapped, keep, out):
    c = lax.axis_index("ep") % 2
    block = keep.shape[1]
    mine = keep[...]
    out[:, :block] = jnp.where(c == 0, mine, swapped[0].astype(f32)).astype(bf16)
    out[:, block:] = jnp.where(c == 0, swapped[1].astype(f32), mine).astype(bf16)


def per_device(
    hidden_in, attn_gain, w_qdown, q_gain, w_qnope, w_qrope, w_kvdown, kv_gain, w_krope, w_ukey,
    w_uvalue, w_out, cache_latent, cache_rope, lengths, ffn_gain, routes, route_weights, w_gate,
    w_up, w_down,
):
    group_rows, width = hidden_in.shape
    own = lengths.shape[0]
    tp = lax.axis_size("tp")
    experts = lax.axis_size("ep") // 2
    quarter = width // tp
    block = quarter // 2
    columns = [[(2 * k + c) * tp + t for c in range(2) for t in range(tp)] for k in range(experts)]
    same_core = [[2 * k + c for k in range(experts)] for c in range(2)]
    pairs = [[2 * k, 2 * k + 1] for k in range(experts)]

    inverse = jnp.power(rope_base, -jnp.arange(0, ROPE, 2).astype(f32) / ROPE)
    positions = jnp.pad(lengths, (0, 8 - own)).astype(f32)
    angles = positions[:, None] * jnp.tile(inverse, 2 * HEADS)[None, :]
    table = jnp.stack([jnp.cos(angles), jnp.sin(angles)])
    big = [hidden_in, w_qdown, w_qnope, w_qrope, w_kvdown, w_krope.T, w_ukey, cache_rope,
           cache_latent, w_uvalue]
    lines = w_out.shape[0] // 2 + own * (tp + 2)
    rows = experts * 4
    small_vmem = pltpu.CompilerParams(vmem_limit_bytes=8 << 20)
    payload, gain = pl.pallas_call(
        attend_kernel,
        out_shape=[
            jax.ShapeDtypeStruct((2 * tp, lines, block), bf16),
            jax.ShapeDtypeStruct((1, width), f32),
        ],
        in_specs=[SMEM] + [VMEM] * 7 + [HBM] * 11,
        out_specs=[VMEM] * 2,
        scratch_shapes=[pltpu.VMEM(a.shape, a.dtype) for a in big]
        + [pltpu.VMEM((own * HEADS, KVLORA), f32)]
        + [pltpu.SemaphoreType.DMA((len(big) + 2 * tp,))],
        compiler_params=pltpu.CompilerParams(vmem_limit_bytes=12 << 20),
        name="attend",
    )(
        lengths, attn_gain[None], q_gain[None], kv_gain[None], ffn_gain[None], table, routes.T,
        route_weights.T, *[pltpu.with_memory_space_constraint(a, pltpu.HBM) for a in [*big, w_out]],
    )
    inbox = lax.all_to_all(
        payload, ("ep", "tp"), 0, 0, axis_index_groups=columns, tiled=True
    )
    sent, residual, meta = pl.pallas_call(
        project_kernel,
        out_shape=[
            jax.ShapeDtypeStruct((rows, block), bf16),
            jax.ShapeDtypeStruct((2 * group_rows, block), f32),
            jax.ShapeDtypeStruct((2 * group_rows, 128), f32),
        ],
        in_specs=[VMEM],
        out_specs=[VMEM] * 3,
        compiler_params=small_vmem,
        name="project",
    )(inbox)
    arrived = lax.all_to_all(
        sent.reshape(experts, 4, block), "ep", 0, 0, axis_index_groups=same_core, tiled=True
    ).reshape(rows, block)
    over_tp = lax.all_to_all(
        jnp.broadcast_to(arrived, (tp, rows, block)), "tp", 0, 0, tiled=True
    )
    both = lax.all_gather(over_tp, "ep", axis_index_groups=pairs)
    stay, away = pl.pallas_call(
        expert_kernel,
        out_shape=[jax.ShapeDtypeStruct((tp, rows, block), bf16)] * 2,
        in_specs=[VMEM] * 5,
        out_specs=[VMEM] * 2,
        scratch_shapes=[pltpu.VMEM((rows, width), bf16)],
        compiler_params=pltpu.CompilerParams(vmem_limit_bytes=20 << 20),
        name="expert",
    )(both, gain, jnp.swapaxes(w_gate[0], 0, 1), jnp.swapaxes(w_up[0], 0, 1), w_down[0])
    swapped = lax.all_gather(away, "ep", axis_index_groups=pairs)
    partial = pl.pallas_call(
        pair_kernel,
        out_shape=jax.ShapeDtypeStruct((tp, rows, block), bf16),
        in_specs=[VMEM] * 2,
        out_specs=VMEM,
        compiler_params=small_vmem,
        name="pair",
    )(stay, swapped)
    pieces = lax.all_to_all(partial, "tp", 0, 0, tiled=True)
    unit_out = jnp.sum(pieces.astype(f32), axis=0).astype(bf16)
    returned = lax.all_to_all(
        unit_out.reshape(experts, 4, block), "ep", 0, 0, axis_index_groups=same_core, tiled=True
    ).reshape(rows, block)
    send, keep = pl.pallas_call(
        combine_kernel,
        out_shape=[
            jax.ShapeDtypeStruct((group_rows, block), bf16),
            jax.ShapeDtypeStruct((group_rows, block), f32),
        ],
        in_specs=[VMEM] * 3,
        out_specs=[VMEM] * 2,
        compiler_params=small_vmem,
        name="combine",
    )(returned, meta, residual)
    return pl.pallas_call(
        finish_kernel,
        out_shape=jax.ShapeDtypeStruct((group_rows, quarter), bf16),
        in_specs=[VMEM] * 2,
        out_specs=VMEM,
        compiler_params=small_vmem,
        name="finish",
    )(lax.all_gather(send, "ep", axis_index_groups=pairs), keep)


def solution(mesh):
    placed = (
        P("ep", None),
        P(),
        P(),
        P(),
        P(),
        P(),
        P(),
        P(),
        P(),
        P(),
        P(),
        P("tp", None),
        P(("ep", "tp"), None, None),
        P(("ep", "tp"), None, None),
        P(("ep", "tp")),
        P(),
        P("ep", None),
        P("ep", None),
        P("ep", None, "tp"),
        P("ep", None, "tp"),
        P("ep", "tp", None),
    )
    return jax.shard_map(
        per_device, mesh=mesh, in_specs=placed, out_specs=P("ep", "tp"), check_vma=False
    )
```

time: 114 us -> 99.4 us (0.87)
  local copies, waits for them, and re-layouts: 9.62 us -> 1.49 us
  starting transfers between devices: 5.13 us -> 0 us
  Pallas kernels: 6.06 us -> 7.82 us
  blocking collectives: 91.2 us -> 89.5 us
    unnamed x40 -> x20, local copies, waits for them, and re-layouts: 8.37 us -> 1.37 us
    all_to_all x1 -> x0, starting transfers between devices: 5.13 us -> none  [per_device(): lax.all_to_all(jnp.stack([w_out[:, n * quarter:(n + 1) * quarter] for n i...]
    all_to_all x1, blocking collectives: 11.6 us -> 8.78 us  [per_device(): pieces = lax.all_to_all(partial, 'tp', 0, 0, tiled=True)]
    pallas_call x3 -> x4, Pallas kernels: 5.04 us -> 6.9 us  [the longest x1 5.47 us: per_device(): pl.pallas_call(attend_kernel, out_shape=[jax.ShapeDtypeStruct((2 * tp, li...]
    all_to_all x1, blocking collectives: 19.5 us -> 17.9 us  [per_device(): lax.all_to_all(unit_out.reshape(experts, 4, block), 'ep', 0, 0, axis_inde...]
    all_gather x1 -> x2, blocking collectives: 4.57 us -> 5.98 us  [the longest x1 3.8 us: per_device(): lax.all_gather(send, 'ep', axis_index_groups=pairs)]
  transfers between devices with their start and end apart: 1 -> 0, of which waited for: 0 -> 0; matrix products, arithmetic and copies ran while one was open for 0% -> 0% of each run, Pallas kernels for 3% -> 0%
where the time goes in v3:
time: 99.4 us; the launch traced here: 99.1 us
  blocking collectives  89.5 us (90%)
  Pallas kernels  7.82 us (8%)
  local copies, waits for them, and re-layouts  1.49 us (1%)
    all_to_all x1, blocking collectives, per_device(): lax.all_to_all(sent.reshape(experts, 4, block), 'ep', 0, 0, axis_index_gr...  28.8 us
    all_to_all x1, blocking collectives, per_device(): lax.all_to_all(unit_out.reshape(experts, 4, block), 'ep', 0, 0, axis_inde...  17.9 us
    all_to_all x1, blocking collectives, per_device(): lax.all_to_all(payload, ('ep', 'tp'), 0, 0, axis_index_groups=columns, ti...  14.9 us
    all_to_all x1, blocking collectives, per_device(): pieces = lax.all_to_all(partial, 'tp', 0, 0, tiled=True)  8.78 us
    all_to_all x1, blocking collectives, per_device(): lax.all_to_all(jnp.broadcast_to(arrived, (tp, rows, block)), 'tp', 0, 0,...  7.92 us
    pallas_call x1, Pallas kernels, per_device(): pl.pallas_call(attend_kernel, out_shape=[jax.ShapeDtypeStruct((2 * tp, li...  5.47 us
    all_gather x1, blocking collectives, per_device(): both = lax.all_gather(over_tp, 'ep', axis_index_groups=pairs)  5.26 us
    all_gather x1, blocking collectives, per_device(): lax.all_gather(send, 'ep', axis_index_groups=pairs)  3.8 us

profile of v3, /device:TPU:1, one launch (start us, length us, event | category | flops | bytes accessed | tf_op | source)
XLA Modules:
  0.0 99.1 jit_solution(10112397822080869576)
XLA Ops:
  0.0 0.0 copy-start.8
  0.0 0.6 copy-done.8
  0.7 0.1 mul.35
  0.7 0.1 multiply_cosine_fusion
  0.9 0.0 copy-start.9
  0.9 0.0 copy-start.6
  0.9 0.0 copy-start.7
  0.9 0.0 copy-start.4
  0.9 0.0 copy-start.3
  0.9 0.0 copy-start.5
  1.0 0.6 copy-done.9
  1.5 0.0 copy-done.6
  1.6 0.0 copy-done.7
  1.6 0.0 copy-done.4
  1.6 0.0 copy-done.3
  1.6 0.0 copy-done.5
  1.6 0.0 copy-start.2
  1.6 5.5 %attend.1 = (bf16[8,88,128]{2,1,0:T(8,128)(2,1)S(1)}, f32[1,1024]{1,0:T(1,128)S(1)}) custom-call(s32[4]{0:T(128)S(1)} %copy-done.8, f32[1,1024]{1,0:T(1,128)S(1)} %bitcast.29, f32[1,256]{1,0:T(1,128)S(1)} %bitcast.31, f32[1,128]{1,0:T(1,128)S(1)} %bitcast.34, f32[1,1024]{1,0:T(1,128)S(1)} %bitcast.30, f32[2,8,256]{2,1,0:T(8,128)S(1)} %pad_maximum_fusion.table, ...), custom_call_target="tpu_custom_call" | custom-call | tf_op jit(solution)/shard_map/attend/pallas_call | solution.py:281
  7.1 14.9 %all_to_all.25.inbox = bf16[8,88,128]{2,1,0:T(8,128)(2,1)S(1)} all-to-all(bf16[8,88,128]{2,1,0:T(8,128)(2,1)S(1)} %get-tuple-element.14), channel_id=1, replica_groups={{0,1,2,3,4,5,6,7},{8,9,10,11,12,13,14,15},{16,17,18,19,20,21,22,23},{24..., dimensions={0} | all-to-all | bytes 360448 | tf_op jit(solution)/shard_map/all_to_all | solution.py:298
  22.0 0.0 copy-start.1
  22.0 0.3 project.1
  22.3 0.0 copy-start
  22.4 28.8 %all_to_all.26 = bf16[64,4,128]{2,1,0:T(4,128)(2,1)S(1)} all-to-all(bf16[64,4,128]{2,1,0:T(4,128)(2,1)S(1)} %bitcast.27), channel_id=1, replica_groups={{0,8,16,24,32,40,48,56,64,72,80,88,96,104,112,120,128,136,144,152,160,1..., dimensions={0} | all-to-all | bytes 131072 | tf_op jit(solution)/shard_map/all_to_all | solution.py:313
  51.1 7.9 %all_to_all.27 = bf16[4,256,128]{2,1,0:T(8,128)(2,1)S(1)} all-to-all(bf16[4,256,128]{2,1,0:T(8,128)(2,1)S(1)} %broadcast_in_dim.20), channel_id=1, replica_groups=mesh['ep'=128,'tp'=4] {'tp'}, dimensions={0} | all-to-all | bytes 524288 | tf_op jit(solution)/shard_map/all_to_all | solution.py:316
  59.1 5.3 %all-gather = bf16[8,256,128]{2,1,0:T(8,128)(2,1)S(1)} all-gather(bf16[4,256,128]{2,1,0:T(8,128)(2,1)S(1)} %all_to_all.27), channel_id=2, replica_groups={{0,4},{8,12},{16,20},{24,28},{32,36},{40,44},{48,52},{56,60},{64,68},{7..., dimensions={0}, use_global_device_ids=true | all-gather | bytes 786432 | tf_op jit(solution)/shard_map/all_gather | solution.py:319
  64.3 0.0 copy-done.2
  64.3 0.0 copy-done.1
  64.3 0.0 copy-done
  64.3 1.2 %expert.1 = (bf16[4,256,128]{2,1,0:T(8,128)(2,1)S(1)}, bf16[4,256,128]{2,1,0:T(8,128)(2,1)S(1)}) custom-call(bf16[2,4,256,128]{3,2,1,0:T(8,128)(2,1)S(1)} %bitcast.21, f32[1,1024]{1,0:T(1,128)S(1)} %get-tuple-element.16.gain, bf16[448,1024]{1,0:T(8,128)(2,1)S(1)} %bitcast.23, bf16[448,1024]{1,0:T(8,128)(2,1)S(1)} %bitcast.24, bf16[448,1024]{1,0:T(8,128)(2,1)S(1)} %bitcast.25), custom_call_target="tpu_custom_call" | custom-call | tf_op jit(solution)/shard_map/expert/pallas_call | solution.py:320
  65.5 2.2 %all-gather.1 = bf16[8,256,128]{2,1,0:T(8,128)(2,1)S(1)} all-gather(bf16[4,256,128]{2,1,0:T(8,128)(2,1)S(1)} %get-tuple-element.18), channel_id=3, replica_groups={{0,4},{8,12},{16,20},{24,28},{32,36},{40,44},{48,52},{56,60},{64,68},{7..., dimensions={0}, use_global_device_ids=true | all-gather | bytes 786432 | tf_op jit(solution)/shard_map/all_gather | solution.py:329
  67.7 0.1 pair.1
  67.8 8.8 %all_to_all.28 = bf16[4,256,128]{2,1,0:T(8,128)(2,1)S(1)} all-to-all(bf16[4,256,128]{2,1,0:T(8,128)(2,1)S(1)} %pair.1), channel_id=1, replica_groups=mesh['ep'=128,'tp'=4] {'tp'}, dimensions={0} | all-to-all | bytes 524288 | tf_op jit(solution)/shard_map/all_to_all | solution.py:338
  76.6 17.9 %all_to_all.29 = bf16[64,4,128]{2,1,0:T(4,128)(2,1)S(1)} all-to-all(bf16[64,4,128]{2,1,0:T(4,128)(2,1)S(1)} %bitcast.35), channel_id=1, replica_groups={{0,8,16,24,32,40,48,56,64,72,80,88,96,104,112,120,128,136,144,152,160,1..., dimensions={0} | all-to-all | bytes 131072 | tf_op jit(solution)/shard_map/all_to_all | solution.py:340
  94.5 0.2 combine.1
  94.7 3.8 %all-gather.2 = bf16[32,128]{1,0:T(8,128)(2,1)S(1)} all-gather(bf16[16,128]{1,0:T(8,128)(2,1)S(1)} %get-tuple-element.21), channel_id=4, replica_groups={{0,4},{8,12},{16,20},{24,28},{32,36},{40,44},{48,52},{56,60},{64,68},{7..., dimensions={0}, use_global_device_ids=true | all-gather | bytes 12288 | tf_op jit(solution)/shard_map/all_gather | solution.py:361
  98.5 0.6 finish.1
  (6 shorter events, 0.1 us)
Async XLA Ops:
  0.0 0.7 copy-start.8
  0.9 0.7 copy-start.9
  0.9 0.7 copy-start.6
  0.9 0.7 copy-start.7
  0.9 0.7 copy-start.4
  0.9 0.7 copy-start.3
  0.9 0.7 copy-start.5
  1.6 62.7 %copy-start.2 = (bf16[1,448,1024]{2,1,0:T(8,128)(2,1)S(1)}, bf16[1,448,1024]{2,1,0:T(8,128)(2,1)}, u32[]{:S(2)}) copy-start(bf16[1,448,1024]{2,1,0:T(8,128)(2,1)} %param.41) | copy-start | bytes 2752516
  22.0 42.3 %copy-start.1 = (bf16[1,1024,448]{1,2,0:T(8,128)(2,1)S(1)}, bf16[1,1024,448]{1,2,0:T(8,128)(2,1)}, u32[]{:S(2)}) copy-start(bf16[1,1024,448]{1,2,0:T(8,128)(2,1)} %param.40) | copy-start | bytes 2752516
  22.3 42.0 %copy-start = (bf16[1,1024,448]{1,2,0:T(8,128)(2,1)S(1)}, bf16[1,1024,448]{1,2,0:T(8,128)(2,1)}, u32[]{:S(2)}) copy-start(bf16[1,1024,448]{1,2,0:T(8,128)(2,1)} %param.39) | copy-start | bytes 2752516

commit v4 on v3

--- a/solution.py
+++ b/solution.py
@@ -1,3 +1,5 @@
+import math
+
 import jax
 import jax.numpy as jnp
 from jax import lax
@@ -15,7 +17,6 @@
 rope_base = 10000.0
 VMEM = pl.BlockSpec(memory_space=pltpu.VMEM)
 HBM = pl.BlockSpec(memory_space=pltpu.HBM)
-SMEM = pl.BlockSpec(memory_space=pltpu.SMEM)
 NT = (((1,), (1,)), ((), ()))
 TN = (((0,), (0,)), ((), ()))
 f32 = jnp.float32
@@ -43,10 +44,19 @@
     return values * cosine + turned * sine
 
 
+def angles_of(positions, width):
+    lane = (iota((positions.shape[0], width), 1) % (ROPE // 2)).astype(f32)
+    angle = positions * jnp.exp(lane * (-2.0 / ROPE * math.log(rope_base)))
+    turns = jnp.floor(angle * (0.5 / math.pi) + 0.5)
+    angle = (angle - turns * 6.28125) - turns * (2.0 * math.pi - 6.28125)
+    return jnp.cos(angle), jnp.sin(angle)
+
+
 def attend_kernel(
-    lengths, attn_gain, q_gain, kv_gain, ffn_gain, table, routes, weights, h_hidden, h_wqd, h_wqn,
-    h_wqr, h_wkv, h_wkr, h_wuk, h_rope, h_latent, h_wuv, h_wout, payload, gain_out, hidden, wqd,
-    wqn, wqr, wkv, wkr, wuk, rope, latent, wuv, mixed, sems,
+    h_lengths, h_attn_gain, h_q_gain, h_kv_gain, h_ffn_gain, h_routes, h_weights, h_hidden, h_wqd,
+    h_wqn, h_wqr, h_wkv, h_wkr, h_wuk, h_rope, h_latent, h_wuv, h_wout, payload, gain_out, lengths,
+    attn_gain, q_gain, kv_gain, routes, weights, hidden, wqd, wqn, wqr, wkv, wkr, wuk, rope,
+    latent, wuv, sems,
 ):
     own = latent.shape[0]
     rows, width = hidden.shape
@@ -55,122 +65,128 @@
     part = h_wout.shape[0] // 2
     t = lax.axis_index("tp")
     c = lax.axis_index("ep") % 2
-    pairs = [
-        (h_hidden, hidden), (h_wqd, wqd), (h_wqn, wqn), (h_wqr, wqr), (h_wkv, wkv), (h_wkr, wkr),
-        (h_wuk, wuk), (h_rope, rope), (h_latent, latent), (h_wuv, wuv),
+    moves = [
+        (h_hidden, hidden), (h_attn_gain, attn_gain), (h_lengths, lengths), (h_wqd, wqd),
+        (h_q_gain, q_gain), (h_wqn, wqn), (h_wqr, wqr), (h_wuk, wuk), (h_wkv, wkv), (h_wkr, wkr),
+        (h_kv_gain, kv_gain), (h_rope, rope), (h_latent, latent), (h_wuv, wuv), (h_routes, routes),
+        (h_weights, weights), (h_ffn_gain, gain_out),
     ]
-    copies = [pltpu.make_async_copy(src, dst, sems.at[n]) for n, (src, dst) in enumerate(pairs)]
     for j in range(2 * tp):
         column = (2 * (j % tp) + j // tp) * block
-        copies.append(
-            pltpu.make_async_copy(
+        moves.append(
+            (
                 h_wout.at[pl.ds(pl.multiple_of(c * part, part), part), column : column + block],
                 payload.at[j, 0:part, :],
-                sems.at[len(copies)],
             )
         )
+    copies = [pltpu.make_async_copy(src, dst, sems.at[n]) for n, (src, dst) in enumerate(moves)]
     for copy in copies:
         copy.start()
-    gain_out[...] = ffn_gain[...]
+
+    row, col = iota((rows, rows), 0), iota((rows, rows), 1)
+    pick = jnp.where(
+        (iota((8, rows), 1) == t * own + iota((8, rows), 0)) & (iota((8, rows), 0) < own), 1.0, 0.0
+    ).astype(bf16)
+    copies[0].wait()
+    own_hidden = dot(pick, hidden[...])
+    copies[1].wait()
+    normed = rms(own_hidden, attn_gain[...]).astype(bf16)
+    copies[2].wait()
+    positions = jnp.zeros((8, 1), f32)
+    for s in range(own):
+        positions = jnp.where(iota((8, 1), 0) == s, lengths[s].astype(f32), positions)
+    cosine, sine = angles_of(positions, HEADS * ROPE)
+    copies[3].wait()
+    q_first = dot(normed, wqd[...])
+    copies[4].wait()
+    q_small = rms(q_first, q_gain[...]).astype(bf16)
+    copies[5].wait()
+    q_plain = dot(q_small, wqn[...])
+    copies[6].wait()
+    q_turned = turn(dot(q_small, wqr[...]), cosine, sine)
+
+    def spread(values, size):
+        head = iota((HEADS, values.shape[1]), 1) // size
+        mask = head == iota((HEADS, values.shape[1]), 0)
+        return jnp.concatenate(
+            [jnp.where(mask, values[s : s + 1, :], 0.0) for s in range(own)], axis=0
+        ).astype(bf16)
+
+    def per_head(values):
+        return jnp.concatenate(
+            [jnp.broadcast_to(values[s : s + 1, :], (HEADS, values.shape[1])) for s in range(own)],
+            axis=0,
+        )
+
+    copies[7].wait()
+    q_latent = dot(spread(q_plain, NOPE), wuk[...], NT).astype(bf16)
+    fold = jnp.where(
+        iota((HEADS * ROPE, ROPE), 0) % ROPE == iota((HEADS * ROPE, ROPE), 1), 1.0, 0.0
+    ).astype(bf16)
+    q_rope = dot(spread(q_turned, ROPE), fold).astype(bf16)
+    copies[8].wait()
+    latent_first = dot(normed, wkv[...])
+    copies[9].wait()
+    plain_key = dot(normed, wkr[...], NT)
+    copies[10].wait()
+    new_latent = per_head(rms(latent_first, kv_gain[...]).astype(bf16).astype(f32))
+    swap = jnp.concatenate([-plain_key[:, ROPE // 2 :], plain_key[:, : ROPE // 2]], axis=1)
+    new_rope = per_head(
+        (plain_key * cosine[:, :ROPE] + swap * sine[:, :ROPE]).astype(bf16).astype(f32)
+    )
+    scale = (NOPE + ROPE) ** (-0.5)
+    fresh = (
+        jnp.sum(q_latent.astype(f32) * new_latent, axis=1, keepdims=True)
+        + jnp.sum(q_rope.astype(f32) * new_rope, axis=1, keepdims=True)
+    ) * scale
+    copies[11].wait()
+    copies[12].wait()
+    limits = per_head(positions).astype(jnp.int32)
+    heads = [slice(s * HEADS, (s + 1) * HEADS) for s in range(own)]
+    scores = jnp.concatenate(
+        [dot(q_latent[h], latent[s], NT) + dot(q_rope[h], rope[s]) for s, h in enumerate(heads)],
+        axis=0,
+    )
+    scores = jnp.where(iota(scores.shape, 1) < limits, scores * scale, -1e30)
+    highest = jnp.maximum(jnp.max(scores, axis=1, keepdims=True), fresh)
+    past = jnp.exp(scores - highest)
+    now = jnp.exp(fresh - highest)
+    divisor = jnp.sum(past, axis=1, keepdims=True) + now
+    past = (past / divisor).astype(bf16)
+    mix = jnp.concatenate([dot(past[h], latent[s]) for s, h in enumerate(heads)], axis=0)
+    mix = (mix + (now / divisor).astype(bf16).astype(f32) * new_latent).astype(bf16)
+    copies[13].wait()
+    values = dot(mix, wuv[...])
+    head = iota((HEADS, HEADS * VDIM), 1) // VDIM == iota((HEADS, HEADS * VDIM), 0)
+    head_values = jnp.concatenate(
+        [jnp.sum(jnp.where(head, values[h], 0.0), axis=0, keepdims=True) for h in heads], axis=0
+    )
+
+    copies[14].wait()
+    copies[15].wait()
+    copies[16].wait()
     r0, r1 = routes[0:1, :], routes[1:2, :]
-    row, col = iota((rows, rows), 0), iota((rows, rows), 1)
-    earlier = col < row
-    ids = []
-    for line in (r0, r1):
+    lane = iota((rows, 128), 1)
+    meta = jnp.zeros((rows, 128), f32)
+    for k, line in enumerate((r0, r1)):
         mine = jnp.sum(jnp.where(row == col, line, 0), axis=1, keepdims=True)
-        hits = (jnp.where(r0 == mine, 1, 0) + jnp.where(r1 == mine, 1, 0)) * jnp.where(
-            earlier, 1, 0
-        )
-        slot = jnp.sum(hits, axis=1, keepdims=True)
-        ids.append(mine * 4 + c * 2 + slot)
-    lane = iota((rows, 128), 1)
-    meta = jnp.where(lane == 0, ids[0], jnp.where(lane == 1, ids[1], 0)).astype(f32)
-    for k in range(2):
+        hits = jnp.where(r0 == mine, 1, 0) + jnp.where(r1 == mine, 1, 0)
+        slot = jnp.sum(jnp.where(col < row, hits, 0), axis=1, keepdims=True)
+        meta = jnp.where(lane == k, (mine * 4 + c * 2 + slot).astype(f32), meta)
         rest = jnp.sum(jnp.where(row == col, weights[k : k + 1, :], 0.0), axis=1, keepdims=True)
         for n in range(3):
             piece = rest.astype(bf16).astype(f32)
             meta = jnp.where(lane == 2 + 3 * k + n, piece, meta)
             rest = rest - piece
-    meta = meta.astype(bf16)
-    pick = jnp.where(
-        (iota((8, rows), 1) == t * own + iota((8, rows), 0)) & (iota((8, rows), 0) < own), 1.0, 0.0
-    ).astype(bf16)
-    copies[0].wait()
-    own_hidden = dot(pick, hidden[...])
-    own_meta = dot(pick, meta)
-    normed = rms(own_hidden, attn_gain[...]).astype(bf16)
-    copies[1].wait()
-    q_small = rms(dot(normed, wqd[...]), q_gain[...]).astype(bf16)
-    copies[2].wait()
-    q_plain = dot(q_small, wqn[...])
-    cosine, sine = table[0], table[1]
-    copies[3].wait()
-    q_turned = turn(dot(q_small, wqr[...]), cosine, sine)
-    copies[4].wait()
-    new_latent = rms(dot(normed, wkv[...]), kv_gain[...]).astype(bf16).astype(f32)
-    copies[5].wait()
-    plain_key = dot(normed, wkr[...], NT)
-    swap = jnp.concatenate([-plain_key[:, ROPE // 2 :], plain_key[:, : ROPE // 2]], axis=1)
-    new_rope = (
-        (plain_key * cosine[:, :ROPE] + swap * sine[:, :ROPE]).astype(bf16).astype(f32)
-    )
-
-    def spread(values, size):
-        width = values.shape[1]
-        head = iota((HEADS, width), 1) // size
-        mask = head == iota((HEADS, width), 0)
-        return jnp.concatenate(
-            [jnp.where(mask, values[s : s + 1, :], 0.0) for s in range(own)], axis=0
-        ).astype(bf16)
-
-    copies[6].wait()
-    q_latent = dot(spread(q_plain, NOPE), wuk[...], NT).astype(bf16)
-    fold = jnp.where(
-        iota((HEADS * ROPE, ROPE), 0) % ROPE == iota((HEADS * ROPE, ROPE), 1), 1.0, 0.0
-    ).astype(bf16)
-    q_rope = dot(spread(q_turned, ROPE), fold).astype(bf16)
-    scale = (NOPE + ROPE) ** (-0.5)
-    copies[7].wait()
-    copies[8].wait()
-    for s in range(own):
-        mine = slice(s * HEADS, (s + 1) * HEADS)
-        scores = (
-            dot(q_latent[mine], latent[s], NT) + dot(q_rope[mine], rope[s])
-        ) * scale
-        scores = jnp.where(iota(scores.shape, 1) < lengths[s], scores, -1e30)
-        fresh = (
-            jnp.sum(q_latent[mine].astype(f32) * new_latent[s : s + 1, :], axis=1, keepdims=True)
-            + jnp.sum(q_rope[mine].astype(f32) * new_rope[s : s + 1, :], axis=1, keepdims=True)
-        ) * scale
-        highest = jnp.maximum(jnp.max(scores, axis=1, keepdims=True), fresh)
-        past = jnp.exp(scores - highest)
-        now = jnp.exp(fresh - highest)
-        divisor = jnp.sum(past, axis=1, keepdims=True) + now
-        mix = dot((past / divisor).astype(bf16), latent[s])
-        mix = mix + (now / divisor).astype(bf16).astype(f32) * new_latent[s : s + 1, :]
-        mixed[mine, :] = mix.astype(bf16).astype(f32)
-    copies[9].wait()
-    values = dot(mixed[...].astype(bf16), wuv[...])
-    head = iota((HEADS, HEADS * VDIM), 1) // VDIM == iota((HEADS, HEADS * VDIM), 0)
-    head_values = jnp.concatenate(
-        [
-            jnp.sum(
-                jnp.where(head, values[s * HEADS : (s + 1) * HEADS], 0.0), axis=0, keepdims=True
-            )
-            for s in range(own)
-        ],
-        axis=0,
-    )
-    parts = [
-        head_values[:, b * (HEADS * VDIM // tp) : (b + 1) * (HEADS * VDIM // tp)]
-        for b in range(tp)
-    ]
+    own_meta = dot(pick, meta.astype(bf16))
+    section = HEADS * VDIM // tp
+    parts = [head_values[:, b * section : (b + 1) * section] for b in range(tp)]
     for j in range(2 * tp):
         column = (2 * (j % tp) + j // tp) * block
         payload[j, part:, :] = jnp.concatenate(
             [*parts, own_hidden[:own, column : column + block], own_meta[:own]], axis=0
         ).astype(bf16)
-    for copy in copies[len(pairs) :]:
+    for copy in copies[17:]:
         copy.wait()
 
 
@@ -269,10 +285,8 @@
     same_core = [[2 * k + c for k in range(experts)] for c in range(2)]
     pairs = [[2 * k, 2 * k + 1] for k in range(experts)]
 
-    inverse = jnp.power(rope_base, -jnp.arange(0, ROPE, 2).astype(f32) / ROPE)
-    positions = jnp.pad(lengths, (0, 8 - own)).astype(f32)
-    angles = positions[:, None] * jnp.tile(inverse, 2 * HEADS)[None, :]
-    table = jnp.stack([jnp.cos(angles), jnp.sin(angles)])
+    small = [lengths, attn_gain[None], q_gain[None], kv_gain[None], ffn_gain[None], routes.T,
+             route_weights.T]
     big = [hidden_in, w_qdown, w_qnope, w_qrope, w_kvdown, w_krope.T, w_ukey, cache_rope,
            cache_latent, w_uvalue]
     lines = w_out.shape[0] // 2 + own * (tp + 2)
@@ -284,17 +298,14 @@
             jax.ShapeDtypeStruct((2 * tp, lines, block), bf16),
             jax.ShapeDtypeStruct((1, width), f32),
         ],
-        in_specs=[SMEM] + [VMEM] * 7 + [HBM] * 11,
+        in_specs=[HBM] * 18,
         out_specs=[VMEM] * 2,
-        scratch_shapes=[pltpu.VMEM(a.shape, a.dtype) for a in big]
-        + [pltpu.VMEM((own * HEADS, KVLORA), f32)]
-        + [pltpu.SemaphoreType.DMA((len(big) + 2 * tp,))],
+        scratch_shapes=[pltpu.SMEM(lengths.shape, jnp.int32)]
+        + [pltpu.VMEM(a.shape, a.dtype) for a in [*small[1:4], *small[5:], *big]]
+        + [pltpu.SemaphoreType.DMA((17 + 2 * tp,))],
         compiler_params=pltpu.CompilerParams(vmem_limit_bytes=12 << 20),
         name="attend",
-    )(
-        lengths, attn_gain[None], q_gain[None], kv_gain[None], ffn_gain[None], table, routes.T,
-        route_weights.T, *[pltpu.with_memory_space_constraint(a, pltpu.HBM) for a in [*big, w_out]],
-    )
+    )(*[pltpu.with_memory_space_constraint(a, pltpu.HBM) for a in [*small, *big, w_out]])
     inbox = lax.all_to_all(
         payload, ("ep", "tp"), 0, 0, axis_index_groups=columns, tiled=True
     )

time: 99.4 us -> 96.3 us (0.969)
  local copies, waits for them, and re-layouts: 1.49 us -> 0.05 us
  Pallas kernels: 7.82 us -> 6.43 us
    pallas_call x1, Pallas kernels: 5.47 us -> 4.08 us  [per_device(): pl.pallas_call(attend_kernel, out_shape=[jax.ShapeDtypeStruct((2 * tp, li...]
    unnamed x20 -> x6, local copies, waits for them, and re-layouts: 1.37 us -> 0.01 us
where the time goes in v4:
time: 96.3 us; the launch traced here: 96 us
  blocking collectives  89.5 us (93%)
  Pallas kernels  6.43 us (7%)
    all_to_all x1, blocking collectives, per_device(): lax.all_to_all(sent.reshape(experts, 4, block), 'ep', 0, 0, axis_index_gr...  28.8 us
    all_to_all x1, blocking collectives, per_device(): lax.all_to_all(unit_out.reshape(experts, 4, block), 'ep', 0, 0, axis_inde...  17.9 us
    all_to_all x1, blocking collectives, per_device(): lax.all_to_all(payload, ('ep', 'tp'), 0, 0, axis_index_groups=columns, ti...  14.9 us
    all_to_all x1, blocking collectives, per_device(): pieces = lax.all_to_all(partial, 'tp', 0, 0, tiled=True)  8.78 us
    all_to_all x1, blocking collectives, per_device(): lax.all_to_all(jnp.broadcast_to(arrived, (tp, rows, block)), 'tp', 0, 0,...  7.92 us
    all_gather x1, blocking collectives, per_device(): both = lax.all_gather(over_tp, 'ep', axis_index_groups=pairs)  5.26 us
    pallas_call x1, Pallas kernels, per_device(): pl.pallas_call(attend_kernel, out_shape=[jax.ShapeDtypeStruct((2 * tp, li...  4.08 us
    all_gather x1, blocking collectives, per_device(): lax.all_gather(send, 'ep', axis_index_groups=pairs)  3.8 us

profile of v4, /device:TPU:1, one launch (start us, length us, event | category | flops | bytes accessed | tf_op | source)
XLA Modules:
  0.0 96.0 jit_solution(7085282793383182593)
XLA Ops:
  0.0 0.0 copy-start.2
  0.0 4.1 %attend.1 = (bf16[8,88,128]{2,1,0:T(8,128)(2,1)S(1)}, f32[1,1024]{1,0:T(1,128)S(1)}) custom-call(s32[4]{0:T(128)} %h_lengths.1, f32[1,1024]{1,0:T(1,128)} %bitcast.32, f32[1,256]{1,0:T(1,128)} %bitcast.34, f32[1,128]{1,0:T(1,128)} %bitcast.37, f32[1,1024]{1,0:T(1,128)} %bitcast.33, s32[2,16]{1,0:T(2,128)} %bitcast.35, f32[2,16]{1,0:T(2,128)} %bitcast.36, ...), custom_call_target="tpu_custom_call" | custom-call | tf_op jit(solution)/shard_map/attend/pallas_call | solution.py:295
  4.1 14.9 %all_to_all.25.inbox = bf16[8,88,128]{2,1,0:T(8,128)(2,1)S(1)} all-to-all(bf16[8,88,128]{2,1,0:T(8,128)(2,1)S(1)} %get-tuple-element.14), channel_id=1, replica_groups={{0,1,2,3,4,5,6,7},{8,9,10,11,12,13,14,15},{16,17,18,19,20,21,22,23},{24..., dimensions={0} | all-to-all | bytes 360448 | tf_op jit(solution)/shard_map/all_to_all | solution.py:309
  19.0 0.0 copy-start.1
  19.0 0.3 project.1
  19.3 0.0 copy-start
  19.3 28.8 %all_to_all.26 = bf16[64,4,128]{2,1,0:T(4,128)(2,1)S(1)} all-to-all(bf16[64,4,128]{2,1,0:T(4,128)(2,1)S(1)} %bitcast.27), channel_id=1, replica_groups={{0,8,16,24,32,40,48,56,64,72,80,88,96,104,112,120,128,136,144,152,160,1..., dimensions={0} | all-to-all | bytes 131072 | tf_op jit(solution)/shard_map/all_to_all | solution.py:324
  48.1 7.9 %all_to_all.27 = bf16[4,256,128]{2,1,0:T(8,128)(2,1)S(1)} all-to-all(bf16[4,256,128]{2,1,0:T(8,128)(2,1)S(1)} %broadcast_in_dim.19), channel_id=1, replica_groups=mesh['ep'=128,'tp'=4] {'tp'}, dimensions={0} | all-to-all | bytes 524288 | tf_op jit(solution)/shard_map/all_to_all | solution.py:327
  56.0 5.3 %all-gather = bf16[8,256,128]{2,1,0:T(8,128)(2,1)S(1)} all-gather(bf16[4,256,128]{2,1,0:T(8,128)(2,1)S(1)} %all_to_all.27), channel_id=2, replica_groups={{0,4},{8,12},{16,20},{24,28},{32,36},{40,44},{48,52},{56,60},{64,68},{7..., dimensions={0}, use_global_device_ids=true | all-gather | bytes 786432 | tf_op jit(solution)/shard_map/all_gather | solution.py:330
  61.3 0.0 copy-done.2
  61.3 0.0 copy-done.1
  61.3 0.0 copy-done
  61.3 1.2 %expert.1 = (bf16[4,256,128]{2,1,0:T(8,128)(2,1)S(1)}, bf16[4,256,128]{2,1,0:T(8,128)(2,1)S(1)}) custom-call(bf16[2,4,256,128]{3,2,1,0:T(8,128)(2,1)S(1)} %bitcast.21, f32[1,1024]{1,0:T(1,128)S(1)} %get-tuple-element.16.gain, bf16[448,1024]{1,0:T(8,128)(2,1)S(1)} %bitcast.23, bf16[448,1024]{1,0:T(8,128)(2,1)S(1)} %bitcast.24, bf16[448,1024]{1,0:T(8,128)(2,1)S(1)} %bitcast.25), custom_call_target="tpu_custom_call" | custom-call | tf_op jit(solution)/shard_map/expert/pallas_call | solution.py:331
  62.5 2.2 %all-gather.1 = bf16[8,256,128]{2,1,0:T(8,128)(2,1)S(1)} all-gather(bf16[4,256,128]{2,1,0:T(8,128)(2,1)S(1)} %get-tuple-element.18), channel_id=3, replica_groups={{0,4},{8,12},{16,20},{24,28},{32,36},{40,44},{48,52},{56,60},{64,68},{7..., dimensions={0}, use_global_device_ids=true | all-gather | bytes 786432 | tf_op jit(solution)/shard_map/all_gather | solution.py:340
  64.6 0.1 pair.1
  64.7 8.8 %all_to_all.28 = bf16[4,256,128]{2,1,0:T(8,128)(2,1)S(1)} all-to-all(bf16[4,256,128]{2,1,0:T(8,128)(2,1)S(1)} %pair.1), channel_id=1, replica_groups=mesh['ep'=128,'tp'=4] {'tp'}, dimensions={0} | all-to-all | bytes 524288 | tf_op jit(solution)/shard_map/all_to_all | solution.py:349
  73.5 17.9 %all_to_all.29 = bf16[64,4,128]{2,1,0:T(4,128)(2,1)S(1)} all-to-all(bf16[64,4,128]{2,1,0:T(4,128)(2,1)S(1)} %bitcast.29), channel_id=1, replica_groups={{0,8,16,24,32,40,48,56,64,72,80,88,96,104,112,120,128,136,144,152,160,1..., dimensions={0} | all-to-all | bytes 131072 | tf_op jit(solution)/shard_map/all_to_all | solution.py:351
  91.4 0.2 combine.1
  91.6 3.8 %all-gather.2 = bf16[32,128]{1,0:T(8,128)(2,1)S(1)} all-gather(bf16[16,128]{1,0:T(8,128)(2,1)S(1)} %get-tuple-element.21), channel_id=4, replica_groups={{0,4},{8,12},{16,20},{24,28},{32,36},{40,44},{48,52},{56,60},{64,68},{7..., dimensions={0}, use_global_device_ids=true | all-gather | bytes 12288 | tf_op jit(solution)/shard_map/all_gather | solution.py:372
  95.4 0.6 finish.1
  (2 shorter events, 0.1 us)
Async XLA Ops:
  0.0 61.3 %copy-start.2 = (bf16[1,448,1024]{2,1,0:T(8,128)(2,1)S(1)}, bf16[1,448,1024]{2,1,0:T(8,128)(2,1)}, u32[]{:S(2)}) copy-start(bf16[1,448,1024]{2,1,0:T(8,128)(2,1)} %param.41) | copy-start | bytes 2752516
  19.0 42.3 %copy-start.1 = (bf16[1,1024,448]{1,2,0:T(8,128)(2,1)S(1)}, bf16[1,1024,448]{1,2,0:T(8,128)(2,1)}, u32[]{:S(2)}) copy-start(bf16[1,1024,448]{1,2,0:T(8,128)(2,1)} %param.40) | copy-start | bytes 2752516
  19.3 42.0 %copy-start = (bf16[1,1024,448]{1,2,0:T(8,128)(2,1)S(1)}, bf16[1,1024,448]{1,2,0:T(8,128)(2,1)}, u32[]{:S(2)}) copy-start(bf16[1,1024,448]{1,2,0:T(8,128)(2,1)} %param.39) | copy-start | bytes 2752516

commit v5 on v4

--- a/solution.py
+++ b/solution.py
@@ -54,15 +54,13 @@
 
 def attend_kernel(
     h_lengths, h_attn_gain, h_q_gain, h_kv_gain, h_ffn_gain, h_routes, h_weights, h_hidden, h_wqd,
-    h_wqn, h_wqr, h_wkv, h_wkr, h_wuk, h_rope, h_latent, h_wuv, h_wout, payload, gain_out, lengths,
+    h_wqn, h_wqr, h_wkv, h_wkr, h_wuk, h_rope, h_latent, h_wuv, payload, gain_out, lengths,
     attn_gain, q_gain, kv_gain, routes, weights, hidden, wqd, wqn, wqr, wkv, wkr, wuk, rope,
     latent, wuv, sems,
 ):
     own = latent.shape[0]
     rows, width = hidden.shape
     tp = rows // own
-    block = width // (2 * tp)
-    part = h_wout.shape[0] // 2
     t = lax.axis_index("tp")
     c = lax.axis_index("ep") % 2
     moves = [
@@ -71,14 +69,6 @@
         (h_kv_gain, kv_gain), (h_rope, rope), (h_latent, latent), (h_wuv, wuv), (h_routes, routes),
         (h_weights, weights), (h_ffn_gain, gain_out),
     ]
-    for j in range(2 * tp):
-        column = (2 * (j % tp) + j // tp) * block
-        moves.append(
-            (
-                h_wout.at[pl.ds(pl.multiple_of(c * part, part), part), column : column + block],
-                payload.at[j, 0:part, :],
-            )
-        )
     copies = [pltpu.make_async_copy(src, dst, sems.at[n]) for n, (src, dst) in enumerate(moves)]
     for copy in copies:
         copy.start()
@@ -179,77 +169,94 @@
             meta = jnp.where(lane == 2 + 3 * k + n, piece, meta)
             rest = rest - piece
     own_meta = dot(pick, meta.astype(bf16))
-    section = HEADS * VDIM // tp
-    parts = [head_values[:, b * section : (b + 1) * section] for b in range(tp)]
-    for j in range(2 * tp):
-        column = (2 * (j % tp) + j // tp) * block
-        payload[j, part:, :] = jnp.concatenate(
-            [*parts, own_hidden[:own, column : column + block], own_meta[:own]], axis=0
-        ).astype(bf16)
-    for copy in copies[17:]:
-        copy.wait()
-
-
-def project_kernel(inbox, sent, residual_out, meta_out):
+    lines = [head_values[:, n : n + 128] for n in range(0, HEADS * VDIM, 128)]
+    lines += [own_hidden[:own, n : n + 128] for n in range(0, width, 128)]
+    lines = jnp.concatenate([*lines, own_meta[:own]], axis=0).astype(bf16)
+    for j in range(payload.shape[0]):
+        payload[j] = lines
+
+
+def project_kernel(inbox, w, residual, meta):
     devices, lines, block = inbox.shape
-    tp = devices // 2
-    own = 4
-    part = lines - own * (tp + 2)
-    tails = [inbox[j, part:, :].astype(f32) for j in range(devices)]
+    tp, depth, width = w.shape
+    own = lines // (tp + width // block + 1)
+    tails = [inbox[j].astype(f32) for j in range(devices)]
 
     def section(n):
         return jnp.concatenate([tail[n * own : (n + 1) * own] for tail in tails], axis=0)
 
-    total = jnp.zeros((devices * own, block), f32)
-    for b in range(tp):
-        w = jnp.concatenate([inbox[b, :part, :], inbox[tp + b, :part, :]], axis=0)
-        total = total + dot(section(b).astype(bf16), w).astype(bf16).astype(f32)
-    residual = section(tp) + total
-    meta = section(tp + 1)
-    targets = meta.astype(jnp.int32)
-    lanes = iota((devices * own, sent.shape[0]), 1)
+    meta[...] = section(tp + width // block)
+
+    @pl.when(lax.axis_index("ep") % 2 == 0)
+    def _():
+        total = jnp.zeros(residual.shape, f32)
+        for b in range(tp):
+            total = total + dot(section(b).astype(bf16), w[b]).astype(bf16).astype(f32)
+        hidden = jnp.concatenate([section(tp + n) for n in range(width // block)], axis=1)
+        residual[...] = hidden + total
+
+
+def select_kernel(shared, meta, sent, mine):
+    c = lax.axis_index("ep") % 2
+    t = lax.axis_index("tp")
+    rows, width = shared.shape[1:]
+    quarter = mine.shape[1]
+    block = quarter // 2
+    group = rows // 2
+    residual = shared[0]
+    half = jnp.concatenate(
+        [
+            jnp.where(c == 0, residual[:, n : n + block], residual[:, n + block : n + quarter])
+            for n in range(0, width, quarter)
+        ],
+        axis=1,
+    ).astype(bf16)
+    targets = meta[...].astype(jnp.int32)
+    lanes = iota((rows, sent.shape[0]), 1)
     chooser = jnp.where(
         (targets[:, 0:1] == lanes) | (targets[:, 1:2] == lanes), 1.0, 0.0
     ).astype(bf16)
-    sent[...] = dot(chooser, residual.astype(bf16), TN).astype(bf16)
-    residual_out[...] = residual
-    meta_out[...] = meta
+    sent[...] = dot(chooser, half, TN).astype(bf16)
+    own = jnp.where(c == 0, residual[:group], residual[group:])
+    kept = own[:, :quarter]
+    for n in range(1, width // quarter):
+        kept = jnp.where(t == n, own[:, n * quarter : (n + 1) * quarter], kept)
+    mine[...] = kept
 
 
 def expert_kernel(both, gain, wg, wu, wd, stay, away, x):
     c = lax.axis_index("ep") % 2
-    cores, tp, rows, block = both.shape
-    quarter = cores * block
+    cores, rows, half = both.shape
+    block = 128
     for part in range(2):
-        size = rows // 2
-        here = slice(part * size, (part + 1) * size)
+        here = slice(part * rows // 2, (part + 1) * rows // 2)
         values = jnp.concatenate(
-            [both[n, t, here, :] for t in range(tp) for n in range(cores)], axis=1
+            [both[n, here, m : m + block] for m in range(0, half, block) for n in range(cores)],
+            axis=1,
         ).astype(f32)
         x[here, :] = rms(values, gain[...]).astype(bf16)
     gate = dot(x[...], wg[...], NT)
     up = dot(x[...], wu[...], NT)
     inner = (gate / (1.0 + jnp.exp(-gate)) * up).astype(bf16)
-    for t in range(tp):
-        term = dot(inner, wd[:, t * quarter : (t + 1) * quarter])
+    for m in range(0, half, block):
+        term = dot(inner, wd[:, 2 * m : 2 * m + 2 * block])
         first, second = term[:, :block], term[:, block:]
-        stay[t] = jnp.where(c == 0, first, second).astype(bf16)
-        away[t] = jnp.where(c == 0, second, first).astype(bf16)
+        stay[:, m : m + block] = jnp.where(c == 0, first, second).astype(bf16)
+        away[:, m : m + block] = jnp.where(c == 0, second, first).astype(bf16)
 
 
 def pair_kernel(stay, swapped, out):
     partner = 1 - lax.axis_index("ep") % 2
-    for t in range(stay.shape[0]):
-        out[t] = (stay[t].astype(f32) + swapped[partner, t].astype(f32)).astype(bf16)
-
-
-def combine_kernel(returned, meta, residual, send, keep):
-    c = lax.axis_index("ep") % 2
+    out[...] = (stay[...].astype(f32) + swapped[partner].astype(f32)).astype(bf16)
+
+
+def combine_kernel(returned, meta, out):
     rows = meta.shape[0]
     group = rows // 2
+    devices, _, block = out.shape
     targets = meta[...].astype(jnp.int32)
     lanes = iota((rows, returned.shape[0]), 1)
-    blended = jnp.zeros(residual.shape, f32)
+    blended = jnp.zeros((rows, returned.shape[1]), f32)
     for k in range(2):
         chooser = jnp.where(targets[:, k : k + 1] == lanes, 1.0, 0.0).astype(bf16)
         first = 2 + 3 * k
@@ -257,17 +264,21 @@
             :, first + 2 : first + 3
         ]
         blended = blended + weight * dot(chooser, returned[...])
-    total = residual[...] + blended
-    send[...] = jnp.where(c == 0, total[group:], total[:group]).astype(bf16)
-    keep[...] = jnp.where(c == 0, total[:group], total[group:])
-
-
-def finish_kernel(swapped, keep, out):
-    c = lax.axis_index("ep") % 2
-    block = keep.shape[1]
-    mine = keep[...]
-    out[:, :block] = jnp.where(c == 0, mine, swapped[0].astype(f32)).astype(bf16)
-    out[:, block:] = jnp.where(c == 0, swapped[1].astype(f32), mine).astype(bf16)
+    tp = devices // 2
+    for j in range(devices):
+        g, t = j // tp, j % tp
+        out[j] = blended[g * group : (g + 1) * group, t * block : (t + 1) * block]
+
+
+def finish_kernel(terms, residual, out):
+    devices, _, block = terms.shape
+    tp = devices // 2
+    for n in range(2):
+        total = terms[n * tp]
+        for t in range(1, tp):
+            total = total + terms[n * tp + t]
+        here = slice(n * block, (n + 1) * block)
+        out[:, here] = (residual[:, here] + total).astype(bf16)
 
 
 def per_device(
@@ -280,7 +291,7 @@
     tp = lax.axis_size("tp")
     experts = lax.axis_size("ep") // 2
     quarter = width // tp
-    block = quarter // 2
+    core = lax.axis_index("ep") % 2
     columns = [[(2 * k + c) * tp + t for c in range(2) for t in range(tp)] for k in range(experts)]
     same_core = [[2 * k + c for k in range(experts)] for c in range(2)]
     pairs = [[2 * k, 2 * k + 1] for k in range(experts)]
@@ -289,48 +300,64 @@
              route_weights.T]
     big = [hidden_in, w_qdown, w_qnope, w_qrope, w_kvdown, w_krope.T, w_ukey, cache_rope,
            cache_latent, w_uvalue]
-    lines = w_out.shape[0] // 2 + own * (tp + 2)
+    lines = own * (tp + width // 128 + 1)
     rows = experts * 4
+    half = width // 2
     small_vmem = pltpu.CompilerParams(vmem_limit_bytes=8 << 20)
     payload, gain = pl.pallas_call(
         attend_kernel,
         out_shape=[
-            jax.ShapeDtypeStruct((2 * tp, lines, block), bf16),
+            jax.ShapeDtypeStruct((2 * tp, lines, 128), bf16),
             jax.ShapeDtypeStruct((1, width), f32),
         ],
-        in_specs=[HBM] * 18,
+        in_specs=[HBM] * 17,
         out_specs=[VMEM] * 2,
         scratch_shapes=[pltpu.SMEM(lengths.shape, jnp.int32)]
         + [pltpu.VMEM(a.shape, a.dtype) for a in [*small[1:4], *small[5:], *big]]
-        + [pltpu.SemaphoreType.DMA((17 + 2 * tp,))],
+        + [pltpu.SemaphoreType.DMA((17,))],
         compiler_params=pltpu.CompilerParams(vmem_limit_bytes=12 << 20),
         name="attend",
-    )(*[pltpu.with_memory_space_constraint(a, pltpu.HBM) for a in [*small, *big, w_out]])
+    )(*[pltpu.with_memory_space_constraint(a, pltpu.HBM) for a in [*small, *big]])
+    w_all = lax.cond(
+        core == 0,
+        lambda w: lax.all_to_all(jnp.broadcast_to(w, (tp, *w.shape)), "tp", 0, 0, tiled=True),
+        lambda w: jnp.zeros((tp, *w.shape), w.dtype),
+        w_out,
+    )
+    payload, w_all = lax.optimization_barrier((payload, w_all))
     inbox = lax.all_to_all(
         payload, ("ep", "tp"), 0, 0, axis_index_groups=columns, tiled=True
     )
-    sent, residual, meta = pl.pallas_call(
+    residual, meta = pl.pallas_call(
         project_kernel,
         out_shape=[
-            jax.ShapeDtypeStruct((rows, block), bf16),
-            jax.ShapeDtypeStruct((2 * group_rows, block), f32),
+            jax.ShapeDtypeStruct((2 * group_rows, width), f32),
             jax.ShapeDtypeStruct((2 * group_rows, 128), f32),
         ],
-        in_specs=[VMEM],
-        out_specs=[VMEM] * 3,
+        in_specs=[VMEM] * 2,
+        out_specs=[VMEM] * 2,
         compiler_params=small_vmem,
         name="project",
-    )(inbox)
+    )(inbox, w_all)
+    shared = lax.all_gather(residual, "ep", axis_index_groups=pairs)
+    sent, mine = pl.pallas_call(
+        select_kernel,
+        out_shape=[
+            jax.ShapeDtypeStruct((rows, half), bf16),
+            jax.ShapeDtypeStruct((group_rows, quarter), f32),
+        ],
+        in_specs=[VMEM] * 2,
+        out_specs=[VMEM] * 2,
+        compiler_params=small_vmem,
+        name="select",
+    )(shared, meta)
     arrived = lax.all_to_all(
-        sent.reshape(experts, 4, block), "ep", 0, 0, axis_index_groups=same_core, tiled=True
-    ).reshape(rows, block)
-    over_tp = lax.all_to_all(
-        jnp.broadcast_to(arrived, (tp, rows, block)), "tp", 0, 0, tiled=True
-    )
-    both = lax.all_gather(over_tp, "ep", axis_index_groups=pairs)
+        sent.reshape(experts, 4, half), "ep", 0, 0, axis_index_groups=same_core, tiled=True
+    ).reshape(rows, half)
+    both = lax.all_gather(arrived, "ep", axis_index_groups=pairs)
     stay, away = pl.pallas_call(
         expert_kernel,
-        out_shape=[jax.ShapeDtypeStruct((tp, rows, block), bf16)] * 2,
+        out_shape=[jax.ShapeDtypeStruct((rows, half), bf16)] * 2,
         in_specs=[VMEM] * 5,
         out_specs=[VMEM] * 2,
         scratch_shapes=[pltpu.VMEM((rows, width), bf16)],
@@ -340,28 +367,24 @@
     swapped = lax.all_gather(away, "ep", axis_index_groups=pairs)
     partial = pl.pallas_call(
         pair_kernel,
-        out_shape=jax.ShapeDtypeStruct((tp, rows, block), bf16),
+        out_shape=jax.ShapeDtypeStruct((rows, half), bf16),
         in_specs=[VMEM] * 2,
         out_specs=VMEM,
         compiler_params=small_vmem,
         name="pair",
     )(stay, swapped)
-    pieces = lax.all_to_all(partial, "tp", 0, 0, tiled=True)
-    unit_out = jnp.sum(pieces.astype(f32), axis=0).astype(bf16)
     returned = lax.all_to_all(
-        unit_out.reshape(experts, 4, block), "ep", 0, 0, axis_index_groups=same_core, tiled=True
-    ).reshape(rows, block)
-    send, keep = pl.pallas_call(
+        partial.reshape(experts, 4, half), "ep", 0, 0, axis_index_groups=same_core, tiled=True
+    ).reshape(rows, half)
+    terms = pl.pallas_call(
         combine_kernel,
-        out_shape=[
-            jax.ShapeDtypeStruct((group_rows, block), bf16),
-            jax.ShapeDtypeStruct((group_rows, block), f32),
-        ],
-        in_specs=[VMEM] * 3,
-        out_specs=[VMEM] * 2,
+        out_shape=jax.ShapeDtypeStruct((2 * tp, group_rows, half // tp), f32),
+        in_specs=[VMEM] * 2,
+        out_specs=VMEM,
         compiler_params=small_vmem,
         name="combine",
-    )(returned, meta, residual)
+    )(returned, meta)
+    terms = lax.all_to_all(terms, ("ep", "tp"), 0, 0, axis_index_groups=columns, tiled=True)
     return pl.pallas_call(
         finish_kernel,
         out_shape=jax.ShapeDtypeStruct((group_rows, quarter), bf16),
@@ -369,7 +392,7 @@
         out_specs=VMEM,
         compiler_params=small_vmem,
         name="finish",
-    )(lax.all_gather(send, "ep", axis_index_groups=pairs), keep)
+    )(terms, mine)
 
 
 def solution(mesh):

time: 96.3 us -> 116 us (1.20)
  blocking collectives: 89.5 us -> 109 us
    all_to_all x1, blocking collectives: 14.9 us -> 28.5 us  [per_device(): lax.all_to_all(payload, ('ep', 'tp'), 0, 0, axis_index_groups=columns, ti...]
    all_to_all x4 -> x3, blocking collectives: 63.3 us -> 70.6 us  [the longest x1 35 us: per_device(): lax.all_to_all(sent.reshape(experts, 4, half), 'ep', 0, 0, axis_index_gro...]
    all_gather x2, blocking collectives: 9.06 us -> 7.32 us  [the longest x1 4.89 us: per_device(): both = lax.all_gather(arrived, 'ep', axis_index_groups=pairs)]
where the time goes in v5:
time: 116 us; the launch traced here: 115 us
  blocking collectives  109 us (94%)
  Pallas kernels  6.32 us (5%)
    all_to_all x1, blocking collectives, per_device(): lax.all_to_all(sent.reshape(experts, 4, half), 'ep', 0, 0, axis_index_gro...  35 us
    all_to_all x1, blocking collectives, per_device(): lax.all_to_all(payload, ('ep', 'tp'), 0, 0, axis_index_groups=columns, ti...  28.5 us
    all_to_all x1, blocking collectives, per_device(): lax.all_to_all(partial.reshape(experts, 4, half), 'ep', 0, 0, axis_index_...  24.8 us
    all_to_all x1, blocking collectives, per_device(): lax.all_to_all(terms, ('ep', 'tp'), 0, 0, axis_index_groups=columns, tile...  10.8 us
    all_gather x1, blocking collectives, per_device(): both = lax.all_gather(arrived, 'ep', axis_index_groups=pairs)  4.89 us
    pallas_call x1, Pallas kernels, per_device(): pl.pallas_call(attend_kernel, out_shape=[jax.ShapeDtypeStruct((2 * tp, li...  3.92 us
    all_gather x1, blocking collectives, per_device(): shared = lax.all_gather(residual, 'ep', axis_index_groups=pairs)  2.43 us

profile of v5, /device:TPU:1, one launch (start us, length us, event | category | flops | bytes accessed | tf_op | source)
XLA Modules:
  0.0 115.5 jit_solution(5940818531050434667)
XLA Ops:
  0.0 0.1 conditional.1
  0.0 0.1 broadcast.3
  0.1 3.9 %attend.1 = (bf16[8,52,128]{2,1,0:T(8,128)(2,1)S(1)}, f32[1,1024]{1,0:T(1,128)S(1)}) custom-call(s32[4]{0:T(128)} %h_lengths.1, f32[1,1024]{1,0:T(1,128)} %bitcast.22, f32[1,256]{1,0:T(1,128)} %bitcast.24, f32[1,128]{1,0:T(1,128)} %bitcast.27, f32[1,1024]{1,0:T(1,128)} %bitcast.23, s32[2,16]{1,0:T(2,128)} %bitcast.25, f32[2,16]{1,0:T(2,128)} %bitcast.26, ...), custom_call_target="tpu_custom_call" | custom-call | tf_op jit(solution)/shard_map/attend/pallas_call | solution.py:307
  4.1 28.5 %all_to_all.25.inbox = bf16[8,52,128]{2,1,0:T(8,128)(2,1)S(1)} all-to-all(bf16[8,52,128]{2,1,0:T(8,128)(2,1)S(1)} %get-tuple-element.20), channel_id=1, replica_groups={{0,1,2,3,4,5,6,7},{8,9,10,11,12,13,14,15},{16,17,18,19,20,21,22,23},{24..., dimensions={0} | all-to-all | bytes 212992 | tf_op jit(solution)/shard_map/all_to_all | solution.py:328
  32.6 0.0 copy-start.2
  32.6 2.4 %all-gather = f32[64,1024]{1,0:T(8,128)S(1)} all-gather(f32[32,1024]{1,0:T(8,128)S(1)} %get-tuple-element.22), channel_id=2, replica_groups={{0,4},{8,12},{16,20},{24,28},{32,36},{40,44},{48,52},{56,60},{64,68},{7..., dimensions={0}, use_global_device_ids=true | all-gather | bytes 393216 | tf_op jit(solution)/shard_map/all_gather | solution.py:342
  35.1 0.3 select.3
  35.4 0.1 reshape.9
  35.5 0.0 copy-start
  35.5 0.0 copy-start.1
  35.5 35.0 %all_to_all.26 = bf16[64,4,512]{2,1,0:T(4,128)(2,1)S(1)} all-to-all(bf16[64,4,512]{2,1,0:T(4,128)(2,1)S(1)} %reshape.9), channel_id=1, replica_groups={{0,8,16,24,32,40,48,56,64,72,80,88,96,104,112,120,128,136,144,152,160,1..., dimensions={0} | all-to-all | bytes 524288 | tf_op jit(solution)/shard_map/all_to_all | solution.py:354
  70.5 0.1 all_gather_reshape.3
  70.6 4.9 %all_gather.17.both = bf16[2,256,512]{2,1,0:T(8,128)(2,1)S(1)} all-gather(bf16[1,256,512]{2,1,0:T(8,128)(2,1)S(1)} %all_gather_reshape.3), channel_id=1, replica_groups={{0,4},{8,12},{16,20},{24,28},{32,36},{40,44},{48,52},{56,60},{64,68},{7..., dimensions={0}, use_global_device_ids=true | all-gather | bytes 786432 | tf_op jit(solution)/shard_map/all_gather | solution.py:357
  75.5 0.0 copy-done.2
  75.5 0.0 copy-done
  75.5 0.0 copy-done.1
  75.5 1.2 %expert.1 = (bf16[256,512]{1,0:T(8,128)(2,1)S(1)}, bf16[256,512]{1,0:T(8,128)(2,1)S(1)}) custom-call(bf16[2,256,512]{2,1,0:T(8,128)(2,1)S(1)} %all_gather.17.both, f32[1,1024]{1,0:T(1,128)S(1)} %get-tuple-element.25.gain, bf16[448,1024]{1,0:T(8,128)(2,1)S(1)} %bitcast.18, bf16[448,1024]{1,0:T(8,128)(2,1)S(1)} %bitcast.19, bf16[448,1024]{1,0:T(8,128)(2,1)S(1)} %bitcast.20), custom_call_target="tpu_custom_call" | custom-call | tf_op jit(solution)/shard_map/expert/pallas_call | solution.py:358
  76.7 2.2 %all-gather.1 = bf16[512,512]{1,0:T(8,128)(2,1)S(1)} all-gather(bf16[256,512]{1,0:T(8,128)(2,1)S(1)} %get-tuple-element.27), channel_id=3, replica_groups={{0,4},{8,12},{16,20},{24,28},{32,36},{40,44},{48,52},{56,60},{64,68},{7..., dimensions={0}, use_global_device_ids=true | all-gather | bytes 786432 | tf_op jit(solution)/shard_map/all_gather | solution.py:367
  78.9 0.1 pair.1
  78.9 0.1 reshape.10
  79.0 24.8 %all_to_all.27 = bf16[64,4,512]{2,1,0:T(4,128)(2,1)S(1)} all-to-all(bf16[64,4,512]{2,1,0:T(4,128)(2,1)S(1)} %reshape.10), channel_id=1, replica_groups={{0,8,16,24,32,40,48,56,64,72,80,88,96,104,112,120,128,136,144,152,160,1..., dimensions={0} | all-to-all | bytes 524288 | tf_op jit(solution)/shard_map/all_to_all | solution.py:376
  103.8 0.1 reshape.11.returned
  103.9 0.2 combine.1
  104.1 10.8 %all_to_all.28.terms = f32[8,16,128]{2,1,0:T(8,128)S(1)} all-to-all(f32[8,16,128]{2,1,0:T(8,128)S(1)} %combine.1), channel_id=1, replica_groups={{0,1,2,3,4,5,6,7},{8,9,10,11,12,13,14,15},{16,17,18,19,20,21,22,23},{24..., dimensions={0} | all-to-all | bytes 131072 | tf_op jit(solution)/shard_map/all_to_all | solution.py:387
  114.9 0.6 finish.1
  (1 shorter events, 0.0 us)
Async XLA Ops:
  32.6 42.9 %copy-start.2 = (bf16[1,448,1024]{2,1,0:T(8,128)(2,1)S(1)}, bf16[1,448,1024]{2,1,0:T(8,128)(2,1)}, u32[]{:S(2)}) copy-start(bf16[1,448,1024]{2,1,0:T(8,128)(2,1)} %param.43) | copy-start | bytes 2752516
  35.5 40.0 %copy-start = (bf16[1,1024,448]{1,2,0:T(8,128)(2,1)S(1)}, bf16[1,1024,448]{1,2,0:T(8,128)(2,1)}, u32[]{:S(2)}) copy-start(bf16[1,1024,448]{1,2,0:T(8,128)(2,1)} %param.41) | copy-start | bytes 2752516
  35.5 40.0 %copy-start.1 = (bf16[1,1024,448]{1,2,0:T(8,128)(2,1)S(1)}, bf16[1,1024,448]{1,2,0:T(8,128)(2,1)}, u32[]{:S(2)}) copy-start(bf16[1,1024,448]{1,2,0:T(8,128)(2,1)} %param.42) | copy-start | bytes 2752516

commit v6 on v4

--- a/solution.py
+++ b/solution.py
@@ -216,12 +216,11 @@
     meta_out[...] = meta
 
 
-def expert_kernel(both, gain, wg, wu, wd, stay, away, x):
+def expert_kernel(both, gain, residual, wg, wu, wd, stay, away, x):
     c = lax.axis_index("ep") % 2
     cores, tp, rows, block = both.shape
-    quarter = cores * block
+    size = rows // 2
     for part in range(2):
-        size = rows // 2
         here = slice(part * size, (part + 1) * size)
         values = jnp.concatenate(
             [both[n, t, here, :] for t in range(tp) for n in range(cores)], axis=1
@@ -230,44 +229,55 @@
     gate = dot(x[...], wg[...], NT)
     up = dot(x[...], wu[...], NT)
     inner = (gate / (1.0 + jnp.exp(-gate)) * up).astype(bf16)
+    line = iota((size, rows), 0)
+    place = iota((size, rows), 1)
+    first = line // 2 * 4 + line % 2
+    mine = jnp.where(place == first + 2 * c, 1.0, 0.0).astype(bf16)
+    other = jnp.where(place == first + 2 * (1 - c), 1.0, 0.0).astype(bf16)
+    away[:size, :] = dot(dot(other, inner).astype(bf16), wd[...]).astype(bf16)
+    stay[...] = dot(dot(mine, inner).astype(bf16), wd[...]).astype(bf16)
+    group = residual.shape[0] // 2
+    theirs = jnp.where(c == 0, residual[group:, :], residual[:group, :])
+    high = theirs.astype(bf16).astype(f32)
+    away[size:, :] = jnp.concatenate(
+        [high, theirs - high, jnp.zeros((group, wd.shape[1] - 2 * block), f32)], axis=1
+    ).astype(bf16)
+
+
+def pair_kernel(stay, swapped, residual, out, kept):
+    c = lax.axis_index("ep") % 2
+    partner = 1 - c
+    tp, rows, quarter = out.shape
     for t in range(tp):
-        term = dot(inner, wd[:, t * quarter : (t + 1) * quarter])
-        first, second = term[:, :block], term[:, block:]
-        stay[t] = jnp.where(c == 0, first, second).astype(bf16)
-        away[t] = jnp.where(c == 0, second, first).astype(bf16)
-
-
-def pair_kernel(stay, swapped, out):
-    partner = 1 - lax.axis_index("ep") % 2
-    for t in range(stay.shape[0]):
-        out[t] = (stay[t].astype(f32) + swapped[partner, t].astype(f32)).astype(bf16)
-
-
-def combine_kernel(returned, meta, residual, send, keep):
+        here = slice(t * quarter, (t + 1) * quarter)
+        out[t] = (
+            stay[:, here].astype(f32) + swapped[partner, :rows, here].astype(f32)
+        ).astype(bf16)
+    block = residual.shape[1]
+    group = residual.shape[0] // 2
+    extra = swapped[partner, rows:, :].astype(f32)
+    theirs = extra[:, :block] + extra[:, block : 2 * block]
+    own = jnp.where(c == 0, residual[:group, :], residual[group:, :])
+    kept[:, :block] = jnp.where(c == 0, own, theirs)
+    kept[:, block:] = jnp.where(c == 0, theirs, own)
+
+
+def combine_kernel(returned, meta, residual, out):
     c = lax.axis_index("ep") % 2
-    rows = meta.shape[0]
-    group = rows // 2
-    targets = meta[...].astype(jnp.int32)
-    lanes = iota((rows, returned.shape[0]), 1)
+    group = residual.shape[0]
+    own = jnp.where(c == 0, meta[:group, :], meta[group:, :])
+    targets = own.astype(jnp.int32)
+    targets = targets // 4 * 2 + targets % 2
+    lanes = iota((group, returned.shape[0]), 1)
     blended = jnp.zeros(residual.shape, f32)
     for k in range(2):
         chooser = jnp.where(targets[:, k : k + 1] == lanes, 1.0, 0.0).astype(bf16)
         first = 2 + 3 * k
-        weight = (meta[:, first : first + 1] + meta[:, first + 1 : first + 2]) + meta[
+        weight = (own[:, first : first + 1] + own[:, first + 1 : first + 2]) + own[
             :, first + 2 : first + 3
         ]
         blended = blended + weight * dot(chooser, returned[...])
-    total = residual[...] + blended
-    send[...] = jnp.where(c == 0, total[group:], total[:group]).astype(bf16)
-    keep[...] = jnp.where(c == 0, total[:group], total[group:])
-
-
-def finish_kernel(swapped, keep, out):
-    c = lax.axis_index("ep") % 2
-    block = keep.shape[1]
-    mine = keep[...]
-    out[:, :block] = jnp.where(c == 0, mine, swapped[0].astype(f32)).astype(bf16)
-    out[:, block:] = jnp.where(c == 0, swapped[1].astype(f32), mine).astype(bf16)
+    out[...] = (residual[...] + blended).astype(bf16)
 
 
 def per_device(
@@ -330,46 +340,44 @@
     both = lax.all_gather(over_tp, "ep", axis_index_groups=pairs)
     stay, away = pl.pallas_call(
         expert_kernel,
-        out_shape=[jax.ShapeDtypeStruct((tp, rows, block), bf16)] * 2,
-        in_specs=[VMEM] * 5,
+        out_shape=[
+            jax.ShapeDtypeStruct((rows // 2, width), bf16),
+            jax.ShapeDtypeStruct((rows // 2 + group_rows, width), bf16),
+        ],
+        in_specs=[VMEM] * 6,
         out_specs=[VMEM] * 2,
         scratch_shapes=[pltpu.VMEM((rows, width), bf16)],
         compiler_params=pltpu.CompilerParams(vmem_limit_bytes=20 << 20),
         name="expert",
-    )(both, gain, jnp.swapaxes(w_gate[0], 0, 1), jnp.swapaxes(w_up[0], 0, 1), w_down[0])
+    )(
+        both, gain, residual, jnp.swapaxes(w_gate[0], 0, 1), jnp.swapaxes(w_up[0], 0, 1),
+        w_down[0],
+    )
     swapped = lax.all_gather(away, "ep", axis_index_groups=pairs)
-    partial = pl.pallas_call(
+    partial, kept = pl.pallas_call(
         pair_kernel,
-        out_shape=jax.ShapeDtypeStruct((tp, rows, block), bf16),
-        in_specs=[VMEM] * 2,
-        out_specs=VMEM,
-        compiler_params=small_vmem,
-        name="pair",
-    )(stay, swapped)
-    pieces = lax.all_to_all(partial, "tp", 0, 0, tiled=True)
-    unit_out = jnp.sum(pieces.astype(f32), axis=0).astype(bf16)
-    returned = lax.all_to_all(
-        unit_out.reshape(experts, 4, block), "ep", 0, 0, axis_index_groups=same_core, tiled=True
-    ).reshape(rows, block)
-    send, keep = pl.pallas_call(
-        combine_kernel,
         out_shape=[
-            jax.ShapeDtypeStruct((group_rows, block), bf16),
-            jax.ShapeDtypeStruct((group_rows, block), f32),
+            jax.ShapeDtypeStruct((tp, rows // 2, quarter), bf16),
+            jax.ShapeDtypeStruct((group_rows, quarter), f32),
         ],
         in_specs=[VMEM] * 3,
         out_specs=[VMEM] * 2,
         compiler_params=small_vmem,
-        name="combine",
-    )(returned, meta, residual)
+        name="pair",
+    )(stay, swapped, residual)
+    pieces = lax.all_to_all(partial, "tp", 0, 0, tiled=True)
+    unit_out = jnp.sum(pieces.astype(f32), axis=0).astype(bf16)
+    returned = lax.all_to_all(
+        unit_out.reshape(experts, 2, quarter), "ep", 0, 0, axis_index_groups=same_core, tiled=True
+    ).reshape(rows // 2, quarter)
     return pl.pallas_call(
-        finish_kernel,
+        combine_kernel,
         out_shape=jax.ShapeDtypeStruct((group_rows, quarter), bf16),
-        in_specs=[VMEM] * 2,
+        in_specs=[VMEM] * 3,
         out_specs=VMEM,
         compiler_params=small_vmem,
-        name="finish",
-    )(lax.all_gather(send, "ep", axis_index_groups=pairs), keep)
+        name="combine",
+    )(returned, meta, kept)
 
 
 def solution(mesh):

time: 96.3 us -> 92.9 us (0.965)
  blocking collectives: 89.5 us -> 85.7 us
    all_gather x1 -> x0, blocking collectives: 3.8 us -> none  [per_device(): lax.all_gather(send, 'ep', axis_index_groups=pairs)]
    pallas_call x4 -> x3, Pallas kernels: 2.03 us -> 2.39 us  [the longest x1 1.49 us: per_device(): pl.pallas_call(expert_kernel, out_shape=[jax.ShapeDtypeStruct((rows // 2,...]
where the time goes in v6:
time: 92.9 us; the launch traced here: 92.6 us
  blocking collectives  85.7 us (92%)
  Pallas kernels  6.78 us (7%)
    all_to_all x1, blocking collectives, per_device(): lax.all_to_all(sent.reshape(experts, 4, block), 'ep', 0, 0, axis_index_gr...  28.8 us
    all_to_all x1, blocking collectives, per_device(): lax.all_to_all(unit_out.reshape(experts, 2, quarter), 'ep', 0, 0, axis_in...  17.8 us
    all_to_all x1, blocking collectives, per_device(): lax.all_to_all(payload, ('ep', 'tp'), 0, 0, axis_index_groups=columns, ti...  14.9 us
    all_to_all x1, blocking collectives, per_device(): pieces = lax.all_to_all(partial, 'tp', 0, 0, tiled=True)  8.79 us
    all_to_all x1, blocking collectives, per_device(): lax.all_to_all(jnp.broadcast_to(arrived, (tp, rows, block)), 'tp', 0, 0,...  7.92 us
    all_gather x1, blocking collectives, per_device(): both = lax.all_gather(over_tp, 'ep', axis_index_groups=pairs)  5.26 us
    pallas_call x1, Pallas kernels, per_device(): pl.pallas_call(attend_kernel, out_shape=[jax.ShapeDtypeStruct((2 * tp, li...  4.08 us
    all_gather x1, blocking collectives, per_device(): swapped = lax.all_gather(away, 'ep', axis_index_groups=pairs)  2.23 us

profile of v6, /device:TPU:1, one launch (start us, length us, event | category | flops | bytes accessed | tf_op | source)
XLA Modules:
  0.0 92.6 jit_solution(18418483652285285565)
XLA Ops:
  0.0 0.0 copy-start.2
  0.0 4.1 %attend.1 = (bf16[8,88,128]{2,1,0:T(8,128)(2,1)S(1)}, f32[1,1024]{1,0:T(1,128)S(1)}) custom-call(s32[4]{0:T(128)} %h_lengths.1, f32[1,1024]{1,0:T(1,128)} %bitcast.26, f32[1,256]{1,0:T(1,128)} %bitcast.28, f32[1,128]{1,0:T(1,128)} %bitcast.31, f32[1,1024]{1,0:T(1,128)} %bitcast.27, s32[2,16]{1,0:T(2,128)} %bitcast.29, f32[2,16]{1,0:T(2,128)} %bitcast.30, ...), custom_call_target="tpu_custom_call" | custom-call | tf_op jit(solution)/shard_map/attend/pallas_call | solution.py:305
  4.1 14.9 %all_to_all.25.inbox = bf16[8,88,128]{2,1,0:T(8,128)(2,1)S(1)} all-to-all(bf16[8,88,128]{2,1,0:T(8,128)(2,1)S(1)} %get-tuple-element.14), channel_id=1, replica_groups={{0,1,2,3,4,5,6,7},{8,9,10,11,12,13,14,15},{16,17,18,19,20,21,22,23},{24..., dimensions={0} | all-to-all | bytes 360448 | tf_op jit(solution)/shard_map/all_to_all | solution.py:319
  19.0 0.0 copy-start.1
  19.0 0.3 project.1
  19.3 0.0 copy-start
  19.3 28.8 %all_to_all.26 = bf16[64,4,128]{2,1,0:T(4,128)(2,1)S(1)} all-to-all(bf16[64,4,128]{2,1,0:T(4,128)(2,1)S(1)} %bitcast.23), channel_id=1, replica_groups={{0,8,16,24,32,40,48,56,64,72,80,88,96,104,112,120,128,136,144,152,160,1..., dimensions={0} | all-to-all | bytes 131072 | tf_op jit(solution)/shard_map/all_to_all | solution.py:334
  48.1 7.9 %all_to_all.27 = bf16[4,256,128]{2,1,0:T(8,128)(2,1)S(1)} all-to-all(bf16[4,256,128]{2,1,0:T(8,128)(2,1)S(1)} %broadcast_in_dim.19), channel_id=1, replica_groups=mesh['ep'=128,'tp'=4] {'tp'}, dimensions={0} | all-to-all | bytes 524288 | tf_op jit(solution)/shard_map/all_to_all | solution.py:337
  56.0 5.3 %all-gather = bf16[8,256,128]{2,1,0:T(8,128)(2,1)S(1)} all-gather(bf16[4,256,128]{2,1,0:T(8,128)(2,1)S(1)} %all_to_all.27), channel_id=2, replica_groups={{0,4},{8,12},{16,20},{24,28},{32,36},{40,44},{48,52},{56,60},{64,68},{7..., dimensions={0}, use_global_device_ids=true | all-gather | bytes 786432 | tf_op jit(solution)/shard_map/all_gather | solution.py:340
  61.3 0.0 copy-done.2
  61.3 0.0 copy-done.1
  61.3 0.0 copy-done
  61.3 1.5 %expert.1 = (bf16[128,1024]{1,0:T(8,128)(2,1)S(1)}, bf16[144,1024]{1,0:T(8,128)(2,1)S(1)}) custom-call(bf16[2,4,256,128]{3,2,1,0:T(8,128)(2,1)S(1)} %bitcast.19, f32[1,1024]{1,0:T(1,128)S(1)} %get-tuple-element.16.gain, f32[32,128]{1,0:T(8,128)S(1)} %get-tuple-element.17.residual, bf16[448,1024]{1,0:T(8,128)(2,1)S(1)} %bitcast.20, ...), custom_call_target="tpu_custom_call" | custom-call | tf_op jit(solution)/shard_map/expert/pallas_call | solution.py:341
  62.8 2.2 %all-gather.1 = bf16[288,1024]{1,0:T(8,128)(2,1)S(1)} all-gather(bf16[144,1024]{1,0:T(8,128)(2,1)S(1)} %get-tuple-element.19), channel_id=3, replica_groups={{0,4},{8,12},{16,20},{24,28},{32,36},{40,44},{48,52},{56,60},{64,68},{7..., dimensions={0}, use_global_device_ids=true | all-gather | bytes 884736 | tf_op jit(solution)/shard_map/all_gather | solution.py:356
  65.0 0.1 pair.1
  65.1 8.8 %all_to_all.28 = bf16[4,128,256]{2,1,0:T(8,128)(2,1)S(1)} all-to-all(bf16[4,128,256]{2,1,0:T(8,128)(2,1)S(1)} %get-tuple-element.20), channel_id=1, replica_groups=mesh['ep'=128,'tp'=4] {'tp'}, dimensions={0} | all-to-all | bytes 524288 | tf_op jit(solution)/shard_map/all_to_all | solution.py:368
  74.0 17.8 %all_to_all.29 = bf16[64,2,256]{2,1,0:T(2,128)(2,1)S(1)} all-to-all(bf16[64,2,256]{2,1,0:T(2,128)(2,1)S(1)} %reshape.14), channel_id=1, replica_groups={{0,8,16,24,32,40,48,56,64,72,80,88,96,104,112,120,128,136,144,152,160,1..., dimensions={0} | all-to-all | bytes 131072 | tf_op jit(solution)/shard_map/all_to_all | solution.py:370
  91.8 0.8 combine.1
  (4 shorter events, 0.1 us)
Async XLA Ops:
  0.0 61.3 %copy-start.2 = (bf16[1,448,1024]{2,1,0:T(8,128)(2,1)S(1)}, bf16[1,448,1024]{2,1,0:T(8,128)(2,1)}, u32[]{:S(2)}) copy-start(bf16[1,448,1024]{2,1,0:T(8,128)(2,1)} %param.41) | copy-start | bytes 2752516
  19.0 42.3 %copy-start.1 = (bf16[1,1024,448]{1,2,0:T(8,128)(2,1)S(1)}, bf16[1,1024,448]{1,2,0:T(8,128)(2,1)}, u32[]{:S(2)}) copy-start(bf16[1,1024,448]{1,2,0:T(8,128)(2,1)} %param.40) | copy-start | bytes 2752516
  19.3 42.0 %copy-start = (bf16[1,1024,448]{1,2,0:T(8,128)(2,1)S(1)}, bf16[1,1024,448]{1,2,0:T(8,128)(2,1)}, u32[]{:S(2)}) copy-start(bf16[1,1024,448]{1,2,0:T(8,128)(2,1)} %param.39) | copy-start | bytes 2752516

commit v7 on v6

v7 whole, which is shorter than its diff:
```python
import math

import jax
import jax.numpy as jnp
from jax import lax
from jax.experimental import pallas as pl
from jax.experimental.pallas import tpu as pltpu
from jax.sharding import PartitionSpec as P

HEADS = 8
NOPE = 64
ROPE = 32
VDIM = 64
KVLORA = 128

eps = 1e-06
rope_base = 10000.0
VMEM = pl.BlockSpec(memory_space=pltpu.VMEM)
HBM = pl.BlockSpec(memory_space=pltpu.HBM)
NT = (((1,), (1,)), ((), ()))
TN = (((0,), (0,)), ((), ()))
f32 = jnp.float32
bf16 = jnp.bfloat16


def dot(a, b, dims=(((1,), (0,)), ((), ()))):
    return lax.dot_general(a, b, dims, preferred_element_type=f32)


def iota(shape, dim):
    return lax.broadcasted_iota(jnp.int32, shape, dim)


def rms(values, gain):
    return values * lax.rsqrt(jnp.mean(values * values, axis=-1, keepdims=True) + eps) * gain


def turn(values, cosine, sine):
    width = values.shape[-1]
    lanes = iota(values.shape, 1) % ROPE
    ahead = pltpu.roll(values, width - ROPE // 2, 1)
    behind = pltpu.roll(values, ROPE // 2, 1)
    turned = jnp.where(lanes < ROPE // 2, -ahead, behind)
    return values * cosine + turned * sine


def angles_of(positions, width):
    lane = (iota((positions.shape[0], width), 1) % (ROPE // 2)).astype(f32)
    angle = positions * jnp.exp(lane * (-2.0 / ROPE * math.log(rope_base)))
    turns = jnp.floor(angle * (0.5 / math.pi) + 0.5)
    angle = (angle - turns * 6.28125) - turns * (2.0 * math.pi - 6.28125)
    return jnp.cos(angle), jnp.sin(angle)


def attend_kernel(
    h_lengths, h_attn_gain, h_q_gain, h_kv_gain, h_ffn_gain, h_routes, h_weights, h_hidden, h_wqd,
    h_wqn, h_wqr, h_wkv, h_wkr, h_wuk, h_rope, h_latent, h_wuv, h_wout, h_wg,
    h_wu, h_wd, payload, gain_out, expert, lengths,
    attn_gain, q_gain, kv_gain, routes, weights, hidden, wqd, wqn, wqr, wkv, wkr, wuk, rope,
    latent, wuv, sems,
):
    own = latent.shape[0]
    rows, width = hidden.shape
    tp = rows // own
    block = 128
    part = 2 * h_wout.shape[0]
    t = lax.axis_index("tp")
    moves = [
        (h_hidden, hidden), (h_attn_gain, attn_gain), (h_lengths, lengths), (h_wqd, wqd),
        (h_q_gain, q_gain), (h_wqn, wqn), (h_wqr, wqr), (h_wuk, wuk), (h_wkv, wkv), (h_wkr, wkr),
        (h_kv_gain, kv_gain), (h_rope, rope), (h_latent, latent), (h_wuv, wuv), (h_routes, routes),
        (h_weights, weights), (h_ffn_gain, gain_out),
    ]
    for j in range(tp):
        for n in range(2):
            column = (2 * j + n) * block
            here = slice(n * part // 2, (n + 1) * part // 2)
            moves.append((h_wout.at[:, column : column + block], payload.at[j, here, :]))
    units = h_wd.shape[0]
    for n, source in enumerate((h_wg, h_wu, h_wd)):
        moves.append((source, expert.at[n * units : (n + 1) * units, :]))
    copies = [pltpu.make_async_copy(src, dst, sems.at[n]) for n, (src, dst) in enumerate(moves)]
    for copy in copies:
        copy.start()

    row, col = iota((rows, rows), 0), iota((rows, rows), 1)
    pick = jnp.where(
        (iota((8, rows), 1) == t * own + iota((8, rows), 0)) & (iota((8, rows), 0) < own), 1.0, 0.0
    ).astype(bf16)
    copies[0].wait()
    own_hidden = dot(pick, hidden[...])
    copies[1].wait()
    normed = rms(own_hidden, attn_gain[...]).astype(bf16)
    copies[2].wait()
    positions = jnp.zeros((8, 1), f32)
    for s in range(own):
        positions = jnp.where(iota((8, 1), 0) == s, lengths[s].astype(f32), positions)
    cosine, sine = angles_of(positions, HEADS * ROPE)
    copies[3].wait()
    q_first = dot(normed, wqd[...])
    copies[4].wait()
    q_small = rms(q_first, q_gain[...]).astype(bf16)
    copies[5].wait()
    q_plain = dot(q_small, wqn[...])
    copies[6].wait()
    q_turned = turn(dot(q_small, wqr[...]), cosine, sine)

    def spread(values, size):
        head = iota((HEADS, values.shape[1]), 1) // size
        mask = head == iota((HEADS, values.shape[1]), 0)
        return jnp.concatenate(
            [jnp.where(mask, values[s : s + 1, :], 0.0) for s in range(own)], axis=0
        ).astype(bf16)

    def per_head(values):
        return jnp.concatenate(
            [jnp.broadcast_to(values[s : s + 1, :], (HEADS, values.shape[1])) for s in range(own)],
            axis=0,
        )

    copies[7].wait()
    q_latent = dot(spread(q_plain, NOPE), wuk[...], NT).astype(bf16)
    fold = jnp.where(
        iota((HEADS * ROPE, ROPE), 0) % ROPE == iota((HEADS * ROPE, ROPE), 1), 1.0, 0.0
    ).astype(bf16)
    q_rope = dot(spread(q_turned, ROPE), fold).astype(bf16)
    copies[8].wait()
    latent_first = dot(normed, wkv[...])
    copies[9].wait()
    plain_key = dot(normed, wkr[...], NT)
    copies[10].wait()
    new_latent = per_head(rms(latent_first, kv_gain[...]).astype(bf16).astype(f32))
    swap = jnp.concatenate([-plain_key[:, ROPE // 2 :], plain_key[:, : ROPE // 2]], axis=1)
    new_rope = per_head(
        (plain_key * cosine[:, :ROPE] + swap * sine[:, :ROPE]).astype(bf16).astype(f32)
    )
    scale = (NOPE + ROPE) ** (-0.5)
    fresh = (
        jnp.sum(q_latent.astype(f32) * new_latent, axis=1, keepdims=True)
        + jnp.sum(q_rope.astype(f32) * new_rope, axis=1, keepdims=True)
    ) * scale
    copies[11].wait()
    copies[12].wait()
    limits = per_head(positions).astype(jnp.int32)
    heads = [slice(s * HEADS, (s + 1) * HEADS) for s in range(own)]
    scores = jnp.concatenate(
        [dot(q_latent[h], latent[s], NT) + dot(q_rope[h], rope[s]) for s, h in enumerate(heads)],
        axis=0,
    )
    scores = jnp.where(iota(scores.shape, 1) < limits, scores * scale, -1e30)
    highest = jnp.maximum(jnp.max(scores, axis=1, keepdims=True), fresh)
    past = jnp.exp(scores - highest)
    now = jnp.exp(fresh - highest)
    divisor = jnp.sum(past, axis=1, keepdims=True) + now
    past = (past / divisor).astype(bf16)
    mix = jnp.concatenate([dot(past[h], latent[s]) for s, h in enumerate(heads)], axis=0)
    mix = (mix + (now / divisor).astype(bf16).astype(f32) * new_latent).astype(bf16)
    copies[13].wait()
    values = dot(mix, wuv[...])
    head = iota((HEADS, HEADS * VDIM), 1) // VDIM == iota((HEADS, HEADS * VDIM), 0)
    head_values = jnp.concatenate(
        [jnp.sum(jnp.where(head, values[h], 0.0), axis=0, keepdims=True) for h in heads], axis=0
    )

    copies[14].wait()
    copies[15].wait()
    copies[16].wait()
    r0, r1 = routes[0:1, :], routes[1:2, :]
    lane = iota((rows, 128), 1)
    meta = jnp.zeros((rows, 128), f32)
    for k, line in enumerate((r0, r1)):
        mine = jnp.sum(jnp.where(row == col, line, 0), axis=1, keepdims=True)
        hits = jnp.where(r0 == mine, 1, 0) + jnp.where(r1 == mine, 1, 0)
        slot = jnp.sum(jnp.where(col < row, hits, 0), axis=1, keepdims=True)
        meta = jnp.where(lane == k, (mine * 2 + slot).astype(f32), meta)
        rest = jnp.sum(jnp.where(row == col, weights[k : k + 1, :], 0.0), axis=1, keepdims=True)
        for n in range(3):
            piece = rest.astype(bf16).astype(f32)
            meta = jnp.where(lane == 2 + 3 * k + n, piece, meta)
            rest = rest - piece
    own_meta = dot(pick, meta.astype(bf16))
    parts = [head_values[:, n : n + block] for n in range(0, HEADS * VDIM, block)]
    for j in range(tp):
        column = 2 * j * block
        payload[j, part:, :] = jnp.concatenate(
            [
                *parts,
                own_hidden[:own, column : column + block],
                own_hidden[:own, column + block : column + 2 * block],
                own_meta[:own],
                jnp.zeros((own, block), f32),
            ],
            axis=0,
        ).astype(bf16)
    for copy in copies[17:]:
        copy.wait()


def project_kernel(inbox, sent, residual_out, meta_out):
    tp, lines, block = inbox.shape
    own = residual_out.shape[0] // tp
    part = lines - own * (tp + 4)
    tails = [inbox[j, part:, :].astype(f32) for j in range(tp)]

    def section(n):
        return jnp.concatenate([tail[n * own : (n + 1) * own] for tail in tails], axis=0)

    total = jnp.zeros(residual_out.shape, f32)
    for b in range(tp):
        w = jnp.concatenate([inbox[b, : part // 2, :], inbox[b, part // 2 : part, :]], axis=1)
        total = total + dot(section(b).astype(bf16), w).astype(bf16).astype(f32)
    residual = jnp.concatenate([section(tp), section(tp + 1)], axis=1) + total
    meta = section(tp + 2)
    targets = meta.astype(jnp.int32)
    lanes = iota((tp * own, sent.shape[0]), 1)
    chooser = jnp.where(
        (targets[:, 0:1] == lanes) | (targets[:, 1:2] == lanes), 1.0, 0.0
    ).astype(bf16)
    sent[...] = dot(chooser, residual.astype(bf16), TN).astype(bf16)
    residual_out[...] = residual
    meta_out[...] = meta


def expert_kernel(gathered, gain, own, h_partner, out, x, partner, sem):
    copy = pltpu.make_async_copy(h_partner, partner, sem)
    copy.start()
    tp, rows, quarter = gathered.shape
    values = jnp.concatenate([gathered[t] for t in range(tp)], axis=1).astype(f32)
    x[...] = rms(values, gain[...]).astype(bf16)
    units = own.shape[0] // 3
    inners = []
    for w in (own, partner):
        if w is partner:
            copy.wait()
        gate = dot(x[...], w[:units, :], NT)
        up = dot(x[...], w[units : 2 * units, :], NT)
        inners.append((gate / (1.0 + jnp.exp(-gate)) * up).astype(bf16))
    for t in range(tp):
        here = slice(t * quarter, (t + 1) * quarter)
        out[t] = (
            dot(inners[0], own[2 * units :, here]) + dot(inners[1], partner[2 * units :, here])
        ).astype(bf16)


def combine_kernel(returned, meta, residual, out):
    targets = meta[...].astype(jnp.int32)
    lanes = iota((residual.shape[0], returned.shape[0]), 1)
    blended = jnp.zeros(residual.shape, f32)
    for k in range(2):
        chooser = jnp.where(targets[:, k : k + 1] == lanes, 1.0, 0.0).astype(bf16)
        first = 2 + 3 * k
        weight = (meta[:, first : first + 1] + meta[:, first + 1 : first + 2]) + meta[
            :, first + 2 : first + 3
        ]
        blended = blended + weight * dot(chooser, returned[...])
    out[...] = (residual[...] + blended).astype(bf16)


def per_device(
    hidden_in, attn_gain, w_qdown, q_gain, w_qnope, w_qrope, w_kvdown, kv_gain, w_krope, w_ukey,
    w_uvalue, w_out, cache_latent, cache_rope, lengths, ffn_gain, routes, route_weights, w_gate,
    w_up, w_down,
):
    group_rows, width = hidden_in.shape
    own = lengths.shape[0]
    tp = lax.axis_size("tp")
    experts = lax.axis_size("ep") // 2
    quarter = width // tp
    same_core = [[2 * k + c for k in range(experts)] for c in range(2)]
    swap = [(i, i ^ 1) for i in range(2 * experts)]

    small = [lengths, attn_gain[None], q_gain[None], kv_gain[None], ffn_gain[None], routes.T,
             route_weights.T]
    big = [hidden_in, w_qdown, w_qnope, w_qrope, w_kvdown, w_krope.T, w_ukey, cache_rope,
           cache_latent, w_uvalue]
    lines = 2 * w_out.shape[0] + own * (tp + 4)
    rows = experts * 2
    units = w_down.shape[1]
    last = [w_out, jnp.swapaxes(w_gate[0], 0, 1), jnp.swapaxes(w_up[0], 0, 1), w_down[0]]
    small_vmem = pltpu.CompilerParams(vmem_limit_bytes=8 << 20)
    payload, gain, halves = pl.pallas_call(
        attend_kernel,
        out_shape=[
            jax.ShapeDtypeStruct((tp, lines, 128), bf16),
            jax.ShapeDtypeStruct((1, width), f32),
            jax.ShapeDtypeStruct((3 * units, width), bf16),
        ],
        in_specs=[HBM] * 21,
        out_specs=[VMEM] * 3,
        scratch_shapes=[pltpu.SMEM(lengths.shape, jnp.int32)]
        + [pltpu.VMEM(a.shape, a.dtype) for a in [*small[1:4], *small[5:], *big]]
        + [pltpu.SemaphoreType.DMA((20 + 2 * tp,))],
        compiler_params=pltpu.CompilerParams(vmem_limit_bytes=12 << 20),
        name="attend",
    )(*[pltpu.with_memory_space_constraint(a, pltpu.HBM) for a in [*small, *big, *last]])
    partner = lax.ppermute(halves, "ep", swap)
    inbox = lax.all_to_all(payload, "tp", 0, 0, tiled=True)
    sent, residual, meta = pl.pallas_call(
        project_kernel,
        out_shape=[
            jax.ShapeDtypeStruct((rows, quarter), bf16),
            jax.ShapeDtypeStruct((group_rows, quarter), f32),
            jax.ShapeDtypeStruct((group_rows, 128), f32),
        ],
        in_specs=[VMEM],
        out_specs=[VMEM] * 3,
        compiler_params=small_vmem,
        name="project",
    )(inbox)
    arrived = lax.all_to_all(
        sent.reshape(experts, 2, quarter), "ep", 0, 0, axis_index_groups=same_core, tiled=True
    ).reshape(rows, quarter)
    gathered = lax.all_to_all(
        jnp.broadcast_to(arrived, (tp, rows, quarter)), "tp", 0, 0, tiled=True
    )
    partial = pl.pallas_call(
        expert_kernel,
        out_shape=jax.ShapeDtypeStruct((tp, rows, quarter), bf16),
        in_specs=[VMEM] * 3 + [pl.BlockSpec(memory_space=pl.ANY)],
        out_specs=VMEM,
        scratch_shapes=[
            pltpu.VMEM((rows, width), bf16),
            pltpu.VMEM((3 * units, width), bf16),
            pltpu.SemaphoreType.DMA(()),
        ],
        compiler_params=pltpu.CompilerParams(vmem_limit_bytes=20 << 20),
        name="expert",
    )(gathered, gain, halves, partner)
    pieces = lax.all_to_all(partial, "tp", 0, 0, tiled=True)
    expert_out = jnp.sum(pieces.astype(f32), axis=0).astype(bf16)
    returned = lax.all_to_all(
        expert_out.reshape(experts, 2, quarter), "ep", 0, 0, axis_index_groups=same_core,
        tiled=True,
    ).reshape(rows, quarter)
    return pl.pallas_call(
        combine_kernel,
        out_shape=jax.ShapeDtypeStruct((group_rows, quarter), bf16),
        in_specs=[VMEM] * 3,
        out_specs=VMEM,
        compiler_params=small_vmem,
        name="combine",
    )(returned, meta, residual)


def solution(mesh):
    placed = (
        P("ep", None),
        P(),
        P(),
        P(),
        P(),
        P(),
        P(),
        P(),
        P(),
        P(),
        P(),
        P("tp", None),
        P(("ep", "tp"), None, None),
        P(("ep", "tp"), None, None),
        P(("ep", "tp")),
        P(),
        P("ep", None),
        P("ep", None),
        P("ep", None, "tp"),
        P("ep", None, "tp"),
        P("ep", "tp", None),
    )
    return jax.shard_map(
        per_device, mesh=mesh, in_specs=placed, out_specs=P("ep", "tp"), check_vma=False
    )
```

time: 92.9 us -> 92.1 us (level)
  the two profiles are of different devices: /device:TPU:1 before, /device:TPU:8 now
where the time goes in v7:
time: 92.1 us; the launch traced here: 91.8 us
  blocking collectives  81.6 us (89%)
  Pallas kernels  7.99 us (9%)
  starting transfers between devices  1.92 us (2%)
    all_to_all x1, blocking collectives, per_device(): lax.all_to_all(sent.reshape(experts, 2, quarter), 'ep', 0, 0, axis_index_...  29.9 us
    all_to_all x1, blocking collectives, per_device(): lax.all_to_all(expert_out.reshape(experts, 2, quarter), 'ep', 0, 0, axis_...  19 us
    all_to_all x1, blocking collectives, per_device(): inbox = lax.all_to_all(payload, 'tp', 0, 0, tiled=True)  14.7 us
    all_to_all x1, blocking collectives, per_device(): lax.all_to_all(jnp.broadcast_to(arrived, (tp, rows, quarter)), 'tp', 0, 0...  9.07 us
    all_to_all x1, blocking collectives, per_device(): pieces = lax.all_to_all(partial, 'tp', 0, 0, tiled=True)  9.07 us
    pallas_call x1, Pallas kernels, per_device(): pl.pallas_call(attend_kernel, out_shape=[jax.ShapeDtypeStruct((tp, lines,...  4.02 us
    pallas_call x1, Pallas kernels, per_device(): pl.pallas_call(expert_kernel, out_shape=jax.ShapeDtypeStruct((tp, rows, q...  2.86 us
    ppermute x1, starting transfers between devices, per_device(): partner = lax.ppermute(halves, 'ep', swap)  1.92 us
  transfers between devices with their start and end apart: 1, of which 0 were waited for; matrix products, arithmetic and copies ran while one was open for 0% of the time, Pallas kernels for 0%

profile of v7, /device:TPU:8, one launch (start us, length us, event | category | flops | bytes accessed | tf_op | source)
XLA Modules:
  0.0 91.8 jit_solution(7353782763361491390)
XLA Ops:
  0.0 4.0 %attend.1 = (bf16[4,288,128]{2,1,0:T(8,128)(2,1)S(1)}, f32[1,1024]{1,0:T(1,128)S(1)}, bf16[1344,1024]{1,0:T(8,128)(2,1)S(1)}) custom-call(s32[4]{0:T(128)} %h_lengths.1, f32[1,1024]{1,0:T(1,128)} %bitcast.18, f32[1,256]{1,0:T(1,128)} %bitcast.20, f32[1,128]{1,0:T(1,128)} %bitcast.23, f32[1,1024]{1,0:T(1,128)} %bitcast.19, s32[2,16]{1,0:T(2,128)} %bitcast.21, ...), custom_call_target="tpu_custom_call" | custom-call | tf_op jit(solution)/shard_map/attend/pallas_call | solution.py:281
  4.0 1.9 %collective-permute-start = (bf16[1344,1024]{1,0:T(8,128)(2,1)S(1)}, bf16[1344,1024]{1,0:T(8,128)(2,1)}, u32[]{:S(2)}, u32[]{:S(2)}) collective-permute-start(bf16[1344,1024]{1,0:T(8,128)(2,1)S(1)} %get-tuple-element.14.own), channel_id=1, source_target_pairs={{0,4},{4,0},{8,12},{12,8},{16,20},{20,16},{24,28},{28,24},{32,36},... | collective-permute-start | bytes 8257544 | tf_op jit(solution)/shard_map/ppermute | solution.py:296
  6.0 14.7 %all_to_all.25.inbox = bf16[4,288,128]{2,1,0:T(8,128)(2,1)S(1)} all-to-all(bf16[4,288,128]{2,1,0:T(8,128)(2,1)S(1)} %get-tuple-element.11), channel_id=1, replica_groups=mesh['ep'=128,'tp'=4] {'tp'}, dimensions={0} | all-to-all | bytes 589824 | tf_op jit(solution)/shard_map/all_to_all | solution.py:297
  20.6 0.3 project.1
  21.0 29.9 %all_to_all.26 = bf16[64,2,256]{2,1,0:T(2,128)(2,1)S(1)} all-to-all(bf16[64,2,256]{2,1,0:T(2,128)(2,1)S(1)} %reshape.12), channel_id=1, replica_groups={{0,8,16,24,32,40,48,56,64,72,80,88,96,104,112,120,128,136,144,152,160,1..., dimensions={0} | all-to-all | bytes 131072 | tf_op jit(solution)/shard_map/all_to_all | solution.py:310
  50.9 9.1 %all_to_all.27.gathered = bf16[4,128,256]{2,1,0:T(8,128)(2,1)S(1)} all-to-all(bf16[4,128,256]{2,1,0:T(8,128)(2,1)S(1)} %broadcast_in_dim.19), channel_id=1, replica_groups=mesh['ep'=128,'tp'=4] {'tp'}, dimensions={0} | all-to-all | bytes 524288 | tf_op jit(solution)/shard_map/all_to_all | solution.py:313
  60.0 0.0 collective-permute-done.h_partner
  60.0 2.9 %expert.1 = bf16[4,128,256]{2,1,0:T(8,128)(2,1)S(1)} custom-call(bf16[4,128,256]{2,1,0:T(8,128)(2,1)S(1)} %all_to_all.27.gathered, f32[1,1024]{1,0:T(1,128)S(1)} %get-tuple-element.13.gain, bf16[1344,1024]{1,0:T(8,128)(2,1)S(1)} %get-tuple-element.14.own, bf16[1344,1024]{1,0:T(8,128)(2,1)} %collective-permute-done.h_partner), custom_call_target="tpu_custom_call" | custom-call | tf_op jit(solution)/shard_map/expert/pallas_call | solution.py:316
  62.9 9.1 %all_to_all.28 = bf16[4,128,256]{2,1,0:T(8,128)(2,1)S(1)} all-to-all(bf16[4,128,256]{2,1,0:T(8,128)(2,1)S(1)} %expert.1), channel_id=1, replica_groups=mesh['ep'=128,'tp'=4] {'tp'}, dimensions={0} | all-to-all | bytes 524288 | tf_op jit(solution)/shard_map/all_to_all | solution.py:329
  72.0 19.0 %all_to_all.29 = bf16[64,2,256]{2,1,0:T(2,128)(2,1)S(1)} all-to-all(bf16[64,2,256]{2,1,0:T(2,128)(2,1)S(1)} %reshape.14), channel_id=1, replica_groups={{0,8,16,24,32,40,48,56,64,72,80,88,96,104,112,120,128,136,144,152,160,1..., dimensions={0} | all-to-all | bytes 131072 | tf_op jit(solution)/shard_map/all_to_all | solution.py:331
  91.0 0.8 combine.1
  (6 shorter events, 0.2 us)
Async XLA Ops:
  4.0 56.0 %collective-permute-start = (bf16[1344,1024]{1,0:T(8,128)(2,1)S(1)}, bf16[1344,1024]{1,0:T(8,128)(2,1)}, u32[]{:S(2)}, u32[]{:S(2)}) collective-permute-start(bf16[1344,1024]{1,0:T(8,128)(2,1)S(1)} %get-tuple-element.14.own), channel_id=1, source_target_pairs={{0,4},{4,0},{8,12},{12,8},{16,20},{20,16},{24,28},{28,24},{32,36},... | collective-permute-start | bytes 8257544 | tf_op jit(solution)/shard_map/ppermute | solution.py:296

commit v8 on v7

--- a/solution.py
+++ b/solution.py
@@ -221,25 +221,30 @@
     meta_out[...] = meta
 
 
-def expert_kernel(gathered, gain, own, h_partner, out, x, partner, sem):
-    copy = pltpu.make_async_copy(h_partner, partner, sem)
-    copy.start()
+def expert_kernel(gathered, gain, own, h_partner, out, x, partner, total, sems):
     tp, rows, quarter = gathered.shape
+    units = own.shape[0] // 3
+    copies = [
+        pltpu.make_async_copy(h_partner.at[here, :], partner.at[here, :], sems.at[n])
+        for n, here in enumerate((slice(0, 2 * units), slice(2 * units, 3 * units)))
+    ]
+    for copy in copies:
+        copy.start()
     values = jnp.concatenate([gathered[t] for t in range(tp)], axis=1).astype(f32)
     x[...] = rms(values, gain[...]).astype(bf16)
-    units = own.shape[0] // 3
-    inners = []
-    for w in (own, partner):
-        if w is partner:
-            copy.wait()
+
+    def inner(w):
         gate = dot(x[...], w[:units, :], NT)
         up = dot(x[...], w[units : 2 * units, :], NT)
-        inners.append((gate / (1.0 + jnp.exp(-gate)) * up).astype(bf16))
+        return (gate / (1.0 + jnp.exp(-gate)) * up).astype(bf16)
+
+    total[...] = dot(inner(own), own[2 * units :, :])
+    copies[0].wait()
+    second = inner(partner)
+    copies[1].wait()
     for t in range(tp):
         here = slice(t * quarter, (t + 1) * quarter)
-        out[t] = (
-            dot(inners[0], own[2 * units :, here]) + dot(inners[1], partner[2 * units :, here])
-        ).astype(bf16)
+        out[t] = (total[:, here] + dot(second, partner[2 * units :, here])).astype(bf16)
 
 
 def combine_kernel(returned, meta, residual, out):
@@ -321,7 +326,8 @@
         scratch_shapes=[
             pltpu.VMEM((rows, width), bf16),
             pltpu.VMEM((3 * units, width), bf16),
-            pltpu.SemaphoreType.DMA(()),
+            pltpu.VMEM((rows, width), f32),
+            pltpu.SemaphoreType.DMA((2,)),
         ],
         compiler_params=pltpu.CompilerParams(vmem_limit_bytes=20 << 20),
         name="expert",

time: 92.1 us -> 91.8 us (level)
  no operation moved by 1% of the time
where the time goes in v8:
time: 91.8 us; the launch traced here: 91.5 us
  blocking collectives  81.6 us (89%)
  Pallas kernels  7.65 us (8%)
  starting transfers between devices  1.92 us (2%)
    all_to_all x1, blocking collectives, per_device(): lax.all_to_all(sent.reshape(experts, 2, quarter), 'ep', 0, 0, axis_index_...  29.9 us
    all_to_all x1, blocking collectives, per_device(): lax.all_to_all(expert_out.reshape(experts, 2, quarter), 'ep', 0, 0, axis_...  19 us
    all_to_all x1, blocking collectives, per_device(): inbox = lax.all_to_all(payload, 'tp', 0, 0, tiled=True)  14.7 us
    all_to_all x1, blocking collectives, per_device(): lax.all_to_all(jnp.broadcast_to(arrived, (tp, rows, quarter)), 'tp', 0, 0...  9.07 us
    all_to_all x1, blocking collectives, per_device(): pieces = lax.all_to_all(partial, 'tp', 0, 0, tiled=True)  9.07 us
    pallas_call x1, Pallas kernels, per_device(): pl.pallas_call(attend_kernel, out_shape=[jax.ShapeDtypeStruct((tp, lines,...  4.02 us
    pallas_call x1, Pallas kernels, per_device(): pl.pallas_call(expert_kernel, out_shape=jax.ShapeDtypeStruct((tp, rows, q...  2.52 us
    ppermute x1, starting transfers between devices, per_device(): partner = lax.ppermute(halves, 'ep', swap)  1.92 us
  transfers between devices with their start and end apart: 1, of which 0 were waited for; matrix products, arithmetic and copies ran while one was open for 0% of the time, Pallas kernels for 0%

profile of v8, /device:TPU:8, one launch (start us, length us, event | category | flops | bytes accessed | tf_op | source)
XLA Modules:
  0.0 91.5 jit_solution(12996005624460424583)
XLA Ops:
  0.0 4.0 %attend.1 = (bf16[4,288,128]{2,1,0:T(8,128)(2,1)S(1)}, f32[1,1024]{1,0:T(1,128)S(1)}, bf16[1344,1024]{1,0:T(8,128)(2,1)S(1)}) custom-call(s32[4]{0:T(128)} %h_lengths.1, f32[1,1024]{1,0:T(1,128)} %bitcast.18, f32[1,256]{1,0:T(1,128)} %bitcast.20, f32[1,128]{1,0:T(1,128)} %bitcast.23, f32[1,1024]{1,0:T(1,128)} %bitcast.19, s32[2,16]{1,0:T(2,128)} %bitcast.21, ...), custom_call_target="tpu_custom_call" | custom-call | tf_op jit(solution)/shard_map/attend/pallas_call | solution.py:286
  4.0 1.9 %collective-permute-start = (bf16[1344,1024]{1,0:T(8,128)(2,1)S(1)}, bf16[1344,1024]{1,0:T(8,128)(2,1)}, u32[]{:S(2)}, u32[]{:S(2)}) collective-permute-start(bf16[1344,1024]{1,0:T(8,128)(2,1)S(1)} %get-tuple-element.14.own), channel_id=1, source_target_pairs={{0,4},{4,0},{8,12},{12,8},{16,20},{20,16},{24,28},{28,24},{32,36},... | collective-permute-start | bytes 8257544 | tf_op jit(solution)/shard_map/ppermute | solution.py:301
  6.0 14.7 %all_to_all.25.inbox = bf16[4,288,128]{2,1,0:T(8,128)(2,1)S(1)} all-to-all(bf16[4,288,128]{2,1,0:T(8,128)(2,1)S(1)} %get-tuple-element.11), channel_id=1, replica_groups=mesh['ep'=128,'tp'=4] {'tp'}, dimensions={0} | all-to-all | bytes 589824 | tf_op jit(solution)/shard_map/all_to_all | solution.py:302
  20.6 0.3 project.1
  21.0 29.9 %all_to_all.26 = bf16[64,2,256]{2,1,0:T(2,128)(2,1)S(1)} all-to-all(bf16[64,2,256]{2,1,0:T(2,128)(2,1)S(1)} %reshape.12), channel_id=1, replica_groups={{0,8,16,24,32,40,48,56,64,72,80,88,96,104,112,120,128,136,144,152,160,1..., dimensions={0} | all-to-all | bytes 131072 | tf_op jit(solution)/shard_map/all_to_all | solution.py:315
  50.9 9.1 %all_to_all.27.gathered = bf16[4,128,256]{2,1,0:T(8,128)(2,1)S(1)} all-to-all(bf16[4,128,256]{2,1,0:T(8,128)(2,1)S(1)} %broadcast_in_dim.19), channel_id=1, replica_groups=mesh['ep'=128,'tp'=4] {'tp'}, dimensions={0} | all-to-all | bytes 524288 | tf_op jit(solution)/shard_map/all_to_all | solution.py:318
  60.0 0.0 collective-permute-done.h_partner
  60.0 2.5 %expert.1 = bf16[4,128,256]{2,1,0:T(8,128)(2,1)S(1)} custom-call(bf16[4,128,256]{2,1,0:T(8,128)(2,1)S(1)} %all_to_all.27.gathered, f32[1,1024]{1,0:T(1,128)S(1)} %get-tuple-element.13.gain, bf16[1344,1024]{1,0:T(8,128)(2,1)S(1)} %get-tuple-element.14.own, bf16[1344,1024]{1,0:T(8,128)(2,1)} %collective-permute-done.h_partner), custom_call_target="tpu_custom_call" | custom-call | tf_op jit(solution)/shard_map/expert/pallas_call | solution.py:321
  62.5 9.1 %all_to_all.28 = bf16[4,128,256]{2,1,0:T(8,128)(2,1)S(1)} all-to-all(bf16[4,128,256]{2,1,0:T(8,128)(2,1)S(1)} %expert.1), channel_id=1, replica_groups=mesh['ep'=128,'tp'=4] {'tp'}, dimensions={0} | all-to-all | bytes 524288 | tf_op jit(solution)/shard_map/all_to_all | solution.py:335
  71.7 19.0 %all_to_all.29 = bf16[64,2,256]{2,1,0:T(2,128)(2,1)S(1)} all-to-all(bf16[64,2,256]{2,1,0:T(2,128)(2,1)S(1)} %reshape.14), channel_id=1, replica_groups={{0,8,16,24,32,40,48,56,64,72,80,88,96,104,112,120,128,136,144,152,160,1..., dimensions={0} | all-to-all | bytes 131072 | tf_op jit(solution)/shard_map/all_to_all | solution.py:337
  90.7 0.8 combine.1
  (6 shorter events, 0.2 us)
Async XLA Ops:
  4.0 56.0 %collective-permute-start = (bf16[1344,1024]{1,0:T(8,128)(2,1)S(1)}, bf16[1344,1024]{1,0:T(8,128)(2,1)}, u32[]{:S(2)}, u32[]{:S(2)}) collective-permute-start(bf16[1344,1024]{1,0:T(8,128)(2,1)S(1)} %get-tuple-element.14.own), channel_id=1, source_target_pairs={{0,4},{4,0},{8,12},{12,8},{16,20},{20,16},{24,28},{28,24},{32,36},... | collective-permute-start | bytes 8257544 | tf_op jit(solution)/shard_map/ppermute | solution.py:301

commit v9 on v8

--- a/solution.py
+++ b/solution.py
@@ -298,8 +298,9 @@
         compiler_params=pltpu.CompilerParams(vmem_limit_bytes=12 << 20),
         name="attend",
     )(*[pltpu.with_memory_space_constraint(a, pltpu.HBM) for a in [*small, *big, *last]])
+    inbox = lax.all_to_all(payload, "tp", 0, 0, tiled=True)
+    inbox, halves = lax.optimization_barrier((inbox, halves))
     partner = lax.ppermute(halves, "ep", swap)
-    inbox = lax.all_to_all(payload, "tp", 0, 0, tiled=True)
     sent, residual, meta = pl.pallas_call(
         project_kernel,
         out_shape=[

time: 91.8 us -> 91.6 us (level)
  the two profiles are of different devices: /device:TPU:8 before, /device:TPU:2 now
where the time goes in v9:
time: 91.6 us; the launch traced here: 91.3 us
  blocking collectives  81.5 us (89%)
  Pallas kernels  7.66 us (8%)
  starting transfers between devices  1.91 us (2%)
    all_to_all x1, blocking collectives, per_device(): lax.all_to_all(sent.reshape(experts, 2, quarter), 'ep', 0, 0, axis_index_...  33 us
    all_to_all x1, blocking collectives, per_device(): lax.all_to_all(expert_out.reshape(experts, 2, quarter), 'ep', 0, 0, axis_...  19 us
    all_to_all x1, blocking collectives, per_device(): inbox = lax.all_to_all(payload, 'tp', 0, 0, tiled=True)  11.3 us
    all_to_all x1, blocking collectives, per_device(): lax.all_to_all(jnp.broadcast_to(arrived, (tp, rows, quarter)), 'tp', 0, 0...  9.07 us
    all_to_all x1, blocking collectives, per_device(): pieces = lax.all_to_all(partial, 'tp', 0, 0, tiled=True)  9.07 us
    pallas_call x1, Pallas kernels, per_device(): pl.pallas_call(attend_kernel, out_shape=[jax.ShapeDtypeStruct((tp, lines,...  4.02 us
    pallas_call x1, Pallas kernels, per_device(): pl.pallas_call(expert_kernel, out_shape=jax.ShapeDtypeStruct((tp, rows, q...  2.53 us
    ppermute x1, starting transfers between devices, per_device(): partner = lax.ppermute(halves, 'ep', swap)  1.91 us
  transfers between devices with their start and end apart: 1, of which 0 were waited for; matrix products, arithmetic and copies ran while one was open for 0% of the time, Pallas kernels for 0%

profile of v9, /device:TPU:2, one launch (start us, length us, event | category | flops | bytes accessed | tf_op | source)
XLA Modules:
  0.0 91.3 jit_solution(6329171045271710607)
XLA Ops:
  0.0 4.0 %attend.1 = (bf16[4,288,128]{2,1,0:T(8,128)(2,1)S(1)}, f32[1,1024]{1,0:T(1,128)S(1)}, bf16[1344,1024]{1,0:T(8,128)(2,1)S(1)}) custom-call(s32[4]{0:T(128)} %h_lengths.1, f32[1,1024]{1,0:T(1,128)} %bitcast.18, f32[1,256]{1,0:T(1,128)} %bitcast.20, f32[1,128]{1,0:T(1,128)} %bitcast.23, f32[1,1024]{1,0:T(1,128)} %bitcast.19, s32[2,16]{1,0:T(2,128)} %bitcast.21, ...), custom_call_target="tpu_custom_call" | custom-call | tf_op jit(solution)/shard_map/attend/pallas_call | solution.py:286
  4.0 11.3 %all_to_all.25.inbox = bf16[4,288,128]{2,1,0:T(8,128)(2,1)S(1)} all-to-all(bf16[4,288,128]{2,1,0:T(8,128)(2,1)S(1)} %get-tuple-element.13), channel_id=1, replica_groups=mesh['ep'=128,'tp'=4] {'tp'}, dimensions={0} | all-to-all | bytes 589824 | tf_op jit(solution)/shard_map/all_to_all | solution.py:301
  15.3 1.9 %collective-permute-start = (bf16[1344,1024]{1,0:T(8,128)(2,1)S(1)}, bf16[1344,1024]{1,0:T(8,128)(2,1)}, u32[]{:S(2)}, u32[]{:S(2)}) collective-permute-start(bf16[1344,1024]{1,0:T(8,128)(2,1)S(1)} %get-tuple-element.18.own), channel_id=1, source_target_pairs={{0,4},{4,0},{8,12},{12,8},{16,20},{20,16},{24,28},{28,24},{32,36},... | collective-permute-start | bytes 8257544 | tf_op jit(solution)/shard_map/ppermute | solution.py:303
  17.2 0.3 project.1
  17.6 33.0 %all_to_all.26 = bf16[64,2,256]{2,1,0:T(2,128)(2,1)S(1)} all-to-all(bf16[64,2,256]{2,1,0:T(2,128)(2,1)S(1)} %reshape.12), channel_id=1, replica_groups={{0,8,16,24,32,40,48,56,64,72,80,88,96,104,112,120,128,136,144,152,160,1..., dimensions={0} | all-to-all | bytes 131072 | tf_op jit(solution)/shard_map/all_to_all | solution.py:316
  50.7 9.1 %all_to_all.27.gathered = bf16[4,128,256]{2,1,0:T(8,128)(2,1)S(1)} all-to-all(bf16[4,128,256]{2,1,0:T(8,128)(2,1)S(1)} %broadcast_in_dim.19), channel_id=1, replica_groups=mesh['ep'=128,'tp'=4] {'tp'}, dimensions={0} | all-to-all | bytes 524288 | tf_op jit(solution)/shard_map/all_to_all | solution.py:319
  59.8 0.0 collective-permute-done.h_partner
  59.8 2.5 %expert.1 = bf16[4,128,256]{2,1,0:T(8,128)(2,1)S(1)} custom-call(bf16[4,128,256]{2,1,0:T(8,128)(2,1)S(1)} %all_to_all.27.gathered, f32[1,1024]{1,0:T(1,128)S(1)} %get-tuple-element.17.gain, bf16[1344,1024]{1,0:T(8,128)(2,1)S(1)} %get-tuple-element.18.own, bf16[1344,1024]{1,0:T(8,128)(2,1)} %collective-permute-done.h_partner), custom_call_target="tpu_custom_call" | custom-call | tf_op jit(solution)/shard_map/expert/pallas_call | solution.py:322
  62.3 9.1 %all_to_all.28 = bf16[4,128,256]{2,1,0:T(8,128)(2,1)S(1)} all-to-all(bf16[4,128,256]{2,1,0:T(8,128)(2,1)S(1)} %expert.1), channel_id=1, replica_groups=mesh['ep'=128,'tp'=4] {'tp'}, dimensions={0} | all-to-all | bytes 524288 | tf_op jit(solution)/shard_map/all_to_all | solution.py:336
  71.5 19.0 %all_to_all.29 = bf16[64,2,256]{2,1,0:T(2,128)(2,1)S(1)} all-to-all(bf16[64,2,256]{2,1,0:T(2,128)(2,1)S(1)} %reshape.14), channel_id=1, replica_groups={{0,8,16,24,32,40,48,56,64,72,80,88,96,104,112,120,128,136,144,152,160,1..., dimensions={0} | all-to-all | bytes 131072 | tf_op jit(solution)/shard_map/all_to_all | solution.py:338
  90.5 0.8 combine.1
  (6 shorter events, 0.2 us)
Async XLA Ops:
  15.3 44.5 %collective-permute-start = (bf16[1344,1024]{1,0:T(8,128)(2,1)S(1)}, bf16[1344,1024]{1,0:T(8,128)(2,1)}, u32[]{:S(2)}, u32[]{:S(2)}) collective-permute-start(bf16[1344,1024]{1,0:T(8,128)(2,1)S(1)} %get-tuple-element.18.own), channel_id=1, source_target_pairs={{0,4},{4,0},{8,12},{12,8},{16,20},{20,16},{24,28},{28,24},{32,36},... | collective-permute-start | bytes 8257544 | tf_op jit(solution)/shard_map/ppermute | solution.py:303
